TPU v7x, 512 devices: a whole 4x4x16 slice. The times are simulated.
512 devices in a mesh: rep: 2 (over z_hi), fs: 32 (over z_lo, y), tp: 8 (over x, core).
Axes of the slice: x: 4, y: 4, z: 16 (z_hi: 2, z_lo: 8; z = z_hi * 8 + z_lo), core: 2. Of those that a mesh axis runs over, the one named last changes fastest.
Arguments:
- tokens_in: bfloat16 [16384, 2048], P(('rep', 'fs', 'tp')), may hold values from -6 to 6
- norm_gains: float32 [3, 2048], replicated, may hold values from 0.1 to 1.9
- gate_w: float32 [2048, 3072], P('fs', 'tp'), may hold values from -0.125 to 0.125
- gate_scale: float32 [3072], P('tp'), may hold values from 0.5 to 2
- up_w: float32 [2048, 3072], P('fs', 'tp'), may hold values from -0.125 to 0.125
- up_scale: float32 [3072], P('tp'), may hold values from 0.5 to 2
- down_w: float32 [3072, 2048], P('tp', 'fs'), may hold values from -0.109375 to 0.109375
- down_scale: float32 [2048], P('fs'), may hold values from 0.5 to 2
- query_w: float32 [2048, 2048], P('fs', 'tp'), may hold values from -0.125 to 0.125
- query_scale: float32 [2048], P('tp'), may hold values from 0.5 to 2
- key_w: float32 [2048, 2048], P('fs', 'tp'), may hold values from -0.125 to 0.125
- key_scale: float32 [2048], P('tp'), may hold values from 0.5 to 2
- value_w: float32 [2048, 2048], P('fs', 'tp'), may hold values from -0.125 to 0.125
- value_scale: float32 [2048], P('tp'), may hold values from 0.5 to 2
- out_w: float32 [2048, 2048], P('tp', 'fs'), may hold values from -0.125 to 0.125
- out_scale: float32 [2048], P('fs'), may hold values from 0.5 to 2
- head_gain: float32 [256], replicated, may hold values from 0.1 to 1.9
- decay_rate: float32 [8], P('tp'), may hold values from 0 to 1, as said below
Outputs:
- tokens_out: bfloat16 [16384, 2048], P(('rep', 'fs', 'tp'))
Inputs may be any that keep to these rules, and one draw needn't show every extreme that they name: `decay_rate`: each head's decay per position, positive.
All inputs are finite; a program needn't handle non-finite values.
Results may differ from a plain program's by a relative error of at most 0.02.
Values may be sent and summed in bfloat16 or wider, within the bound.
No kernel may reach another device: no remote copies, remote signals or barrier semaphores. Data moves between devices by JAX's collectives and lax.ppermute only.
A program may use at most 64 MiB of HBM per device.

v0:
```python
import math

import jax
import jax.numpy as jnp
from jax import lax
from jax.sharding import PartitionSpec as P

DK = 256
DV = 256
BLOCK = 64


EPSILON = 1e-05


def gather_turned(arrays, axis, dims):
    turned = [jnp.moveaxis(a, dim, 0) for a, dim in zip(arrays, dims)]
    widths = [t[0].size for t in turned]
    both = jnp.concatenate([t.reshape(-1, w) for t, w in zip(turned, widths)], axis=1)
    result = lax.all_gather(both, axis, axis=0, tiled=True)
    blocks = jnp.split(result, [sum(widths[:k]) for k in range(1, len(widths))], axis=1)
    return tuple(
        (
            jnp.moveaxis(b.reshape(-1, *t.shape[1:]), 0, dim)
            for b, t, dim in zip(blocks, turned, dims)
        )
    )


def sent_to_all(array, axis):
    copies = jnp.broadcast_to(array, (lax.axis_size(axis), *array.shape))
    return lax.all_to_all(copies, axis, split_axis=0, concat_axis=0, tiled=True)


def in_order(blocks, dim):
    shape = list(blocks.shape[1:])
    shape[dim] *= blocks.shape[0]
    return jnp.moveaxis(blocks, 0, dim).reshape(shape)


def collect(array, axis, dim):
    blocks = sent_to_all(array, axis)
    return in_order(blocks, dim)


def in_blocks(array, dim, devices):
    shape = array.shape
    blocks = array.reshape(*shape[:dim], devices, shape[dim] // devices, *shape[dim + 1 :])
    return jnp.moveaxis(blocks, dim, 0)


def summed_on_arrival(array, axis, dim):
    blocks = in_blocks(array, dim, lax.axis_size(axis))
    arrived = lax.all_to_all(blocks, axis, split_axis=0, concat_axis=0, tiled=True)
    return arrived.astype(jnp.float32).sum(axis=0)


def in_one_piece(arrays, axis, dim, along):
    both = jnp.concatenate(arrays, axis=along)
    result, at, finished = (lax.all_gather(both, axis, axis=dim, tiled=True), 0, [])
    for a in arrays:
        finished.append(lax.slice_in_dim(result, at, at + a.shape[along], axis=along))
        at += a.shape[along]
    return tuple(finished)


def rms_scale(stream, gain):
    return stream * lax.rsqrt(jnp.mean(stream * stream, axis=-1, keepdims=True) + EPSILON) * gain


def retain(query, key_rows, value, decay_rate, head_gain):
    seq_len = query.shape[0]
    blocks = seq_len // BLOCK
    local_heads = decay_rate.shape[0]
    q_heads = query.reshape(blocks, BLOCK, local_heads, DK).transpose(0, 2, 1, 3)
    k_heads = key_rows.reshape(blocks, BLOCK, local_heads, DK).transpose(0, 2, 1, 3)
    v_heads = value.reshape(blocks, BLOCK, local_heads, DV).transpose(0, 2, 1, 3)
    offsets = jnp.arange(BLOCK, dtype=jnp.float32)
    inner_decay = jnp.exp(-decay_rate[:, None, None] * jnp.abs(offsets[:, None] - offsets[None, :]))
    query_decay = jnp.exp(-decay_rate[:, None] * offsets[None, :])[..., None]
    key_decay = jnp.exp(-decay_rate[:, None] * (BLOCK - offsets)[None, :])[..., None]
    block_decay = jnp.exp(-decay_rate * BLOCK)[:, None, None]

    def advance(state, inputs):
        q_blk, k_blk, v_blk = inputs
        scores = (
            jnp.einsum("hid,hjd->hij", q_blk, k_blk, preferred_element_type=jnp.float32)
            * inner_decay
        )
        scores = scores.astype(jnp.bfloat16)
        within = jnp.einsum("hij,hje->hie", scores, v_blk, preferred_element_type=jnp.float32)
        carried = jnp.einsum(
            "hid,hde->hie",
            q_blk.astype(jnp.float32) * query_decay,
            state,
            precision=lax.Precision.HIGHEST,
        )
        k_weighted = k_blk.astype(jnp.float32) * key_decay
        state = state * block_decay + jnp.einsum(
            "hjd,hje->hde", k_weighted, v_blk.astype(jnp.float32), precision=lax.Precision.HIGHEST
        )
        return (state, within + carried)

    initial = jnp.zeros((local_heads, DK, DV), jnp.float32)
    _, retained = lax.scan(advance, initial, (q_heads, k_heads, v_heads))
    retained = retained.transpose(0, 2, 1, 3).reshape(seq_len, local_heads, DV)
    centred = retained - jnp.mean(retained, axis=-1, keepdims=True)
    normed = (
        centred
        * lax.rsqrt(jnp.mean(centred * centred, axis=-1, keepdims=True) + EPSILON)
        * head_gain
    )
    return normed.reshape(seq_len, local_heads * DV).astype(jnp.bfloat16)


def on_device(
    tokens_in,
    norm_gains,
    gate_w,
    gate_scale,
    up_w,
    up_scale,
    down_w,
    down_scale,
    query_w,
    query_scale,
    key_w,
    key_scale,
    value_w,
    value_scale,
    out_w,
    out_scale,
    head_gain,
    decay_rate,
):
    down_cols, out_cols = gather_turned((down_scale, out_scale), "fs", (0, 0))
    gate_b = gate_w.astype(jnp.bfloat16)
    up_b = up_w.astype(jnp.bfloat16)
    down_b = down_w.astype(jnp.bfloat16)
    query_b = query_w.astype(jnp.bfloat16)
    key_b = key_w.astype(jnp.bfloat16)
    value_b = value_w.astype(jnp.bfloat16)
    out_b = out_w.astype(jnp.bfloat16)

    def gather_rows(normed):
        return collect(normed, "tp", 0)

    def return_rows(hidden, weight, scale):
        return summed_on_arrival(
            (jnp.dot(hidden, weight, preferred_element_type=jnp.float32) * scale).astype(
                jnp.bfloat16
            ),
            "tp",
            0,
        )

    def feed_forward(stream, gain, weights):
        gate_full, up_full, down_full = weights
        gathered = gather_rows(rms_scale(stream, gain).astype(jnp.bfloat16))
        gate_value = jnp.dot(gathered, gate_full, preferred_element_type=jnp.float32) * gate_scale
        up_value = jnp.dot(gathered, up_full, preferred_element_type=jnp.float32) * up_scale
        hidden = (jax.nn.silu(gate_value) * up_value).astype(jnp.bfloat16)
        return return_rows(hidden, down_full, down_cols)

    stream = tokens_in.astype(jnp.float32)
    held = gather_turned((gate_b, up_b, down_b), "fs", (0, 0, 1))
    stream = stream + 0.5 * feed_forward(stream, norm_gains[0], held)
    gathered = gather_rows(rms_scale(stream, norm_gains[1]).astype(jnp.bfloat16))
    segments = in_one_piece((query_b, key_b, value_b), "fs", 0, 1)
    query_raw, key_raw, value_raw = tuple(
        (jnp.dot(gathered, segment_w, preferred_element_type=jnp.float32) for segment_w in segments)
    )
    out_full = collect(out_b, "fs", 1)
    query = (query_raw * query_scale).astype(jnp.bfloat16)
    key_rows = (key_raw * key_scale / math.sqrt(DK)).astype(jnp.bfloat16)
    value = (value_raw * value_scale).astype(jnp.bfloat16)
    mixed = retain(query, key_rows, value, decay_rate, head_gain)
    stream = stream + return_rows(mixed, out_full, out_cols)
    stream = stream + 0.5 * feed_forward(stream, norm_gains[2], held)
    return stream.astype(jnp.bfloat16)


def solution(mesh):
    placed = (
        P(("rep", "fs", "tp"), None),
        P(),
        P("fs", "tp"),
        P("tp"),
        P("fs", "tp"),
        P("tp"),
        P("tp", "fs"),
        P("fs"),
        P("fs", "tp"),
        P("tp"),
        P("fs", "tp"),
        P("tp"),
        P("fs", "tp"),
        P("tp"),
        P("tp", "fs"),
        P("fs"),
        P(),
        P("tp"),
    )
    return jax.shard_map(
        on_device,
        mesh=mesh,
        in_specs=placed,
        out_specs=P(("rep", "fs", "tp"), None),
        check_vma=False,
    )
```

profile of v0, /device:TPU:1, one launch (start us, length us, event | category | flops | bytes accessed | tf_op | source)
XLA Modules:
  0.0 551.2 jit_solution(16911982376912300465)
XLA Ops:
  6.5 0.9 convert_bitcast_fusion
  7.4 0.9 convert_element_type.138
  8.3 0.9 convert_element_type.139
  9.2 0.7 pad_maximum_fusion
  10.0 0.8 convert_element_type.145
  10.8 0.9 convert_element_type.146
  11.7 0.8 convert_element_type.147
  12.6 0.6 pad_maximum_fusion.1
  13.2 1.0 fusion.108
  14.3 0.9 fusion.124
  15.2 1.0 fusion.110
  16.2 1.2 broadcast_in_dim.17
  17.4 10.3 %all-to-all-start = ((bf16[8,32,2048]{2,1,0:T(8,128)(2,1)}), bf16[8,32,2048]{2,1,0:T(8,128)(2,1)S(1)}, u32[]{:S(2)}, u32[]{:S(2)}) async-start(bf16[8,32,2048]{2,1,0:T(8,128)(2,1)} %broadcast_in_dim.17), calls=%async_computation | async-start | bytes 2097152 | tf_op jit(solution)/shard_map/all_to_all | solution.py:32
  27.7 107.8 %all-gather = f32[32,64,2]{1,2,0:T(2,128)S(1)} all-gather(f32[1,64,2]{1,2,0:T(2,128)S(1)} %maximum_bitcast_fusion), channel_id=1, replica_groups=mesh['rep'=2,'fs'=32,'tp'=8] {'fs'}, dimensions={0}, use_global_device_ids=true | all-gather | bytes 16896 | tf_op jit(solution)/shard_map/all_gather | solution.py:20
  135.6 87.3 %all-gather.4.cloned.1.call-done = bf16[2048,1152]{1,0:T(8,128)(2,1)} async-done(((bf16[64,1152]{1,0:T(8,128)(2,1)}), bf16[2048,1152]{1,0:T(8,128)(2,1)}) %all-gather.4.cloned.1.call-update) | async-done | bytes 4718608 | tf_op jit(solution)/shard_map/all_gather | solution.py:20
  222.9 2.1 fusion.63
  225.0 3.2 fusion.51
  228.3 40.3 %all_to_all.35 = bf16[8,32,2048]{2,1,0:T(8,128)(2,1)S(1)} all-to-all(bf16[8,32,2048]{2,1,0:T(8,128)(2,1)S(1)} %bitcast.136), channel_id=1, replica_groups=mesh['rep'=2,'fs'=32,'tp'=8] {'tp'}, dimensions={0} | all-to-all | bytes 2097152 | tf_op jit(solution)/shard_map/all_to_all | solution.py:54
  269.1 1.2 broadcast_in_dim.21
  270.3 4.5 all-to-all-start.2
  275.5 14.4 %all-to-all-done.2 = bf16[8,32,2048]{2,1,0:T(8,128)(2,1)S(1)} async-done(((bf16[8,32,2048]{2,1,0:T(8,128)(2,1)}), bf16[8,32,2048]{2,1,0:T(8,128)(2,1)S(1)}, u32[]{:S(2)}, u32[]{:S(2)}) %all-to-all-start.2) | async-done | bytes 1048608 | tf_op jit(solution)/shard_map/all_to_all | solution.py:32
  289.9 1.2 broadcast_in_dim.22
  291.1 11.8 %all-to-all-start.3 = ((bf16[32,256,64]{1,2,0:T(8,128)(2,1)}), bf16[32,256,64]{1,2,0:T(8,128)(2,1)S(1)}, u32[]{:S(2)}, u32[]{:S(2)}) async-start(bf16[32,256,64]{1,2,0:T(8,128)(2,1)} %broadcast_in_dim.22), calls=%async_computation.3 | async-start | bytes 2097152 | tf_op jit(solution)/shard_map/all_to_all | solution.py:32
  302.9 145.8 %all-gather.6.cloned.1.call-done = bf16[2048,768]{1,0:T(8,128)(2,1)} async-done(((bf16[64,768]{1,0:T(8,128)(2,1)}), bf16[2048,768]{1,0:T(8,128)(2,1)}) %all-gather.6.cloned.1.call-update) | async-done | bytes 3145744 | tf_op jit(solution)/shard_map/all_gather | solution.py:60
  448.7 1.7 fusion.92
  450.4 1.7 fusion.93
  452.1 1.7 fusion.94
  453.8 4.5 while.15
  453.8 0.3 fusion.152
  454.2 0.3 fusion.153
  454.4 0.5 fusion.151
  455.0 0.3 fusion.152
  455.3 0.3 fusion.153
  455.5 0.5 fusion.151
  456.1 0.3 fusion.152
  456.4 0.3 fusion.153
  456.7 0.5 fusion.151
  457.2 0.3 fusion.152
  457.5 0.3 fusion.153
  457.8 0.5 fusion.151
  458.5 0.2 multiply_reduce_fusion.1
  458.8 0.5 fusion.50
  459.3 41.5 %all_to_all.36 = bf16[8,32,2048]{2,1,0:T(8,128)(2,1)S(1)} all-to-all(bf16[8,32,2048]{2,1,0:T(8,128)(2,1)S(1)} %bitcast.126), channel_id=1, replica_groups=mesh['rep'=2,'fs'=32,'tp'=8] {'tp'}, dimensions={0} | all-to-all | bytes 2097152 | tf_op jit(solution)/shard_map/all_to_all | solution.py:54
  501.3 18.4 %all_to_all.37 = bf16[8,32,2048]{2,1,0:T(8,128)(2,1)S(1)} all-to-all(bf16[8,32,2048]{2,1,0:T(8,128)(2,1)S(1)} %broadcast_in_dim.23), channel_id=1, replica_groups=mesh['rep'=2,'fs'=32,'tp'=8] {'tp'}, dimensions={0} | all-to-all | bytes 2097152 | tf_op jit(solution)/shard_map/all_to_all | solution.py:32
  519.7 2.1 fusion.66
  521.8 3.3 fusion.52
  525.1 18.4 %all_to_all.38 = bf16[8,32,2048]{2,1,0:T(8,128)(2,1)S(1)} all-to-all(bf16[8,32,2048]{2,1,0:T(8,128)(2,1)S(1)} %bitcast.135), channel_id=1, replica_groups=mesh['rep'=2,'fs'=32,'tp'=8] {'tp'}, dimensions={0} | all-to-all | bytes 2097152 | tf_op jit(solution)/shard_map/all_to_all | solution.py:54
  543.7 0.7 add_convert_fusion
  (53 shorter events, 1.7 us)
Async XLA Ops:
  6.5 216.4 %all-gather.4.cloned.1.call-start = ((), (), s32[]{:S(2)}) async-start(), calls=%async_computation.7 | async-start | bytes 4866048 | tf_op jit(solution)/shard_map/all_gather | solution.py:20
  9.9 438.8 %all-gather.6.cloned.1.call-start = ((), (), s32[]{:S(2)}) async-start(), calls=%async_computation.8 | async-start | bytes 3244032 | tf_op jit(solution)/shard_map/all_gather | solution.py:60
  10.8 16.9 %copy-start.3 = (f32[64]{0:T(128)S(1)}, f32[64]{0:T(128)}, u32[]{:S(2)}) copy-start(f32[64]{0:T(128)} %param.35) | copy-start | bytes 772
  10.8 16.9 %copy-start.4 = (f32[64]{0:T(128)S(1)}, f32[64]{0:T(128)}, u32[]{:S(2)}) copy-start(f32[64]{0:T(128)} %param.27) | copy-start | bytes 772
  12.6 210.4 %copy-start.5 = (f32[384]{0:T(512)S(1)}, f32[384]{0:T(512)}, u32[]{:S(2)}) copy-start(f32[384]{0:T(512)} %param.23) | copy-start | bytes 4612
  17.4 118.2 %all-to-all-start = ((bf16[8,32,2048]{2,1,0:T(8,128)(2,1)}), bf16[8,32,2048]{2,1,0:T(8,128)(2,1)S(1)}, u32[]{:S(2)}, u32[]{:S(2)}) async-start(bf16[8,32,2048]{2,1,0:T(8,128)(2,1)} %broadcast_in_dim.17), calls=%async_computation | async-start | bytes 2097152 | tf_op jit(solution)/shard_map/all_to_all | solution.py:32
  27.7 197.4 %copy-start.6 = (f32[384]{0:T(512)S(1)}, f32[384]{0:T(512)}, u32[]{:S(2)}) copy-start(f32[384]{0:T(512)} %param.25) | copy-start | bytes 4612
  228.3 40.5 %copy-start = (bf16[32,2048]{1,0:T(8,128)(2,1)S(1)}, bf16[32,2048]{1,0:T(8,128)(2,1)}, u32[]{:S(2)}) copy-start(bf16[32,2048]{1,0:T(8,128)(2,1)} %param.20) | copy-start | bytes 393220
  268.8 6.7 %copy-start.1 = (f32[256,64]{0,1:T(8,128)S(1)}, f32[256,64]{0,1:T(8,128)}, u32[]{:S(2)}) copy-start(f32[256,64]{0,1:T(8,128)} %param.34) | copy-start | bytes 196612
  270.3 19.6 %all-to-all-start.2 = ((bf16[8,32,2048]{2,1,0:T(8,128)(2,1)}), bf16[8,32,2048]{2,1,0:T(8,128)(2,1)S(1)}, u32[]{:S(2)}, u32[]{:S(2)}) async-start(bf16[8,32,2048]{2,1,0:T(8,128)(2,1)} %broadcast_in_dim.21), calls=%async_computation.2 | async-start | bytes 2097152 | tf_op jit(solution)/shard_map/all_to_all | solution.py:32
  274.8 173.9 %copy-start.7 = (f32[256]{0:T(256)S(1)}, f32[256]{0:T(256)}, u32[]{:S(2)}) copy-start(f32[256]{0:T(256)} %param.31) | copy-start | bytes 3076
  291.1 159.4 %copy-start.8 = (f32[256]{0:T(256)S(1)}, f32[256]{0:T(256)}, u32[]{:S(2)}) copy-start(f32[256]{0:T(256)} %param.33) | copy-start | bytes 3076
  291.1 167.7 %all-to-all-start.3 = ((bf16[32,256,64]{1,2,0:T(8,128)(2,1)}), bf16[32,256,64]{1,2,0:T(8,128)(2,1)S(1)}, u32[]{:S(2)}, u32[]{:S(2)}) async-start(bf16[32,256,64]{1,2,0:T(8,128)(2,1)} %broadcast_in_dim.22), calls=%async_computation.3 | async-start | bytes 2097152 | tf_op jit(solution)/shard_map/all_to_all | solution.py:32
  448.7 3.4 copy-start.9
  453.8 5.0 copy-start.2
Sparse Core Ops, SparseCore 0:
  10.1 212.8 all-gather.3
  225.0 223.6 all-gather.5
where the time goes:
time: 552 us; the launch traced here: 551 us
  waiting for transfers between devices  248 us (45%)
  blocking collectives  226 us (41%)
  starting transfers between devices  26.7 us (5%)
  matrix products  20.6 us (4%)
  between operations  14.4 us (3%)
  other arithmetic  10.7 us (2%)
    all_gather x1, waiting for transfers between devices, in_one_piece(): lax.all_gather(both, axis, axis=dim, tiled=True)  146 us
    all_gather x1, blocking collectives, gather_turned(): result = lax.all_gather(both, axis, axis=0, tiled=True)  108 us
    all_to_all x3, blocking collectives, summed_on_arrival(): lax.all_to_all(blocks, axis, split_axis=0, concat_axis=0, tiled=True)  100 us
    all_gather x1, waiting for transfers between devices, gather_turned(): result = lax.all_gather(both, axis, axis=0, tiled=True)  87.3 us
    all_to_all x3, starting transfers between devices, sent_to_all(): return lax.all_to_all(copies, axis, split_axis=0, concat_axis=0, tiled=True)  26.6 us
    all_to_all x1, blocking collectives, sent_to_all(): return lax.all_to_all(copies, axis, split_axis=0, concat_axis=0, tiled=True)  18.4 us
    all_to_all x3, waiting for transfers between devices, sent_to_all(): return lax.all_to_all(copies, axis, split_axis=0, concat_axis=0, tiled=True)  14.4 us
  transfers between devices with their start and end apart: 5, of which 3 were waited for; matrix products, arithmetic and copies ran while one was open for 5% of the time, Pallas kernels for 0%

commit v1 on v0

v1 whole, which is shorter than its diff:
```python
import math

import jax
import jax.numpy as jnp
from jax import lax
from jax.sharding import Mesh, PartitionSpec as P

DK = 256
DV = 256
BLOCK = 64
EPSILON = 1e-05


def gather_weights(packed):
    rep = lax.axis_index("rep")
    half = packed.shape[0] // 2
    mine = lax.dynamic_slice_in_dim(packed, rep * half, half, axis=0)
    full = lax.all_gather(mine, ("rep", "z", "y"), axis=0, tiled=True)
    return full.reshape(2, -1, half, packed.shape[1]).transpose(1, 0, 2, 3).reshape(-1, packed.shape[1])


def norm_rows(stream, gain):
    scale = lax.rsqrt(jnp.mean(stream * stream, axis=-1, keepdims=True) + EPSILON)
    return (stream * scale * gain).astype(jnp.bfloat16)


def swap_cores(array):
    return lax.ppermute(array, "core", [(0, 1), (1, 0)])


def gather_rows(rows):
    n = lax.axis_size("x")
    copies = jnp.broadcast_to(rows, (n, *rows.shape))
    own = lax.all_to_all(copies, "x", split_axis=0, concat_axis=0, tiled=True)
    own = own.reshape(-1, rows.shape[1])
    return jnp.concatenate([own, swap_cores(own)], axis=0)


def return_rows(part):
    n = lax.axis_size("x")
    half = part.shape[0] // 2
    sent = swap_cores(part[half:].astype(jnp.bfloat16))
    both = (part[:half] + sent.astype(jnp.float32)).astype(jnp.bfloat16)
    blocks = both.reshape(n, half // n, -1)
    arrived = lax.all_to_all(blocks, "x", split_axis=0, concat_axis=0, tiled=True)
    return arrived.astype(jnp.float32).sum(axis=0)


def dot(a, b):
    return jnp.dot(a, b, preferred_element_type=jnp.float32)


def dot_t(a, b):
    return lax.dot_general(a, b, (((1,), (1,)), ((), ())), preferred_element_type=jnp.float32)


def positions(rows):
    n = lax.axis_size("x")
    core = lax.axis_index("core")
    r = jnp.arange(n * rows, dtype=jnp.int32)
    first = (r // rows) * (2 * rows) + r % rows
    return jnp.concatenate([first + core * rows, first + (1 - core) * rows])


def retain(query, key_rows, value, decay_rate, head_gain, pos):
    apart = jnp.abs(pos[:, None] - pos[None, :]).astype(jnp.float32)
    seen = (pos[None, :] // BLOCK) <= (pos[:, None] // BLOCK)
    decay = jnp.where(seen, jnp.exp(-decay_rate[0] * apart), 0.0)
    scores = (dot_t(query, key_rows) * decay).astype(jnp.bfloat16)
    retained = dot(scores, value)
    centred = retained - jnp.mean(retained, axis=-1, keepdims=True)
    scale = lax.rsqrt(jnp.mean(centred * centred, axis=-1, keepdims=True) + EPSILON)
    return (centred * scale * head_gain).astype(jnp.bfloat16)


def on_device(
    tokens_in, norm_gains, gate_w, gate_scale, up_w, up_scale, down_w, down_scale,
    query_w, query_scale, key_w, key_scale, value_w, value_scale, out_w, out_scale,
    head_gain, decay_rate,
):
    def low(w):
        return w.astype(jnp.bfloat16)

    down_t = low(low(down_w).T.astype(jnp.float32) * down_scale[:, None])
    out_t = low(low(out_w).T.astype(jnp.float32) * out_scale[:, None])
    pieces = [low(gate_w), low(up_w), down_t, low(query_w), low(key_w), low(value_w), out_t]
    packed = jnp.concatenate(pieces, axis=1)
    full = gather_weights(packed)
    at, parts = 0, []
    for p in pieces:
        parts.append(full[:, at : at + p.shape[1]])
        at += p.shape[1]
    gate_f, up_f, down_f, query_f, key_f, value_f, out_f = parts

    def feed_forward(stream, gain):
        rows = gather_rows(norm_rows(stream, gain))
        gate = dot(rows, gate_f) * gate_scale
        up = dot(rows, up_f) * up_scale
        hidden = low(jax.nn.silu(gate) * up)
        return return_rows(dot_t(hidden, down_f))

    stream = tokens_in.astype(jnp.float32)
    stream = stream + 0.5 * feed_forward(stream, norm_gains[0])
    rows = gather_rows(norm_rows(stream, norm_gains[1]))
    query = low(dot(rows, query_f) * query_scale)
    key_rows = low(dot(rows, key_f) * key_scale / math.sqrt(DK))
    value = low(dot(rows, value_f) * value_scale)
    mixed = retain(query, key_rows, value, decay_rate, head_gain, positions(tokens_in.shape[0]))
    stream = stream + return_rows(dot_t(mixed, out_f))
    stream = stream + 0.5 * feed_forward(stream, norm_gains[2])
    return stream.astype(jnp.bfloat16)


def solution(mesh):
    devices = mesh.devices
    reps, fs, tp = devices.shape
    fine = Mesh(devices.reshape(reps, fs // 4, 4, tp // 2, 2), ("rep", "z", "y", "x", "core"))
    F, T = ("z", "y"), ("x", "core")
    rows = P(("rep", "z", "y", "x", "core"), None)
    wide, tall, cols, depth = P(F, T), P(T, F), P(T), P(F)
    placed = (
        rows, P(), wide, cols, wide, cols, tall, depth,
        wide, cols, wide, cols, wide, cols, tall, depth,
        P(), cols,
    )
    return jax.shard_map(on_device, mesh=fine, in_specs=placed, out_specs=rows, check_vma=False)
```

time: 552 us -> 295 us (0.53)
  blocking collectives: 226 us -> 68 us
  waiting for transfers between devices: 248 us -> 140 us
  local copies, waits for them, and re-layouts: 4.9 us -> 11 us
    all_gather x1 -> x0, blocking collectives: 108 us -> none  [gather_turned(): result = lax.all_gather(both, axis, axis=0, tiled=True)]
    all_gather x2 -> x1, waiting for transfers between devices: 233 us -> 133 us  [gather_weights(): full = lax.all_gather(mine, ('rep', 'z', 'y'), axis=0, tiled=True)]
    all_to_all x4 -> x6, blocking collectives: 119 us -> 68 us  [the longest x3 35.6 us: return_rows(): lax.all_to_all(blocks, 'x', split_axis=0, concat_axis=0, tiled=True)]
    ppermute x0 -> x6, starting transfers between devices: none -> 31.4 us  [swap_cores(): return lax.ppermute(array, 'core', [(0, 1), (1, 0)])]
    all_to_all x3 -> x0, starting transfers between devices: 26.6 us -> none  [sent_to_all(): return lax.all_to_all(copies, axis, split_axis=0, concat_axis=0, tiled=True)]
    all_to_all x3 -> x0, waiting for transfers between devices: 14.4 us -> none  [sent_to_all(): return lax.all_to_all(copies, axis, split_axis=0, concat_axis=0, tiled=True)]
    transpose x0 -> x1, local copies, waits for them, and re-layouts: none -> 8.24 us  [gather_weights(): full.reshape(2, -1, half, packed.shape[1]).transpose(1, 0, 2, 3)]
    ppermute x0 -> x6, waiting for transfers between devices: none -> 6.89 us  [swap_cores(): return lax.ppermute(array, 'core', [(0, 1), (1, 0)])]
  transfers between devices with their start and end apart: 5 -> 7, of which waited for: 3 -> 6; matrix products, arithmetic and copies ran while one was open for 5% -> 4% of each run, Pallas kernels for 0% -> 0%
where the time goes in v1:
time: 295 us; the launch traced here: 294 us
  waiting for transfers between devices  140 us (47%)
  blocking collectives  68 us (23%)
  starting transfers between devices  31.4 us (11%)
  matrix products  19.1 us (6%)
  between operations  14.4 us (5%)
  local copies, waits for them, and re-layouts  11 us (4%)
  other arithmetic  10.2 us (3%)
    all_gather x1, waiting for transfers between devices, gather_weights(): full = lax.all_gather(mine, ('rep', 'z', 'y'), axis=0, tiled=True)  133 us
    all_to_all x3, blocking collectives, return_rows(): lax.all_to_all(blocks, 'x', split_axis=0, concat_axis=0, tiled=True)  35.6 us
    all_to_all x3, blocking collectives, gather_rows(): own = lax.all_to_all(copies, 'x', split_axis=0, concat_axis=0, tiled=True)  32.5 us
    ppermute x6, starting transfers between devices, swap_cores(): return lax.ppermute(array, 'core', [(0, 1), (1, 0)])  31.4 us
    dot_general x6, matrix products, dot(): return jnp.dot(a, b, preferred_element_type=jnp.float32)  10.5 us
    dot_general x3, matrix products, dot_t(): lax.dot_general(a, b, (((1,), (1,)), ((), ())), preferred_element_type=jn...  8.57 us
    transpose x1, local copies, waits for them, and re-layouts, gather_weights(): full.reshape(2, -1, half, packed.shape[1]).transpose(1, 0, 2, 3)  8.24 us
    ppermute x6, waiting for transfers between devices, swap_cores(): return lax.ppermute(array, 'core', [(0, 1), (1, 0)])  6.89 us
  transfers between devices with their start and end apart: 7, of which 6 were waited for; matrix products, arithmetic and copies ran while one was open for 4% of the time, Pallas kernels for 0%

profile of v1, /device:TPU:1, one launch (start us, length us, event | category | flops | bytes accessed | tf_op | source)
XLA Modules:
  0.0 294.2 jit_solution(15299229404249725897)
XLA Ops:
  6.5 0.9 convert_dynamic-update-slice_fusion.1
  7.4 0.9 convert_dynamic-update-slice_fusion
  8.3 1.0 fusion.71
  9.3 0.8 convert_dynamic-update-slice_fusion.4
  10.2 0.8 convert_dynamic-update-slice_fusion.3
  11.0 0.8 convert_dynamic-update-slice_fusion.2
  11.9 0.9 fusion.73
  12.8 0.7 constant_dynamic-slice_fusion
  13.5 1.0 fusion.38
  14.6 0.9 fusion.89
  15.5 1.0 fusion.40
  16.5 11.6 %all_to_all.30 = bf16[4,32,2048]{2,1,0:T(8,128)(2,1)S(1)} all-to-all(bf16[4,32,2048]{2,1,0:T(8,128)(2,1)S(1)} %broadcast_in_dim.9), channel_id=1, replica_groups=mesh['rep'=2,'z'=8,'y'=4,'x'=4,'core'=2] {'x'}, dimensions={0} | all-to-all | bytes 1048576 | tf_op jit(solution)/shard_map/all_to_all | solution.py:34
  28.1 7.7 %collective-permute-start = (bf16[128,2048]{1,0:T(8,128)(2,1)S(1)}, bf16[128,2048]{1,0:T(8,128)(2,1)S(1)}, u32[]{:S(2)}, u32[]{:S(2)}) collective-permute-start(bf16[128,2048]{1,0:T(8,128)(2,1)S(1)} %bitcast.41), channel_id=1, source_target_pairs={{0,1},{1,0},{2,3},{3,2},{4,5},{5,4},{6,7},{7,6},{8,9},{9,8},{10,11... | collective-permute-start | bytes 1572872 | tf_op jit(solution)/shard_map/ppermute | solution.py:28
  35.8 133.1 %all-gather.2.cloned.1.call-done = bf16[2048,2176]{1,0:T(8,128)(2,1)} async-done(((bf16[32,2176]{1,0:T(8,128)(2,1)}), bf16[2048,2176]{1,0:T(8,128)(2,1)}) %all-gather.2.cloned.1.call-update) | async-done | bytes 8912912 | tf_op jit(solution)/shard_map/all_gather | solution.py:18
  168.9 8.2 %copy.19 = bf16[32,2,32,2176]{3,2,1,0:T(8,128)(2,1)} copy(bf16[32,2,32,2176]{3,2,0,1:T(8,128)(2,1)} %bitcast.33) | data formatting | bytes 17825792 | tf_op jit(solution)/shard_map/transpose | solution.py:19
  177.1 2.9 fusion.12
  180.1 3.4 %fusion.2 = f32[256,2048]{1,0:T(8,128)S(1)} fusion(bf16[2048,2176]{1,0:T(8,128)(2,1)} %bitcast.26, f32[256,384]{1,0:T(8,128)} %fusion.12, bf16[128,2048]{1,0:T(8,128)(2,1)S(1)} %collective-permute-done, bf16[128,2048]{1,0:T(8,128)(2,1)S(1)} %bitcast.43, f32[384]{0:T(512)S(1)} %copy-done.5), kind=kOutput, calls=%fused_computation.2 | convolution fusion | flops 808091648 | bytes 6686208 | tf_op jit(solution)/shard_map/dot_general | solution.py:54
  183.5 10.4 %collective-permute-start.1 = (bf16[128,2048]{1,0:T(8,128)(2,1)S(1)}, bf16[128,2048]{1,0:T(8,128)(2,1)S(1)}, u32[]{:S(2)}, u32[]{:S(2)}) collective-permute-start(bf16[128,2048]{1,0:T(8,128)(2,1)S(1)} %slice.130), channel_id=1, source_target_pairs={{0,1},{1,0},{2,3},{3,2},{4,5},{5,4},{6,7},{7,6},{8,9},{9,8},{10,11... | collective-permute-start | bytes 1572872 | tf_op jit(solution)/shard_map/ppermute | solution.py:28
  193.9 1.5 collective-permute-done.1
  195.4 0.1 fusion.37
  195.6 12.4 %all_to_all.31 = bf16[4,32,2048]{2,1,0:T(8,128)(2,1)S(1)} all-to-all(bf16[4,32,2048]{2,1,0:T(8,128)(2,1)S(1)} %bitcast.34), channel_id=1, replica_groups=mesh['rep'=2,'z'=8,'y'=4,'x'=4,'core'=2] {'x'}, dimensions={0} | all-to-all | bytes 1048576 | tf_op jit(solution)/shard_map/all_to_all | solution.py:45
  208.0 0.2 multiply_reduce_fusion.2
  208.2 0.1 multiply_convert_fusion.4
  208.3 10.2 %all_to_all.32 = bf16[4,32,2048]{2,1,0:T(8,128)(2,1)S(1)} all-to-all(bf16[4,32,2048]{2,1,0:T(8,128)(2,1)S(1)} %broadcast_in_dim.10), channel_id=1, replica_groups=mesh['rep'=2,'z'=8,'y'=4,'x'=4,'core'=2] {'x'}, dimensions={0} | all-to-all | bytes 1048576 | tf_op jit(solution)/shard_map/all_to_all | solution.py:34
  218.5 4.7 %collective-permute-start.2 = (bf16[128,2048]{1,0:T(8,128)(2,1)S(1)}, bf16[128,2048]{1,0:T(8,128)(2,1)S(1)}, u32[]{:S(2)}, u32[]{:S(2)}) collective-permute-start(bf16[128,2048]{1,0:T(8,128)(2,1)S(1)} %bitcast.37), channel_id=1, source_target_pairs={{0,1},{1,0},{2,3},{3,2},{4,5},{5,4},{6,7},{7,6},{8,9},{9,8},{10,11... | collective-permute-start | bytes 1572872 | tf_op jit(solution)/shard_map/ppermute | solution.py:28
  223.9 0.8 collective-permute-done.2
  224.7 1.7 fusion.26
  226.4 1.7 fusion.25
  228.1 1.7 fusion.27
  229.8 0.5 fusion.90
  230.3 1.8 fusion.32
  232.2 2.3 collective-permute-start.3
  234.5 1.5 collective-permute-done.3
  236.0 0.1 fusion.31
  236.1 11.6 %all_to_all.33 = bf16[4,32,2048]{2,1,0:T(8,128)(2,1)S(1)} all-to-all(bf16[4,32,2048]{2,1,0:T(8,128)(2,1)S(1)} %bitcast.35), channel_id=1, replica_groups=mesh['rep'=2,'z'=8,'y'=4,'x'=4,'core'=2] {'x'}, dimensions={0} | all-to-all | bytes 1048576 | tf_op jit(solution)/shard_map/all_to_all | solution.py:45
  247.8 0.2 multiply_reduce_fusion
  248.0 0.1 multiply_convert_fusion.2
  248.2 10.7 %all_to_all.34 = bf16[4,32,2048]{2,1,0:T(8,128)(2,1)S(1)} all-to-all(bf16[4,32,2048]{2,1,0:T(8,128)(2,1)S(1)} %broadcast_in_dim.12), channel_id=1, replica_groups=mesh['rep'=2,'z'=8,'y'=4,'x'=4,'core'=2] {'x'}, dimensions={0} | all-to-all | bytes 1048576 | tf_op jit(solution)/shard_map/all_to_all | solution.py:34
  258.9 4.1 %collective-permute-start.4 = (bf16[128,2048]{1,0:T(8,128)(2,1)S(1)}, bf16[128,2048]{1,0:T(8,128)(2,1)S(1)}, u32[]{:S(2)}, u32[]{:S(2)}) collective-permute-start(bf16[128,2048]{1,0:T(8,128)(2,1)S(1)} %bitcast.44), channel_id=1, source_target_pairs={{0,1},{1,0},{2,3},{3,2},{4,5},{5,4},{6,7},{7,6},{8,9},{9,8},{10,11... | collective-permute-start | bytes 1572872 | tf_op jit(solution)/shard_map/ppermute | solution.py:28
  263.0 1.5 collective-permute-done.4
  264.5 0.9 copy-done.2
  265.4 2.1 fusion.15
  267.6 3.4 %fusion = f32[256,2048]{1,0:T(8,128)S(1)} fusion(bf16[2048,2176]{1,0:T(8,128)(2,1)} %bitcast.32, f32[256,384]{1,0:T(8,128)S(1)} %fusion.15, bf16[128,2048]{1,0:T(8,128)(2,1)} %copy-done.2, bf16[128,2048]{1,0:T(8,128)(2,1)S(1)} %bitcast.46, f32[384]{0:T(512)S(1)} %copy-done.6), kind=kOutput, calls=%fused_computation | convolution fusion | flops 808091648 | bytes 6686208 | tf_op jit(solution)/shard_map/dot_general | solution.py:54
  271.0 2.3 collective-permute-start.5
  273.3 1.5 collective-permute-done.5
  274.9 0.1 fusion.30
  275.0 11.6 %all_to_all.35 = bf16[4,32,2048]{2,1,0:T(8,128)(2,1)S(1)} all-to-all(bf16[4,32,2048]{2,1,0:T(8,128)(2,1)S(1)} %bitcast.36), channel_id=1, replica_groups=mesh['rep'=2,'z'=8,'y'=4,'x'=4,'core'=2] {'x'}, dimensions={0} | all-to-all | bytes 1048576 | tf_op jit(solution)/shard_map/all_to_all | solution.py:45
  286.7 0.7 add_convert_fusion
  (39 shorter events, 0.7 us)
Async XLA Ops:
  6.5 162.3 %all-gather.2.cloned.1.call-start = ((), (), s32[]{:S(2)}) async-start(), calls=%async_computation.6 | async-start | bytes 9052160 | tf_op jit(solution)/shard_map/all_gather | solution.py:18
  28.1 149.0 %collective-permute-start = (bf16[128,2048]{1,0:T(8,128)(2,1)S(1)}, bf16[128,2048]{1,0:T(8,128)(2,1)S(1)}, u32[]{:S(2)}, u32[]{:S(2)}) collective-permute-start(bf16[128,2048]{1,0:T(8,128)(2,1)S(1)} %bitcast.41), channel_id=1, source_target_pairs={{0,1},{1,0},{2,3},{3,2},{4,5},{5,4},{6,7},{7,6},{8,9},{9,8},{10,11... | collective-permute-start | bytes 1572872 | tf_op jit(solution)/shard_map/ppermute | solution.py:28
  168.9 8.2 %copy-start.3 = (f32[384]{0:T(512)S(1)}, f32[384]{0:T(512)}, u32[]{:S(2)}) copy-start(f32[384]{0:T(512)} %param.21) | copy-start | bytes 4612
  177.1 2.9 %copy-start.5 = (f32[384]{0:T(512)S(1)}, f32[384]{0:T(512)}, u32[]{:S(2)}) copy-start(f32[384]{0:T(512)} %param.23) | copy-start | bytes 4612
  183.5 24.5 %copy-start = (bf16[32,2048]{1,0:T(8,128)(2,1)S(1)}, bf16[32,2048]{1,0:T(8,128)(2,1)}, u32[]{:S(2)}) copy-start(bf16[32,2048]{1,0:T(8,128)(2,1)} %param.18) | copy-start | bytes 393220
  183.5 11.9 %collective-permute-start.1 = (bf16[128,2048]{1,0:T(8,128)(2,1)S(1)}, bf16[128,2048]{1,0:T(8,128)(2,1)S(1)}, u32[]{:S(2)}, u32[]{:S(2)}) collective-permute-start(bf16[128,2048]{1,0:T(8,128)(2,1)S(1)} %slice.130), channel_id=1, source_target_pairs={{0,1},{1,0},{2,3},{3,2},{4,5},{5,4},{6,7},{7,6},{8,9},{9,8},{10,11... | collective-permute-start | bytes 1572872 | tf_op jit(solution)/shard_map/ppermute | solution.py:28
  195.5 29.2 %copy-start.7 = (f32[256]{0:T(256)S(1)}, f32[256]{0:T(256)}, u32[]{:S(2)}) copy-start(f32[256]{0:T(256)} %param.29) | copy-start | bytes 3076
  218.5 7.9 %copy-start.8 = (f32[256]{0:T(256)S(1)}, f32[256]{0:T(256)}, u32[]{:S(2)}) copy-start(f32[256]{0:T(256)} %param.27) | copy-start | bytes 3076
  218.5 6.2 %collective-permute-start.2 = (bf16[128,2048]{1,0:T(8,128)(2,1)S(1)}, bf16[128,2048]{1,0:T(8,128)(2,1)S(1)}, u32[]{:S(2)}, u32[]{:S(2)}) collective-permute-start(bf16[128,2048]{1,0:T(8,128)(2,1)S(1)} %bitcast.37), channel_id=1, source_target_pairs={{0,1},{1,0},{2,3},{3,2},{4,5},{5,4},{6,7},{7,6},{8,9},{9,8},{10,11... | collective-permute-start | bytes 1572872 | tf_op jit(solution)/shard_map/ppermute | solution.py:28
  226.4 1.7 copy-start.9
  228.1 2.2 copy-start.1
  232.2 3.8 %collective-permute-start.3 = (bf16[128,2048]{1,0:T(8,128)(2,1)S(1)}, bf16[128,2048]{1,0:T(8,128)(2,1)S(1)}, u32[]{:S(2)}, u32[]{:S(2)}) collective-permute-start(bf16[128,2048]{1,0:T(8,128)(2,1)S(1)} %slice.129), channel_id=1, source_target_pairs={{0,1},{1,0},{2,3},{3,2},{4,5},{5,4},{6,7},{7,6},{8,9},{9,8},{10,11... | collective-permute-start | bytes 1572872 | tf_op jit(solution)/shard_map/ppermute | solution.py:28
  247.7 17.7 %copy-start.4 = (f32[384]{0:T(512)S(1)}, f32[384]{0:T(512)}, u32[]{:S(2)}) copy-start(f32[384]{0:T(512)} %param.21) | copy-start | bytes 4612
  258.9 8.7 %copy-start.6 = (f32[384]{0:T(512)S(1)}, f32[384]{0:T(512)}, u32[]{:S(2)}) copy-start(f32[384]{0:T(512)} %param.23) | copy-start | bytes 4612
  258.9 5.6 %collective-permute-start.4 = (bf16[128,2048]{1,0:T(8,128)(2,1)S(1)}, bf16[128,2048]{1,0:T(8,128)(2,1)S(1)}, u32[]{:S(2)}, u32[]{:S(2)}) collective-permute-start(bf16[128,2048]{1,0:T(8,128)(2,1)S(1)} %bitcast.44), channel_id=1, source_target_pairs={{0,1},{1,0},{2,3},{3,2},{4,5},{5,4},{6,7},{7,6},{8,9},{9,8},{10,11... | collective-permute-start | bytes 1572872 | tf_op jit(solution)/shard_map/ppermute | solution.py:28
  264.5 0.9 copy-start.2
  271.0 3.8 %collective-permute-start.5 = (bf16[128,2048]{1,0:T(8,128)(2,1)S(1)}, bf16[128,2048]{1,0:T(8,128)(2,1)S(1)}, u32[]{:S(2)}, u32[]{:S(2)}) collective-permute-start(bf16[128,2048]{1,0:T(8,128)(2,1)S(1)} %slice.128), channel_id=1, source_target_pairs={{0,1},{1,0},{2,3},{3,2},{4,5},{5,4},{6,7},{7,6},{8,9},{9,8},{10,11... | collective-permute-start | bytes 1572872 | tf_op jit(solution)/shard_map/ppermute | solution.py:28
Sparse Core Ops, SparseCore 0:
  13.6 155.1 all-gather.1

commit v2 on v1

v2 whole, which is shorter than its diff:
```python
import math

import jax
import jax.numpy as jnp
from jax import lax
from jax.experimental import pallas as pl
from jax.experimental.pallas import tpu as pltpu
from jax.sharding import Mesh, PartitionSpec as P

DK = 256
DV = 256
BLOCK = 64
EPSILON = 1e-05
NZ, NY, NX = 8, 4, 4
ROWS = 32
VMEM = pl.BlockSpec(memory_space=pltpu.VMEM)
SMEM = pl.BlockSpec(memory_space=pltpu.SMEM)
ANY = pl.BlockSpec(memory_space=pl.ANY)


def dot(a, b):
    return jnp.dot(a, b, preferred_element_type=jnp.float32)


def dot_t(a, b):
    return lax.dot_general(a, b, (((1,), (1,)), ((), ())), preferred_element_type=jnp.float32)


def low(w):
    return w.astype(jnp.bfloat16)


def pack_kernel(gate, up, down, ds, query, key, value, out, os, tokens, gain, ffn_ref, mix_ref, rows_ref):
    def column(row):
        n = row.shape[1]
        i = lax.broadcasted_iota(jnp.int32, (n, n), 0)
        j = lax.broadcasted_iota(jnp.int32, (n, n), 1)
        return jnp.sum(jnp.where(i == j, row, 0.0), axis=1, keepdims=True)

    def scaled(w, s):
        return low(low(w[...]).astype(jnp.float32) * column(s[...]))

    n = gate.shape[1]
    ffn_ref[:, :n] = low(gate[...])
    ffn_ref[:, n : 2 * n] = low(up[...])
    ffn_ref[:, 2 * n :] = scaled(down, ds)
    mix = (low(query[...]), low(key[...]), low(value[...]), scaled(out, os))
    for k in range(NY):
        for i, w in enumerate(mix):
            mix_ref[k, :, i * DK : (i + 1) * DK] = w
    stream = tokens[...].astype(jnp.float32)
    scale = lax.rsqrt(jnp.mean(stream * stream, axis=-1, keepdims=True) + EPSILON)
    normed = low(stream * scale * gain[...])
    for k in range(NX):
        rows_ref[k] = normed


def pack(gate, up, down, ds, query, key, value, out, os, tokens, gain):
    rows, n = gate.shape
    return pl.pallas_call(
        pack_kernel,
        out_shape=(
            jax.ShapeDtypeStruct((rows, 3 * n), jnp.bfloat16),
            jax.ShapeDtypeStruct((NY, rows, 4 * DK), jnp.bfloat16),
            jax.ShapeDtypeStruct((NX, *tokens.shape), jnp.bfloat16),
        ),
        in_specs=[VMEM] * 11,
        out_specs=(VMEM,) * 3,
        name="pack",
    )(gate, up, down, ds, query, key, value, out, os, tokens, gain)


def along_z(array, step):
    return lax.ppermute(array, ("rep", "z"), [(g, (g + step) % (2 * NZ)) for g in range(2 * NZ)])


def along_y(array, step):
    return lax.ppermute(array, "y", [(g, (g + step) % NY) for g in range(NY)])


def gather_ffn(mine):
    up, down = [mine], [mine]
    for k in range(4):
        with jax.named_scope(f"ffn_z{k}_up"):
            up.append(along_z(up[-1], 1))
        if k < 3:
            with jax.named_scope(f"ffn_z{k}_down"):
                down.append(along_z(down[-1], -1))
    arrays, owners = [], []

    def spread(name, blocks, dz, cut):
        own = jnp.stack(blocks)
        with jax.named_scope(f"ffn_{name}_up"):
            below = along_y(own, 1)
        with jax.named_scope(f"ffn_{name}_down"):
            above = along_y(own, -1)
        with jax.named_scope(f"ffn_{name}_far_up"):
            far = along_y(below[:cut], 1)
        with jax.named_scope(f"ffn_{name}_far_down"):
            far2 = along_y(above[cut:], -1)
        arrays.extend((own, below, above, far, far2))
        for dy, which in ((0, dz), (-1, dz), (1, dz), (-2, dz[:cut]), (-2, dz[cut:])):
            owners.append([(d, dy) for d in which])

    spread("y0", [mine, up[1], down[1], up[2], down[2]], [0, -1, 1, -2, 2], 3)
    spread("y1", [up[3], down[3], up[4]], [-3, 3, -4], 1)
    return arrays, owners


def gather_mix(copies):
    with jax.named_scope("mix_y"):
        mine = lax.all_to_all(copies, "y", split_axis=0, concat_axis=0, tiled=True)
    mine = mine.reshape(-1, copies.shape[2])
    up, down = [mine], [mine]
    for k in range(4):
        with jax.named_scope(f"mix_z{k}_up"):
            up.append(along_z(up[-1], 1))
        if k < 3:
            with jax.named_scope(f"mix_z{k}_down"):
                down.append(along_z(down[-1], -1))
    return up + down[1:], [0, -1, -2, -3, -4, 1, 2, 3]


def swap_cores(array):
    return lax.ppermute(array, "core", [(0, 1), (1, 0)])


def gather_rows(copies):
    own = lax.all_to_all(copies, "x", split_axis=0, concat_axis=0, tiled=True)
    own = own.reshape(-1, copies.shape[2])
    return own, swap_cores(own)


def return_rows(own, other):
    both = low(own + swap_cores(other).astype(jnp.float32))
    blocks = both.reshape(NX, -1, both.shape[1])
    arrived = lax.all_to_all(blocks, "x", split_axis=0, concat_axis=0, tiled=True)
    return arrived.astype(jnp.float32).sum(axis=0)


def norm_copies(stream, gain):
    scale = lax.rsqrt(jnp.mean(stream * stream, axis=-1, keepdims=True) + EPSILON)
    rows = low(stream * scale * gain)
    return jnp.broadcast_to(rows, (NX, *rows.shape))


def fetch(at, arrays, owners, held, sem, rows):
    copies = []
    for ref, blocks in zip(arrays, owners):
        for i, (dz, dy) in enumerate(blocks):
            row = pl.multiple_of(at(dz, dy) * rows, rows)
            src = ref.at[i] if len(ref.shape) == 3 else ref
            copies.append(pltpu.make_async_copy(src, held.at[pl.ds(row, rows)], sem.at[len(copies)]))
    for c in copies:
        c.start()
    return copies


def ffn_kernel(owners, place, own_rows, other_rows, gs, us, *rest):
    n = len(owners)
    arrays, (own_ref, other_ref, held, sem) = rest[:n], rest[n:]
    z, y = place[0], place[1]

    def at(dz, dy):
        return lax.rem(z + (NZ + dz), NZ) * NY + lax.rem(y + (NY + dy), NY)

    for c in fetch(at, arrays, owners, held, sem, held.shape[0] // (NZ * NY)):
        c.wait()
    units = held.shape[1] // 3
    rows = jnp.concatenate([own_rows[...], other_rows[...]], axis=0)
    gate = dot(rows, held[:, :units]) * gs[...]
    up = dot(rows, held[:, units : 2 * units]) * us[...]
    hidden = low(gate / (1.0 + jnp.exp(-gate)) * up)
    part = dot_t(hidden, held[:, 2 * units :])
    half = own_ref.shape[0]
    own_ref[...] = part[:half]
    other_ref[...] = low(part[half:])


def feed_forward(place, own, other, gate_scale, up_scale, arrays, owners):
    rows, wide = own.shape
    count = sum(len(o) for o in owners)
    own_part, other_part = pl.pallas_call(
        lambda *refs: ffn_kernel(owners, *refs),
        out_shape=(
            jax.ShapeDtypeStruct((rows, wide), jnp.float32),
            jax.ShapeDtypeStruct((rows, wide), jnp.bfloat16),
        ),
        in_specs=[SMEM] + [VMEM] * 4 + [ANY] * len(arrays),
        out_specs=(VMEM, VMEM),
        scratch_shapes=[
            pltpu.VMEM((wide, arrays[0].shape[-1]), jnp.bfloat16),
            pltpu.SemaphoreType.DMA((count,)),
        ],
        compiler_params=pltpu.CompilerParams(vmem_limit_bytes=40 * 1024 * 1024),
        name="ffn",
    )(place, own, other, gate_scale, up_scale, *arrays)
    return return_rows(own_part, other_part)


def mix_kernel(dzs, place, rate, own_rows, other_rows, qs, ks, vs, gain, *rest):
    n = len(dzs)
    arrays, (own_ref, other_ref, held, sem) = rest[:n], rest[n:]
    z, core = place[0], place[2]

    def at(dz, _):
        return lax.rem(z + (NZ + dz), NZ)

    owners = [[(dz, 0)] for dz in dzs]
    for c in fetch(at, arrays, owners, held, sem, held.shape[0] // NZ):
        c.wait()
    rows = jnp.concatenate([own_rows[...], other_rows[...]], axis=0)
    query = low(dot(rows, held[:, :DK]) * qs[...])
    key_rows = low(dot(rows, held[:, DK : 2 * DK]) * ks[...] / math.sqrt(DK))
    value = low(dot(rows, held[:, 2 * DK : 3 * DK]) * vs[...])

    total = rows.shape[0]

    def position(axis):
        r = lax.broadcasted_iota(jnp.int32, (total, total), axis)
        half = r // (total // 2)
        side = jnp.where(half == 0, core, 1 - core)
        return (r % (total // 2)) // ROWS * (2 * ROWS) + side * ROWS + r % ROWS

    pi, pj = position(0), position(1)
    apart = jnp.abs(pi - pj).astype(jnp.float32)
    decay = jnp.where(pj // BLOCK <= pi // BLOCK, jnp.exp(-rate[0] * apart), 0.0)
    scores = low(dot_t(query, key_rows) * decay)
    retained = dot(scores, value)
    centred = retained - jnp.mean(retained, axis=-1, keepdims=True)
    scale = lax.rsqrt(jnp.mean(centred * centred, axis=-1, keepdims=True) + EPSILON)
    mixed = low(centred * scale * gain[...])
    part = dot_t(mixed, held[:, 3 * DK :])
    half = own_ref.shape[0]
    own_ref[...] = part[:half]
    other_ref[...] = low(part[half:])


def mix(place, rate, own, other, scales, head_gain, arrays, dzs):
    rows, wide = own.shape
    own_part, other_part = pl.pallas_call(
        lambda *refs: mix_kernel(dzs, *refs),
        out_shape=(
            jax.ShapeDtypeStruct((rows, wide), jnp.float32),
            jax.ShapeDtypeStruct((rows, wide), jnp.bfloat16),
        ),
        in_specs=[SMEM, SMEM] + [VMEM] * 6 + [ANY] * len(arrays),
        out_specs=(VMEM, VMEM),
        scratch_shapes=[
            pltpu.VMEM((wide, 4 * DK), jnp.bfloat16),
            pltpu.SemaphoreType.DMA((len(arrays),)),
        ],
        compiler_params=pltpu.CompilerParams(vmem_limit_bytes=40 * 1024 * 1024),
        name="mix",
    )(place, rate, own, other, *scales, head_gain, *arrays)
    return return_rows(own_part, other_part)


def on_device(
    tokens_in, norm_gains, gate_w, gate_scale, up_w, up_scale, down_w, down_scale,
    query_w, query_scale, key_w, key_scale, value_w, value_scale, out_w, out_scale,
    head_gain, decay_rate,
):
    def row(v):
        return v.reshape(1, -1)

    place = jnp.stack([lax.axis_index(a).astype(jnp.int32) for a in ("z", "y", "core")])
    ffn_mine, mix_mine, copies = pack(
        gate_w, up_w, down_w.T, row(down_scale), query_w, key_w, value_w, out_w.T, row(out_scale),
        tokens_in, norm_gains[:1],
    )
    ffn_arrays, owners = gather_ffn(ffn_mine)
    with jax.named_scope("rows0"):
        own, other = gather_rows(copies)
    mix_arrays, dzs = gather_mix(mix_mine)
    gs, us = row(gate_scale), row(up_scale)
    scales = (row(query_scale), row(key_scale), row(value_scale))

    stream = tokens_in.astype(jnp.float32)
    stream = stream + 0.5 * feed_forward(place, own, other, gs, us, ffn_arrays, owners)
    own, other = gather_rows(norm_copies(stream, norm_gains[1]))
    stream = stream + mix(place, decay_rate, own, other, scales, row(head_gain), mix_arrays, dzs)
    own, other = gather_rows(norm_copies(stream, norm_gains[2]))
    stream = stream + 0.5 * feed_forward(place, own, other, gs, us, ffn_arrays, owners)
    return stream.astype(jnp.bfloat16)


def solution(mesh):
    devices = mesh.devices
    fine = Mesh(devices.reshape(2, NZ, NY, NX, 2), ("rep", "z", "y", "x", "core"))
    F, T = ("z", "y"), ("x", "core")
    rows = P(("rep", "z", "y", "x", "core"), None)
    wide, tall, cols, depth = P(F, T), P(T, F), P(T), P(F)
    placed = (
        rows, P(), wide, cols, wide, cols, tall, depth,
        wide, cols, wide, cols, wide, cols, tall, depth,
        P(), cols,
    )
    return jax.shard_map(on_device, mesh=fine, in_specs=placed, out_specs=rows, check_vma=False)
```

time: 295 us -> 228 us (0.77)
  waiting for transfers between devices: 140 us -> 30.9 us
  starting transfers between devices: 31.4 us -> 119 us
  blocking collectives: 68 us -> 33.5 us
  Pallas kernels: 0 us -> 26.8 us
  matrix products: 19.1 us -> 0 us
  between operations: 14.4 us -> 1.21 us
  other arithmetic: 10.2 us -> 3.79 us
    all_gather x1 -> x0, waiting for transfers between devices: 133 us -> none  [gather_weights(): full = lax.all_gather(mine, ('rep', 'z', 'y'), axis=0, tiled=True)]
    ppermute x0 -> x22, starting transfers between devices: none -> 76.1 us  [the longest x14 52.5 us: along_z(): lax.ppermute(array, ('rep', 'z'), [(g, (g + step) % (2 * NZ)) for g in ra...]
    pallas_call x0 -> x4, Pallas kernels: none -> 26.8 us  [the longest x2 19 us: feed_forward(): pl.pallas_call(lambda *refs: ffn_kernel(owners, *refs), out_shape=(jax.Sh...]
    ppermute x0 -> x22, waiting for transfers between devices: none -> 23.5 us  [the longest x14 19.7 us: along_z(): lax.ppermute(array, ('rep', 'z'), [(g, (g + step) % (2 * NZ)) for g in ra...]
    all_to_all x3 -> x1, blocking collectives: 32.5 us -> 10.2 us  [gather_rows(): own = lax.all_to_all(copies, 'x', split_axis=0, concat_axis=0, tiled=True)]
    dot_general x9 -> x0, matrix products: 19.1 us -> none  [the longest x6 10.5 us: dot(): return jnp.dot(a, b, preferred_element_type=jnp.float32)]
    all_to_all x0 -> x4, starting transfers between devices: none -> 16.7 us  [the longest x2 8.42 us: gather_rows(): own = lax.all_to_all(copies, 'x', split_axis=0, concat_axis=0, tiled=True)]
    all_to_all x3 -> x2, blocking collectives: 35.6 us -> 23.3 us  [return_rows(): lax.all_to_all(blocks, 'x', split_axis=0, concat_axis=0, tiled=True)]
  transfers between devices with their start and end apart: 7 -> 32, of which waited for: 6 -> 12; matrix products, arithmetic and copies ran while one was open for 4% -> 3% of each run, Pallas kernels for 0% -> 4%
where the time goes in v2:
time: 228 us; the launch traced here: 227 us
  starting transfers between devices  119 us (52%)
  blocking collectives  33.5 us (15%)
  waiting for transfers between devices  30.9 us (14%)
  Pallas kernels  26.8 us (12%)
  local copies, waits for them, and re-layouts  11.9 us (5%)
  other arithmetic  3.79 us (2%)
    ppermute x14, starting transfers between devices, along_z(): lax.ppermute(array, ('rep', 'z'), [(g, (g + step) % (2 * NZ)) for g in ra...  52.5 us
    ppermute x6, starting transfers between devices, swap_cores(): return lax.ppermute(array, 'core', [(0, 1), (1, 0)])  25.9 us
    ppermute x8, starting transfers between devices, along_y(): return lax.ppermute(array, 'y', [(g, (g + step) % NY) for g in range(NY)])  23.6 us
    all_to_all x2, blocking collectives, return_rows(): lax.all_to_all(blocks, 'x', split_axis=0, concat_axis=0, tiled=True)  23.3 us
    ppermute x14, waiting for transfers between devices, along_z(): lax.ppermute(array, ('rep', 'z'), [(g, (g + step) % (2 * NZ)) for g in ra...  19.7 us
    pallas_call x2, Pallas kernels, feed_forward(): pl.pallas_call(lambda *refs: ffn_kernel(owners, *refs), out_shape=(jax.Sh...  19 us
    all_to_all x1, blocking collectives, gather_rows(): own = lax.all_to_all(copies, 'x', split_axis=0, concat_axis=0, tiled=True)  10.2 us
    all_to_all x2, starting transfers between devices, gather_rows(): own = lax.all_to_all(copies, 'x', split_axis=0, concat_axis=0, tiled=True)  8.42 us
  transfers between devices with their start and end apart: 32, of which 12 were waited for; matrix products, arithmetic and copies ran while one was open for 3% of the time, Pallas kernels for 4%

profile of v2, /device:TPU:1, one launch (start us, length us, event | category | flops | bytes accessed | tf_op | source)
XLA Modules:
  0.0 226.8 jit_solution(6342565104140620496)
XLA Ops:
  1.5 2.3 %pack.1 = (bf16[64,1152]{1,0:T(8,128)(2,1)}, bf16[4,64,1024]{2,1,0:T(8,128)(2,1)}, bf16[4,32,2048]{2,1,0:T(8,128)(2,1)}) custom-call(f32[64,384]{1,0:T(8,128)} %gate.1, f32[64,384]{1,0:T(8,128)} %up.1, f32[64,384]{1,0:T(8,128)} %bitcast.45, f32[1,64]{1,0:T(1,128)} %bitcast.49, f32[64,256]{1,0:T(8,128)} %query.1, f32[64,256]{1,0:T(8,128)} %key.1, ...), custom_call_target="tpu_custom_call" | custom-call | tf_op jit(solution)/shard_map/pack/pallas_call | solution.py:60
  3.8 11.9 %collective-permute-start.2 = (bf16[64,1152]{1,0:T(8,128)(2,1)}, bf16[64,1152]{1,0:T(8,128)(2,1)S(1)}, u32[]{:S(2)}, u32[]{:S(2)}) collective-permute-start(bf16[64,1152]{1,0:T(8,128)(2,1)} %get-tuple-element.15), channel_id=1, source_target_pairs={{0,480},{32,0},{64,32},{96,64},{128,96},{160,128},{192,160},{224,1... | collective-permute-start | bytes 442376 | tf_op jit(solution)/shard_map/ffn_z0_down/ppermute | solution.py:74
  15.8 1.9 collective-permute-start.1
  18.6 5.2 %collective-permute-start.4 = (bf16[64,1152]{1,0:T(8,128)(2,1)S(1)}, bf16[64,1152]{1,0:T(8,128)(2,1)S(1)}, u32[]{:S(2)}, u32[]{:S(2)}) collective-permute-start(bf16[64,1152]{1,0:T(8,128)(2,1)S(1)} %collective-permute-done.2), channel_id=1, source_target_pairs={{0,480},{32,0},{64,32},{96,64},{128,96},{160,128},{192,160},{224,1... | collective-permute-start | bytes 442376 | tf_op jit(solution)/shard_map/ffn_z1_down/ppermute | solution.py:74
  23.8 1.9 collective-permute-start.3
  25.8 5.1 %collective-permute-done.3 = bf16[64,1152]{1,0:T(8,128)(2,1)S(1)} collective-permute-done((bf16[64,1152]{1,0:T(8,128)(2,1)S(1)}, bf16[64,1152]{1,0:T(8,128)(2,1)S(1)}, u32[]{:S(2)}, u32[]{:S(2)}) %collective-permute-start.3) | collective-permute-done | bytes 147488 | tf_op jit(solution)/shard_map/ffn_z1_up/ppermute | solution.py:74
  30.9 1.9 collective-permute-start.9
  32.9 3.2 %collective-permute-start.5 = (bf16[5,64,1152]{2,1,0:T(8,128)(2,1)S(1)}, bf16[5,64,1152]{2,1,0:T(8,128)(2,1)S(1)}, u32[]{:S(2)}, u32[]{:S(2)}) collective-permute-start(bf16[5,64,1152]{2,1,0:T(8,128)(2,1)S(1)} %bitcast_dynamic-update-slice_fusion.refs_5_), channel_id=1, source_target_pairs={{0,8},{8,16},{16,24},{24,0},{1,9},{9,17},{17,25},{25,1},{2,10},{10... | collective-permute-start | bytes 2211848 | tf_op jit(solution)/shard_map/ffn_y0_up/ppermute | solution.py:78
  36.1 4.6 %collective-permute-start.10 = (bf16[64,1152]{1,0:T(8,128)(2,1)S(1)}, bf16[64,1152]{1,0:T(8,128)(2,1)S(1)}, u32[]{:S(2)}, u32[]{:S(2)}) collective-permute-start(bf16[64,1152]{1,0:T(8,128)(2,1)S(1)} %collective-permute-done.4), channel_id=1, source_target_pairs={{0,480},{32,0},{64,32},{96,64},{128,96},{160,128},{192,160},{224,1... | collective-permute-start | bytes 442376 | tf_op jit(solution)/shard_map/ffn_z2_down/ppermute | solution.py:74
  40.7 1.9 collective-permute-start.11
  42.6 3.4 %collective-permute-start.6 = (bf16[5,64,1152]{2,1,0:T(8,128)(2,1)S(1)}, bf16[5,64,1152]{2,1,0:T(8,128)(2,1)S(1)}, u32[]{:S(2)}, u32[]{:S(2)}) collective-permute-start(bf16[5,64,1152]{2,1,0:T(8,128)(2,1)S(1)} %bitcast_dynamic-update-slice_fusion.refs_5_), channel_id=1, source_target_pairs={{0,24},{8,0},{16,8},{24,16},{1,25},{9,1},{17,9},{25,17},{2,26},{10... | collective-permute-start | bytes 2211848 | tf_op jit(solution)/shard_map/ffn_y0_down/ppermute | solution.py:78
  46.0 4.2 %all-to-all-start = ((bf16[4,32,2048]{2,1,0:T(8,128)(2,1)}), bf16[4,32,2048]{2,1,0:T(8,128)(2,1)}, u32[]{:S(2)}, u32[]{:S(2)}) async-start(bf16[4,32,2048]{2,1,0:T(8,128)(2,1)} %get-tuple-element.14), calls=%async_computation | async-start | bytes 1048576 | tf_op jit(solution)/shard_map/rows0/all_to_all | solution.py:129
  50.2 3.4 %collective-permute-start.13 = (bf16[3,64,1152]{2,1,0:T(8,128)(2,1)S(1)}, bf16[3,64,1152]{2,1,0:T(8,128)(2,1)S(1)}, u32[]{:S(2)}, u32[]{:S(2)}) collective-permute-start(bf16[3,64,1152]{2,1,0:T(8,128)(2,1)S(1)} %pad_maximum_fusion.refs_10_), channel_id=1, source_target_pairs={{0,24},{8,0},{16,8},{24,16},{1,25},{9,1},{17,9},{25,17},{2,26},{10... | collective-permute-start | bytes 1327112 | tf_op jit(solution)/shard_map/ffn_y1_down/ppermute | solution.py:78
  53.6 1.9 collective-permute-start.12
  55.5 1.6 all-to-all-done
  57.1 7.2 %collective-permute-start = (bf16[128,2048]{1,0:T(8,128)(2,1)}, bf16[128,2048]{1,0:T(8,128)(2,1)}, u32[]{:S(2)}, u32[]{:S(2)}) collective-permute-start(bf16[128,2048]{1,0:T(8,128)(2,1)} %bitcast.7.refs_1_), channel_id=1, source_target_pairs={{0,1},{1,0},{2,3},{3,2},{4,5},{5,4},{6,7},{7,6},{8,9},{9,8},{10,11... | collective-permute-start | bytes 1572872 | tf_op jit(solution)/shard_map/rows0/ppermute | solution.py:125
  65.2 2.0 collective-permute-start.7
  67.2 4.1 %all-to-all-start.3 = ((bf16[4,64,1024]{2,1,0:T(8,128)(2,1)}), bf16[4,64,1024]{2,1,0:T(8,128)(2,1)}, u32[]{:S(2)}, u32[]{:S(2)}) async-start(bf16[4,64,1024]{2,1,0:T(8,128)(2,1)} %get-tuple-element.18), calls=%async_computation.3 | async-start | bytes 1048576 | tf_op jit(solution)/shard_map/mix_y/all_to_all | solution.py:112
  72.1 4.5 %collective-permute-start.15 = (bf16[2,64,1152]{2,1,0:T(8,128)(2,1)}, bf16[2,64,1152]{2,1,0:T(8,128)(2,1)}, u32[]{:S(2)}, u32[]{:S(2)}) collective-permute-start(bf16[2,64,1152]{2,1,0:T(8,128)(2,1)} %slice.31), channel_id=1, source_target_pairs={{0,24},{8,0},{16,8},{24,16},{1,25},{9,1},{17,9},{25,17},{2,26},{10... | collective-permute-start | bytes 884744 | tf_op jit(solution)/shard_map/ffn_y1_far_down/ppermute | solution.py:78
  77.4 2.5 %collective-permute-start.8 = (bf16[2,64,1152]{2,1,0:T(8,128)(2,1)}, bf16[2,64,1152]{2,1,0:T(8,128)(2,1)}, u32[]{:S(2)}, u32[]{:S(2)}) collective-permute-start(bf16[2,64,1152]{2,1,0:T(8,128)(2,1)} %slice.29), channel_id=1, source_target_pairs={{0,24},{8,0},{16,8},{24,16},{1,25},{9,1},{17,9},{25,17},{2,26},{10... | collective-permute-start | bytes 884744 | tf_op jit(solution)/shard_map/ffn_y0_far_down/ppermute | solution.py:78
  80.5 2.8 %collective-permute-start.14 = (bf16[1,64,1152]{2,1,0:T(8,128)(2,1)}, bf16[1,64,1152]{2,1,0:T(8,128)(2,1)}, u32[]{:S(2)}, u32[]{:S(2)}) collective-permute-start(bf16[1,64,1152]{2,1,0:T(8,128)(2,1)} %slice.30), channel_id=1, source_target_pairs={{0,8},{8,16},{16,24},{24,0},{1,9},{9,17},{17,25},{25,1},{2,10},{10... | collective-permute-start | bytes 442376 | tf_op jit(solution)/shard_map/ffn_y1_far_up/ppermute | solution.py:78
  86.0 1.9 collective-permute-start.18
  88.1 3.7 %collective-permute-done.8.refs_9_ = bf16[2,64,1152]{2,1,0:T(8,128)(2,1)} collective-permute-done((bf16[2,64,1152]{2,1,0:T(8,128)(2,1)}, bf16[2,64,1152]{2,1,0:T(8,128)(2,1)}, u32[]{:S(2)}, u32[]{:S(2)}) %collective-permute-start.8) | collective-permute-done | bytes 294944 | tf_op jit(solution)/shard_map/ffn_y0_far_down/ppermute | solution.py:78
  91.7 9.8 %ffn.2 = (f32[128,2048]{1,0:T(8,128)S(1)}, bf16[128,2048]{1,0:T(8,128)(2,1)S(1)}) custom-call(s32[3]{0:T(128)S(1)} %pad_add_fusion.refs_0_, bf16[128,2048]{1,0:T(8,128)(2,1)} %bitcast.7.refs_1_, bf16[128,2048]{1,0:T(8,128)(2,1)} %collective-permute-done.refs_2_, f32[1,384]{1,0:T(1,128)S(1)} %reshape.64.refs_3_, f32[1,384]{1,0:T(1,128)S(1)} %reshape.65.refs_4_, ...), custom_call_target="tpu_custom_call" | custom-call | tf_op jit(solution)/shard_map/ffn/pallas_call | solution.py:183
  101.6 3.1 %collective-permute-start.16 = (bf16[128,2048]{1,0:T(8,128)(2,1)S(1)}, bf16[128,2048]{1,0:T(8,128)(2,1)S(1)}, u32[]{:S(2)}, u32[]{:S(2)}) collective-permute-start(bf16[128,2048]{1,0:T(8,128)(2,1)S(1)} %get-tuple-element.17), channel_id=1, source_target_pairs={{0,1},{1,0},{2,3},{3,2},{4,5},{5,4},{6,7},{7,6},{8,9},{9,8},{10,11... | collective-permute-start | bytes 1572872 | tf_op jit(solution)/shard_map/ppermute | solution.py:125
  104.7 4.9 %collective-permute-start.22 = (bf16[256,1024]{1,0:T(8,128)(2,1)}, bf16[256,1024]{1,0:T(8,128)(2,1)}, u32[]{:S(2)}, u32[]{:S(2)}) collective-permute-start(bf16[256,1024]{1,0:T(8,128)(2,1)} %bitcast.23.refs_8_), channel_id=1, source_target_pairs={{0,480},{32,0},{64,32},{96,64},{128,96},{160,128},{192,160},{224,1... | collective-permute-start | bytes 1572872 | tf_op jit(solution)/shard_map/mix_z0_down/ppermute | solution.py:74
  109.6 1.9 collective-permute-start.19
  112.4 4.1 %all-to-all-start.1 = ((bf16[4,32,2048]{2,1,0:T(8,128)(2,1)}), bf16[4,32,2048]{2,1,0:T(8,128)(2,1)}, u32[]{:S(2)}, u32[]{:S(2)}) async-start(bf16[4,32,2048]{2,1,0:T(8,128)(2,1)} %bitcast.39), calls=%async_computation.1 | async-start | bytes 1048576 | tf_op jit(solution)/shard_map/all_to_all | solution.py:137
  116.6 4.6 %collective-permute-done.22.refs_13_ = bf16[256,1024]{1,0:T(8,128)(2,1)} collective-permute-done((bf16[256,1024]{1,0:T(8,128)(2,1)}, bf16[256,1024]{1,0:T(8,128)(2,1)}, u32[]{:S(2)}, u32[]{:S(2)}) %collective-permute-start.22) | collective-permute-done | bytes 524320 | tf_op jit(solution)/shard_map/mix_z0_down/ppermute | solution.py:74
  121.1 5.3 %collective-permute-start.23 = (bf16[256,1024]{1,0:T(8,128)(2,1)}, bf16[256,1024]{1,0:T(8,128)(2,1)}, u32[]{:S(2)}, u32[]{:S(2)}) collective-permute-start(bf16[256,1024]{1,0:T(8,128)(2,1)} %collective-permute-done.22.refs_13_), channel_id=1, source_target_pairs={{0,480},{32,0},{64,32},{96,64},{128,96},{160,128},{192,160},{224,1... | collective-permute-start | bytes 1572872 | tf_op jit(solution)/shard_map/mix_z1_down/ppermute | solution.py:74
  126.5 1.9 collective-permute-start.20
  131.3 4.3 %all-to-all-start.2 = ((bf16[4,32,2048]{2,1,0:T(8,128)(2,1)}), bf16[4,32,2048]{2,1,0:T(8,128)(2,1)}, u32[]{:S(2)}, u32[]{:S(2)}) async-start(bf16[4,32,2048]{2,1,0:T(8,128)(2,1)} %broadcast_in_dim.8), calls=%async_computation.2 | async-start | bytes 1048576 | tf_op jit(solution)/shard_map/all_to_all | solution.py:129
  135.6 1.6 collective-permute-done.23.refs_14_
  137.2 5.3 %collective-permute-start.24 = (bf16[256,1024]{1,0:T(8,128)(2,1)}, bf16[256,1024]{1,0:T(8,128)(2,1)}, u32[]{:S(2)}, u32[]{:S(2)}) collective-permute-start(bf16[256,1024]{1,0:T(8,128)(2,1)} %collective-permute-done.23.refs_14_), channel_id=1, source_target_pairs={{0,480},{32,0},{64,32},{96,64},{128,96},{160,128},{192,160},{224,1... | collective-permute-start | bytes 1572872 | tf_op jit(solution)/shard_map/mix_z2_down/ppermute | solution.py:74
  142.5 1.9 collective-permute-start.21
  144.4 3.9 %collective-permute-start.17 = (bf16[128,2048]{1,0:T(8,128)(2,1)}, bf16[128,2048]{1,0:T(8,128)(2,1)S(1)}, u32[]{:S(2)}, u32[]{:S(2)}) collective-permute-start(bf16[128,2048]{1,0:T(8,128)(2,1)} %bitcast.18.refs_2_), channel_id=1, source_target_pairs={{0,1},{1,0},{2,3},{3,2},{4,5},{5,4},{6,7},{7,6},{8,9},{9,8},{10,11... | collective-permute-start | bytes 1572872 | tf_op jit(solution)/shard_map/ppermute | solution.py:125
  149.0 3.3 %collective-permute-done.24.refs_15_ = bf16[256,1024]{1,0:T(8,128)(2,1)} collective-permute-done((bf16[256,1024]{1,0:T(8,128)(2,1)}, bf16[256,1024]{1,0:T(8,128)(2,1)}, u32[]{:S(2)}, u32[]{:S(2)}) %collective-permute-start.24) | collective-permute-done | bytes 524320 | tf_op jit(solution)/shard_map/mix_z2_down/ppermute | solution.py:74
  152.3 5.1 %collective-permute-done.21.refs_12_ = bf16[256,1024]{1,0:T(8,128)(2,1)} collective-permute-done((bf16[256,1024]{1,0:T(8,128)(2,1)}, bf16[256,1024]{1,0:T(8,128)(2,1)}, u32[]{:S(2)}, u32[]{:S(2)}) %collective-permute-start.21) | collective-permute-done | bytes 524320 | tf_op jit(solution)/shard_map/mix_z3_up/ppermute | solution.py:74
  159.4 5.5 %mix.1 = (f32[128,2048]{1,0:T(8,128)S(1)}, bf16[128,2048]{1,0:T(8,128)(2,1)S(1)}) custom-call(s32[3]{0:T(128)S(1)} %pad_add_fusion.refs_0_, f32[1]{0:T(128)S(6)} %copy.23.refs_1_, bf16[128,2048]{1,0:T(8,128)(2,1)} %bitcast.18.refs_2_, bf16[128,2048]{1,0:T(8,128)(2,1)S(1)} %collective-permute-done.17.refs_3_, f32[1,256]{1,0:T(1,128)S(1)} %bitcast.35, ...), custom_call_target="tpu_custom_call" | custom-call | tf_op jit(solution)/shard_map/mix/pallas_call | solution.py:241
  165.0 4.8 %collective-permute-start.25 = (bf16[128,2048]{1,0:T(8,128)(2,1)S(1)}, bf16[128,2048]{1,0:T(8,128)(2,1)S(1)}, u32[]{:S(2)}, u32[]{:S(2)}) collective-permute-start(bf16[128,2048]{1,0:T(8,128)(2,1)S(1)} %get-tuple-element.20), channel_id=1, source_target_pairs={{0,1},{1,0},{2,3},{3,2},{4,5},{5,4},{6,7},{7,6},{8,9},{9,8},{10,11... | collective-permute-start | bytes 1572872 | tf_op jit(solution)/shard_map/ppermute | solution.py:125
  169.7 1.5 collective-permute-done.25
  171.4 11.7 %all_to_all.35 = bf16[4,32,2048]{2,1,0:T(8,128)(2,1)S(1)} all-to-all(bf16[4,32,2048]{2,1,0:T(8,128)(2,1)S(1)} %bitcast.40), channel_id=1, replica_groups=mesh['rep'=2,'z'=8,'y'=4,'x'=4,'core'=2] {'x'}, dimensions={0} | all-to-all | bytes 1048576 | tf_op jit(solution)/shard_map/all_to_all | solution.py:137
  185.1 10.2 %all_to_all.36 = bf16[4,32,2048]{2,1,0:T(8,128)(2,1)S(1)} all-to-all(bf16[4,32,2048]{2,1,0:T(8,128)(2,1)S(1)} %broadcast_in_dim.9), channel_id=1, replica_groups=mesh['rep'=2,'z'=8,'y'=4,'x'=4,'core'=2] {'x'}, dimensions={0} | all-to-all | bytes 1048576 | tf_op jit(solution)/shard_map/all_to_all | solution.py:129
  195.2 4.6 %collective-permute-start.26 = (bf16[128,2048]{1,0:T(8,128)(2,1)S(1)}, bf16[128,2048]{1,0:T(8,128)(2,1)S(1)}, u32[]{:S(2)}, u32[]{:S(2)}) collective-permute-start(bf16[128,2048]{1,0:T(8,128)(2,1)S(1)} %bitcast.33), channel_id=1, source_target_pairs={{0,1},{1,0},{2,3},{3,2},{4,5},{5,4},{6,7},{7,6},{8,9},{9,8},{10,11... | collective-permute-start | bytes 1572872 | tf_op jit(solution)/shard_map/ppermute | solution.py:125
  201.3 9.2 %ffn.3 = (f32[128,2048]{1,0:T(8,128)S(1)}, bf16[128,2048]{1,0:T(8,128)(2,1)S(1)}) custom-call(s32[3]{0:T(128)S(1)} %pad_add_fusion.refs_0_, bf16[128,2048]{1,0:T(8,128)(2,1)S(1)} %bitcast.34, bf16[128,2048]{1,0:T(8,128)(2,1)S(1)} %collective-permute-done.26.refs_2_, f32[1,384]{1,0:T(1,128)S(1)} %reshape.64.refs_3_, f32[1,384]{1,0:T(1,128)S(1)} %reshape.65.refs_4_, ...), custom_call_target="tpu_custom_call" | custom-call | tf_op jit(solution)/shard_map/ffn/pallas_call | solution.py:183
  210.5 2.3 %collective-permute-start.27 = (bf16[128,2048]{1,0:T(8,128)(2,1)S(1)}, bf16[128,2048]{1,0:T(8,128)(2,1)S(1)}, u32[]{:S(2)}, u32[]{:S(2)}) collective-permute-start(bf16[128,2048]{1,0:T(8,128)(2,1)S(1)} %get-tuple-element.22), channel_id=1, source_target_pairs={{0,1},{1,0},{2,3},{3,2},{4,5},{5,4},{6,7},{7,6},{8,9},{9,8},{10,11... | collective-permute-start | bytes 1572872 | tf_op jit(solution)/shard_map/ppermute | solution.py:125
  212.8 1.5 collective-permute-done.27
  214.4 11.6 %all_to_all.37 = bf16[4,32,2048]{2,1,0:T(8,128)(2,1)S(1)} all-to-all(bf16[4,32,2048]{2,1,0:T(8,128)(2,1)S(1)} %bitcast.41), channel_id=1, replica_groups=mesh['rep'=2,'z'=8,'y'=4,'x'=4,'core'=2] {'x'}, dimensions={0} | all-to-all | bytes 1048576 | tf_op jit(solution)/shard_map/all_to_all | solution.py:137
  (76 shorter events, 18.6 us)
Async XLA Ops:
  3.8 14.8 %collective-permute-start.2 = (bf16[64,1152]{1,0:T(8,128)(2,1)}, bf16[64,1152]{1,0:T(8,128)(2,1)S(1)}, u32[]{:S(2)}, u32[]{:S(2)}) collective-permute-start(bf16[64,1152]{1,0:T(8,128)(2,1)} %get-tuple-element.15), channel_id=1, source_target_pairs={{0,480},{32,0},{64,32},{96,64},{128,96},{160,128},{192,160},{224,1... | collective-permute-start | bytes 442376 | tf_op jit(solution)/shard_map/ffn_z0_down/ppermute | solution.py:74
  15.8 8.0 %collective-permute-start.1 = (bf16[64,1152]{1,0:T(8,128)(2,1)}, bf16[64,1152]{1,0:T(8,128)(2,1)S(1)}, u32[]{:S(2)}, u32[]{:S(2)}) collective-permute-start(bf16[64,1152]{1,0:T(8,128)(2,1)} %get-tuple-element.15), channel_id=1, source_target_pairs={{0,32},{32,64},{64,96},{96,128},{128,160},{160,192},{192,224},{224... | collective-permute-start | bytes 442376 | tf_op jit(solution)/shard_map/ffn_z0_up/ppermute | solution.py:74
  18.6 14.2 %collective-permute-start.4 = (bf16[64,1152]{1,0:T(8,128)(2,1)S(1)}, bf16[64,1152]{1,0:T(8,128)(2,1)S(1)}, u32[]{:S(2)}, u32[]{:S(2)}) collective-permute-start(bf16[64,1152]{1,0:T(8,128)(2,1)S(1)} %collective-permute-done.2), channel_id=1, source_target_pairs={{0,480},{32,0},{64,32},{96,64},{128,96},{160,128},{192,160},{224,1... | collective-permute-start | bytes 442376 | tf_op jit(solution)/shard_map/ffn_z1_down/ppermute | solution.py:74
  23.8 7.1 %collective-permute-start.3 = (bf16[64,1152]{1,0:T(8,128)(2,1)S(1)}, bf16[64,1152]{1,0:T(8,128)(2,1)S(1)}, u32[]{:S(2)}, u32[]{:S(2)}) collective-permute-start(bf16[64,1152]{1,0:T(8,128)(2,1)S(1)} %collective-permute-done.1), channel_id=1, source_target_pairs={{0,32},{32,64},{64,96},{96,128},{128,160},{160,192},{192,224},{224... | collective-permute-start | bytes 442376 | tf_op jit(solution)/shard_map/ffn_z1_up/ppermute | solution.py:74
  30.9 9.8 %collective-permute-start.9 = (bf16[64,1152]{1,0:T(8,128)(2,1)S(1)}, bf16[64,1152]{1,0:T(8,128)(2,1)S(1)}, u32[]{:S(2)}, u32[]{:S(2)}) collective-permute-start(bf16[64,1152]{1,0:T(8,128)(2,1)S(1)} %collective-permute-done.3), channel_id=1, source_target_pairs={{0,32},{32,64},{64,96},{96,128},{128,160},{160,192},{192,224},{224... | collective-permute-start | bytes 442376 | tf_op jit(solution)/shard_map/ffn_z2_up/ppermute | solution.py:74
  32.9 31.5 %collective-permute-start.5 = (bf16[5,64,1152]{2,1,0:T(8,128)(2,1)S(1)}, bf16[5,64,1152]{2,1,0:T(8,128)(2,1)S(1)}, u32[]{:S(2)}, u32[]{:S(2)}) collective-permute-start(bf16[5,64,1152]{2,1,0:T(8,128)(2,1)S(1)} %bitcast_dynamic-update-slice_fusion.refs_5_), channel_id=1, source_target_pairs={{0,8},{8,16},{16,24},{24,0},{1,9},{9,17},{17,25},{25,1},{2,10},{10... | collective-permute-start | bytes 2211848 | tf_op jit(solution)/shard_map/ffn_y0_up/ppermute | solution.py:78
  36.1 14.0 %collective-permute-start.10 = (bf16[64,1152]{1,0:T(8,128)(2,1)S(1)}, bf16[64,1152]{1,0:T(8,128)(2,1)S(1)}, u32[]{:S(2)}, u32[]{:S(2)}) collective-permute-start(bf16[64,1152]{1,0:T(8,128)(2,1)S(1)} %collective-permute-done.4), channel_id=1, source_target_pairs={{0,480},{32,0},{64,32},{96,64},{128,96},{160,128},{192,160},{224,1... | collective-permute-start | bytes 442376 | tf_op jit(solution)/shard_map/ffn_z2_down/ppermute | solution.py:74
  40.7 9.5 %collective-permute-start.11 = (bf16[64,1152]{1,0:T(8,128)(2,1)S(1)}, bf16[64,1152]{1,0:T(8,128)(2,1)S(1)}, u32[]{:S(2)}, u32[]{:S(2)}) collective-permute-start(bf16[64,1152]{1,0:T(8,128)(2,1)S(1)} %collective-permute-done.9), channel_id=1, source_target_pairs={{0,32},{32,64},{64,96},{96,128},{128,160},{160,192},{192,224},{224... | collective-permute-start | bytes 442376 | tf_op jit(solution)/shard_map/ffn_z3_up/ppermute | solution.py:74
  42.6 34.0 %collective-permute-start.6 = (bf16[5,64,1152]{2,1,0:T(8,128)(2,1)S(1)}, bf16[5,64,1152]{2,1,0:T(8,128)(2,1)S(1)}, u32[]{:S(2)}, u32[]{:S(2)}) collective-permute-start(bf16[5,64,1152]{2,1,0:T(8,128)(2,1)S(1)} %bitcast_dynamic-update-slice_fusion.refs_5_), channel_id=1, source_target_pairs={{0,24},{8,0},{16,8},{24,16},{1,25},{9,1},{17,9},{25,17},{2,26},{10... | collective-permute-start | bytes 2211848 | tf_op jit(solution)/shard_map/ffn_y0_down/ppermute | solution.py:78
  46.0 11.2 %all-to-all-start = ((bf16[4,32,2048]{2,1,0:T(8,128)(2,1)}), bf16[4,32,2048]{2,1,0:T(8,128)(2,1)}, u32[]{:S(2)}, u32[]{:S(2)}) async-start(bf16[4,32,2048]{2,1,0:T(8,128)(2,1)} %get-tuple-element.14), calls=%async_computation | async-start | bytes 1048576 | tf_op jit(solution)/shard_map/rows0/all_to_all | solution.py:129
  50.2 21.1 %collective-permute-start.13 = (bf16[3,64,1152]{2,1,0:T(8,128)(2,1)S(1)}, bf16[3,64,1152]{2,1,0:T(8,128)(2,1)S(1)}, u32[]{:S(2)}, u32[]{:S(2)}) collective-permute-start(bf16[3,64,1152]{2,1,0:T(8,128)(2,1)S(1)} %pad_maximum_fusion.refs_10_), channel_id=1, source_target_pairs={{0,24},{8,0},{16,8},{24,16},{1,25},{9,1},{17,9},{25,17},{2,26},{10... | collective-permute-start | bytes 1327112 | tf_op jit(solution)/shard_map/ffn_y1_down/ppermute | solution.py:78
  53.6 26.2 %collective-permute-start.12 = (bf16[3,64,1152]{2,1,0:T(8,128)(2,1)S(1)}, bf16[3,64,1152]{2,1,0:T(8,128)(2,1)S(1)}, u32[]{:S(2)}, u32[]{:S(2)}) collective-permute-start(bf16[3,64,1152]{2,1,0:T(8,128)(2,1)S(1)} %pad_maximum_fusion.refs_10_), channel_id=1, source_target_pairs={{0,8},{8,16},{16,24},{24,0},{1,9},{9,17},{17,25},{25,1},{2,10},{10... | collective-permute-start | bytes 1327112 | tf_op jit(solution)/shard_map/ffn_y1_up/ppermute | solution.py:78
  57.1 28.9 %collective-permute-start = (bf16[128,2048]{1,0:T(8,128)(2,1)}, bf16[128,2048]{1,0:T(8,128)(2,1)}, u32[]{:S(2)}, u32[]{:S(2)}) collective-permute-start(bf16[128,2048]{1,0:T(8,128)(2,1)} %bitcast.7.refs_1_), channel_id=1, source_target_pairs={{0,1},{1,0},{2,3},{3,2},{4,5},{5,4},{6,7},{7,6},{8,9},{9,8},{10,11... | collective-permute-start | bytes 1572872 | tf_op jit(solution)/shard_map/rows0/ppermute | solution.py:125
  65.2 26.5 %collective-permute-start.7 = (bf16[3,64,1152]{2,1,0:T(8,128)(2,1)}, bf16[3,64,1152]{2,1,0:T(8,128)(2,1)}, u32[]{:S(2)}, u32[]{:S(2)}) collective-permute-start(bf16[3,64,1152]{2,1,0:T(8,128)(2,1)} %slice.28), channel_id=1, source_target_pairs={{0,8},{8,16},{16,24},{24,0},{1,9},{9,17},{17,25},{25,1},{2,10},{10... | collective-permute-start | bytes 1327112 | tf_op jit(solution)/shard_map/ffn_y0_far_up/ppermute | solution.py:78
  67.2 18.8 %all-to-all-start.3 = ((bf16[4,64,1024]{2,1,0:T(8,128)(2,1)}), bf16[4,64,1024]{2,1,0:T(8,128)(2,1)}, u32[]{:S(2)}, u32[]{:S(2)}) async-start(bf16[4,64,1024]{2,1,0:T(8,128)(2,1)} %get-tuple-element.18), calls=%async_computation.3 | async-start | bytes 1048576 | tf_op jit(solution)/shard_map/mix_y/all_to_all | solution.py:112
  72.1 16.0 %collective-permute-start.15 = (bf16[2,64,1152]{2,1,0:T(8,128)(2,1)}, bf16[2,64,1152]{2,1,0:T(8,128)(2,1)}, u32[]{:S(2)}, u32[]{:S(2)}) collective-permute-start(bf16[2,64,1152]{2,1,0:T(8,128)(2,1)} %slice.31), channel_id=1, source_target_pairs={{0,24},{8,0},{16,8},{24,16},{1,25},{9,1},{17,9},{25,17},{2,26},{10... | collective-permute-start | bytes 884744 | tf_op jit(solution)/shard_map/ffn_y1_far_down/ppermute | solution.py:78
  77.4 14.4 %collective-permute-start.8 = (bf16[2,64,1152]{2,1,0:T(8,128)(2,1)}, bf16[2,64,1152]{2,1,0:T(8,128)(2,1)}, u32[]{:S(2)}, u32[]{:S(2)}) collective-permute-start(bf16[2,64,1152]{2,1,0:T(8,128)(2,1)} %slice.29), channel_id=1, source_target_pairs={{0,24},{8,0},{16,8},{24,16},{1,25},{9,1},{17,9},{25,17},{2,26},{10... | collective-permute-start | bytes 884744 | tf_op jit(solution)/shard_map/ffn_y0_far_down/ppermute | solution.py:78
  80.5 7.6 %collective-permute-start.14 = (bf16[1,64,1152]{2,1,0:T(8,128)(2,1)}, bf16[1,64,1152]{2,1,0:T(8,128)(2,1)}, u32[]{:S(2)}, u32[]{:S(2)}) collective-permute-start(bf16[1,64,1152]{2,1,0:T(8,128)(2,1)} %slice.30), channel_id=1, source_target_pairs={{0,8},{8,16},{16,24},{24,0},{1,9},{9,17},{17,25},{25,1},{2,10},{10... | collective-permute-start | bytes 442376 | tf_op jit(solution)/shard_map/ffn_y1_far_up/ppermute | solution.py:78
  83.3 0.7 copy-start.10
  84.0 0.7 copy-start.11
  86.0 23.6 %collective-permute-start.18 = (bf16[256,1024]{1,0:T(8,128)(2,1)}, bf16[256,1024]{1,0:T(8,128)(2,1)}, u32[]{:S(2)}, u32[]{:S(2)}) collective-permute-start(bf16[256,1024]{1,0:T(8,128)(2,1)} %bitcast.23.refs_8_), channel_id=1, source_target_pairs={{0,32},{32,64},{64,96},{96,128},{128,160},{160,192},{192,224},{224... | collective-permute-start | bytes 1572872 | tf_op jit(solution)/shard_map/mix_z0_up/ppermute | solution.py:74
  101.6 10.0 %collective-permute-start.16 = (bf16[128,2048]{1,0:T(8,128)(2,1)S(1)}, bf16[128,2048]{1,0:T(8,128)(2,1)S(1)}, u32[]{:S(2)}, u32[]{:S(2)}) collective-permute-start(bf16[128,2048]{1,0:T(8,128)(2,1)S(1)} %get-tuple-element.17), channel_id=1, source_target_pairs={{0,1},{1,0},{2,3},{3,2},{4,5},{5,4},{6,7},{7,6},{8,9},{9,8},{10,11... | collective-permute-start | bytes 1572872 | tf_op jit(solution)/shard_map/ppermute | solution.py:125
  104.7 16.4 %collective-permute-start.22 = (bf16[256,1024]{1,0:T(8,128)(2,1)}, bf16[256,1024]{1,0:T(8,128)(2,1)}, u32[]{:S(2)}, u32[]{:S(2)}) collective-permute-start(bf16[256,1024]{1,0:T(8,128)(2,1)} %bitcast.23.refs_8_), channel_id=1, source_target_pairs={{0,480},{32,0},{64,32},{96,64},{128,96},{160,128},{192,160},{224,1... | collective-permute-start | bytes 1572872 | tf_op jit(solution)/shard_map/mix_z0_down/ppermute | solution.py:74
  109.6 16.9 %collective-permute-start.19 = (bf16[256,1024]{1,0:T(8,128)(2,1)}, bf16[256,1024]{1,0:T(8,128)(2,1)}, u32[]{:S(2)}, u32[]{:S(2)}) collective-permute-start(bf16[256,1024]{1,0:T(8,128)(2,1)} %collective-permute-done.18.refs_9_), channel_id=1, source_target_pairs={{0,32},{32,64},{64,96},{96,128},{128,160},{160,192},{192,224},{224... | collective-permute-start | bytes 1572872 | tf_op jit(solution)/shard_map/mix_z1_up/ppermute | solution.py:74
  112.4 16.0 %all-to-all-start.1 = ((bf16[4,32,2048]{2,1,0:T(8,128)(2,1)}), bf16[4,32,2048]{2,1,0:T(8,128)(2,1)}, u32[]{:S(2)}, u32[]{:S(2)}) async-start(bf16[4,32,2048]{2,1,0:T(8,128)(2,1)} %bitcast.39), calls=%async_computation.1 | async-start | bytes 1048576 | tf_op jit(solution)/shard_map/all_to_all | solution.py:137
  121.1 16.0 %collective-permute-start.23 = (bf16[256,1024]{1,0:T(8,128)(2,1)}, bf16[256,1024]{1,0:T(8,128)(2,1)}, u32[]{:S(2)}, u32[]{:S(2)}) collective-permute-start(bf16[256,1024]{1,0:T(8,128)(2,1)} %collective-permute-done.22.refs_13_), channel_id=1, source_target_pairs={{0,480},{32,0},{64,32},{96,64},{128,96},{160,128},{192,160},{224,1... | collective-permute-start | bytes 1572872 | tf_op jit(solution)/shard_map/mix_z1_down/ppermute | solution.py:74
  126.5 16.0 %collective-permute-start.20 = (bf16[256,1024]{1,0:T(8,128)(2,1)}, bf16[256,1024]{1,0:T(8,128)(2,1)}, u32[]{:S(2)}, u32[]{:S(2)}) collective-permute-start(bf16[256,1024]{1,0:T(8,128)(2,1)} %collective-permute-done.19.refs_10_), channel_id=1, source_target_pairs={{0,32},{32,64},{64,96},{96,128},{128,160},{160,192},{192,224},{224... | collective-permute-start | bytes 1572872 | tf_op jit(solution)/shard_map/mix_z2_up/ppermute | solution.py:74
  128.4 1.2 copy-start.6
  129.6 0.8 copy-start.4
  129.6 0.7 copy-start.8
  131.3 26.1 %copy-start.1 = (f32[256]{0:T(256)S(1)}, f32[256]{0:T(256)}, u32[]{:S(2)}) copy-start(f32[256]{0:T(256)} %param.29) | copy-start | bytes 3076
  131.3 13.1 %all-to-all-start.2 = ((bf16[4,32,2048]{2,1,0:T(8,128)(2,1)}), bf16[4,32,2048]{2,1,0:T(8,128)(2,1)}, u32[]{:S(2)}, u32[]{:S(2)}) async-start(bf16[4,32,2048]{2,1,0:T(8,128)(2,1)} %broadcast_in_dim.8), calls=%async_computation.2 | async-start | bytes 1048576 | tf_op jit(solution)/shard_map/all_to_all | solution.py:129
  137.2 15.2 %collective-permute-start.24 = (bf16[256,1024]{1,0:T(8,128)(2,1)}, bf16[256,1024]{1,0:T(8,128)(2,1)}, u32[]{:S(2)}, u32[]{:S(2)}) collective-permute-start(bf16[256,1024]{1,0:T(8,128)(2,1)} %collective-permute-done.23.refs_14_), channel_id=1, source_target_pairs={{0,480},{32,0},{64,32},{96,64},{128,96},{160,128},{192,160},{224,1... | collective-permute-start | bytes 1572872 | tf_op jit(solution)/shard_map/mix_z2_down/ppermute | solution.py:74
  142.5 14.9 %collective-permute-start.21 = (bf16[256,1024]{1,0:T(8,128)(2,1)}, bf16[256,1024]{1,0:T(8,128)(2,1)}, u32[]{:S(2)}, u32[]{:S(2)}) collective-permute-start(bf16[256,1024]{1,0:T(8,128)(2,1)} %collective-permute-done.20.refs_11_), channel_id=1, source_target_pairs={{0,32},{32,64},{64,96},{96,128},{128,160},{160,192},{192,224},{224... | collective-permute-start | bytes 1572872 | tf_op jit(solution)/shard_map/mix_z3_up/ppermute | solution.py:74
  144.4 13.0 %collective-permute-start.17 = (bf16[128,2048]{1,0:T(8,128)(2,1)}, bf16[128,2048]{1,0:T(8,128)(2,1)S(1)}, u32[]{:S(2)}, u32[]{:S(2)}) collective-permute-start(bf16[128,2048]{1,0:T(8,128)(2,1)} %bitcast.18.refs_2_), channel_id=1, source_target_pairs={{0,1},{1,0},{2,3},{3,2},{4,5},{5,4},{6,7},{7,6},{8,9},{9,8},{10,11... | collective-permute-start | bytes 1572872 | tf_op jit(solution)/shard_map/ppermute | solution.py:125
  157.4 0.7 copy-start
  158.1 0.7 copy-start.2
  158.8 0.7 copy-start.3
  165.0 6.3 %collective-permute-start.25 = (bf16[128,2048]{1,0:T(8,128)(2,1)S(1)}, bf16[128,2048]{1,0:T(8,128)(2,1)S(1)}, u32[]{:S(2)}, u32[]{:S(2)}) collective-permute-start(bf16[128,2048]{1,0:T(8,128)(2,1)S(1)} %get-tuple-element.20), channel_id=1, source_target_pairs={{0,1},{1,0},{2,3},{3,2},{4,5},{5,4},{6,7},{7,6},{8,9},{9,8},{10,11... | collective-permute-start | bytes 1572872 | tf_op jit(solution)/shard_map/ppermute | solution.py:125
  183.1 1.0 copy-start.5
  183.1 1.0 copy-start.7
  184.2 0.7 copy-start.9
  195.2 6.1 %collective-permute-start.26 = (bf16[128,2048]{1,0:T(8,128)(2,1)S(1)}, bf16[128,2048]{1,0:T(8,128)(2,1)S(1)}, u32[]{:S(2)}, u32[]{:S(2)}) collective-permute-start(bf16[128,2048]{1,0:T(8,128)(2,1)S(1)} %bitcast.33), channel_id=1, source_target_pairs={{0,1},{1,0},{2,3},{3,2},{4,5},{5,4},{6,7},{7,6},{8,9},{9,8},{10,11... | collective-permute-start | bytes 1572872 | tf_op jit(solution)/shard_map/ppermute | solution.py:125
  210.5 3.8 %collective-permute-start.27 = (bf16[128,2048]{1,0:T(8,128)(2,1)S(1)}, bf16[128,2048]{1,0:T(8,128)(2,1)S(1)}, u32[]{:S(2)}, u32[]{:S(2)}) collective-permute-start(bf16[128,2048]{1,0:T(8,128)(2,1)S(1)} %get-tuple-element.22), channel_id=1, source_target_pairs={{0,1},{1,0},{2,3},{3,2},{4,5},{5,4},{6,7},{7,6},{8,9},{9,8},{10,11... | collective-permute-start | bytes 1572872 | tf_op jit(solution)/shard_map/ppermute | solution.py:125

commit v3 on v2

v3 whole, which is shorter than its diff:
```python
import math

import jax
import jax.numpy as jnp
from jax import lax
from jax.experimental import pallas as pl
from jax.experimental.pallas import tpu as pltpu
from jax.sharding import Mesh, PartitionSpec as P


DK = 256
BLOCK = 64
EPSILON = 1e-05
NZ, NY, NX = 8, 4, 4
ROWS = 32
VMEM = pl.BlockSpec(memory_space=pltpu.VMEM)
SMEM = pl.BlockSpec(memory_space=pltpu.SMEM)
ANY = pl.BlockSpec(memory_space=pl.ANY)


def dot(a, b):
    return jnp.dot(a, b, preferred_element_type=jnp.float32)


def dot_t(a, b):
    return lax.dot_general(a, b, (((1,), (1,)), ((), ())), preferred_element_type=jnp.float32)


def low(w):
    return w.astype(jnp.bfloat16)


NEAR = (0, -1, 1, -2, 2)
DISTANT = (-3, 3, -4)
SIDES = (0, -1, 1, 2)
RING = (0, -1, -2, -3, -4, 1, 2, 3)


def plain(dz, dy):
    return dz % NZ * NY + dy % NY


FFN_ORDER = [plain(dz, dy) for dzs in (NEAR, DISTANT) for dy in SIDES for dz in dzs]
MIX_ORDER = [plain(dz, dy) for dz in RING for dy in range(NY)]
PLAIN_TO_FFN = FFN_ORDER
FFN_TO_PLAIN = [FFN_ORDER.index(b) for b in range(NZ * NY)]
FFN_TO_MIX = [FFN_ORDER.index(b) for b in MIX_ORDER]
MIX_TO_FFN = [MIX_ORDER.index(b) for b in FFN_ORDER]


def joined(tiles):
    (a, turn_a), (b, turn_b) = tiles
    lane = lax.broadcasted_iota(jnp.int32, a.shape, 1)
    a, b = (
        jnp.where(t, pltpu.roll(v, 64, 1), v) if not isinstance(t, bool) else (pltpu.roll(v, 64, 1) if t else v)
        for v, t in ((a, turn_a), (b, turn_b))
    )
    return jnp.where(lane < 64, a, b)


def shuffled(value, order):
    tiles = []
    for p, q in zip(order[::2], order[1::2]):
        a, b = (value[:, i // 2 * 128 : i // 2 * 128 + 128] for i in (p, q))
        tiles.append(joined(((a, p % 2 == 1), (b, q % 2 == 0))))
    return jnp.concatenate(tiles, axis=1)


def turned(ref, z, y):
    tiles = []
    for t in range(NZ * NY // 2):
        pair = []
        for half in range(2):
            b = 2 * t + half
            side = lax.rem(b % NY + y, NY)
            at = pl.multiple_of((lax.rem(b // NY + z, NZ) * (NY // 2) + side // 2) * 128, 128)
            pair.append((ref[:, pl.ds(at, 128)].astype(jnp.float32), side % 2 != half))
        tiles.append(joined(pair))
    return jnp.concatenate(tiles, axis=1)


def normed(stream, gain):
    scale = lax.rsqrt(jnp.mean(stream * stream, axis=-1, keepdims=True) + EPSILON)
    return low(stream * scale * gain)


def pack_kernel(place, gate, up, down, ds, query, key, value, out, os, tokens, gains, *rest):
    small, (ffn_ref, mix_ref, rows_ref, small_ref, stream_ref, gains_ref) = rest[:-6], rest[-6:]

    def column(row):
        n = row.shape[1]
        i = lax.broadcasted_iota(jnp.int32, (n, n), 0)
        j = lax.broadcasted_iota(jnp.int32, (n, n), 1)
        return jnp.sum(jnp.where(i == j, row, 0.0), axis=1, keepdims=True)

    def scaled(w, s):
        return low(low(w[...]).astype(jnp.float32) * column(s[...]))

    n = gate.shape[1]
    ffn_ref[:, :n] = low(gate[...])
    ffn_ref[:, n : 2 * n] = low(up[...])
    ffn_ref[:, 2 * n :] = scaled(down, ds)
    mix = (low(query[...]), low(key[...]), low(value[...]), scaled(out, os))
    for k in range(NY):
        for i, w in enumerate(mix):
            mix_ref[k, :, i * DK : (i + 1) * DK] = w
    z, y = place[0], place[1]
    stream = shuffled(turned(tokens, z, y), PLAIN_TO_FFN)
    ordered = shuffled(turned(gains, z, y), PLAIN_TO_FFN)
    stream_ref[...] = low(stream)
    gains_ref[...] = ordered
    first = normed(stream, ordered[:1, :])
    for k in range(rows_ref.shape[0]):
        rows_ref[k] = first
    for i, v in enumerate(small):
        small_ref[i : i + 1, : v.shape[1]] = v[...]


def pack(place, gate, up, down, ds, query, key, value, out, os, tokens, gains, small):
    rows, n = gate.shape
    return pl.pallas_call(
        pack_kernel,
        out_shape=(
            jax.ShapeDtypeStruct((rows, 3 * n), jnp.bfloat16),
            jax.ShapeDtypeStruct((NY, rows, 4 * DK), jnp.bfloat16),
            jax.ShapeDtypeStruct((2 * NX, *tokens.shape), jnp.bfloat16),
            jax.ShapeDtypeStruct((8, n), jnp.float32),
            jax.ShapeDtypeStruct(tokens.shape, jnp.bfloat16),
            jax.ShapeDtypeStruct(gains.shape, jnp.float32),
        ),
        in_specs=[SMEM] + [VMEM] * (11 + len(small)),
        out_specs=(VMEM,) * 6,
        compiler_params=pltpu.CompilerParams(vmem_limit_bytes=12 * 1024 * 1024),
        name="pack",
    )(place, gate, up, down, ds, query, key, value, out, os, tokens, gains, *small)


def join_kernel(weight, which, arrived_as, rows_as, place, arrived, stream, gains, next_ref, last_ref):
    total = arrived[0].astype(jnp.float32)
    for k in range(1, NX):
        total = total + arrived[k].astype(jnp.float32)
    if arrived_as is not None:
        total = shuffled(total, arrived_as)
    total = stream[...].astype(jnp.float32) + weight * total
    if which is None:
        z, y = place[0], place[1]
        last_ref[...] = shuffled(total, FFN_TO_PLAIN)
        next_ref[...] = low(turned(last_ref, NZ - z, NY - y))
        return
    next_ref[...] = total
    rows = total * lax.rsqrt(jnp.mean(total * total, axis=-1, keepdims=True) + EPSILON)
    rows = rows * gains[which : which + 1, :]
    if rows_as is not None:
        rows = shuffled(rows, rows_as)
    rows = low(rows)
    for k in range(NX):
        last_ref[k] = rows


def join(place, weight, which, arrived, stream, gains, arrived_as=None, rows_as=None):
    shape = stream.shape
    last = which is None
    outs = [jax.ShapeDtypeStruct(shape, jnp.bfloat16 if last else jnp.float32)]
    if not last:
        outs.append(jax.ShapeDtypeStruct((NX, *shape), jnp.bfloat16))
    return pl.pallas_call(
        lambda *refs: join_kernel(weight, which, arrived_as, rows_as, *refs),
        out_shape=outs,
        in_specs=[SMEM] + [VMEM] * 3,
        out_specs=[VMEM] * len(outs),
        scratch_shapes=[pltpu.VMEM(shape, jnp.float32)] if last else [],
        compiler_params=pltpu.CompilerParams(vmem_limit_bytes=8 * 1024 * 1024),
        name="join",
    )(place, arrived, stream, gains)


def along_z(array, step):
    return lax.ppermute(array, ("rep", "z"), [(g, (g + step) % (2 * NZ)) for g in range(2 * NZ)])


def along_y(array, step):
    return lax.ppermute(array, "y", [(g, (g + step) % NY) for g in range(NY)])


def gather_ffn(mine):
    u1, d1 = along_z(mine, 1), along_z(mine, -1)
    u2, d2 = along_z(u1, 1), along_z(d1, -1)
    u3, d3 = along_z(u1, 2), along_z(d1, -2)
    u4 = along_z(u2, 2)
    arrays = []

    def spread(blocks, far_up):
        own = jnp.stack(blocks)
        below = along_y(own, 1)
        above = along_y(own, -1)
        far = along_y(below, 1) if far_up else along_y(above, -1)
        arrays.extend((own, below, above, far))

    spread([mine, u1, d1, u2, d2], True)
    spread([u3, d3, u4], False)
    return arrays


def gather_mix(copies):
    mine = lax.all_to_all(copies, "y", split_axis=0, concat_axis=0, tiled=True)
    mine = lax.dynamic_slice_in_dim(jnp.concatenate([mine, mine]), lax.axis_index("y"), NY)
    mine = mine.reshape(-1, copies.shape[2])
    up, down = [mine], [mine]
    for k in range(4):
        up.append(along_z(up[-1], 1))
        if k < 3:
            down.append(along_z(down[-1], -1))
    return up + down[1:]


def swap_cores(array):
    return lax.ppermute(array, "core", [(0, 1), (1, 0)])


def gather_rows(copies):
    own = lax.all_to_all(copies, "x", split_axis=0, concat_axis=0, tiled=True)
    own = own.reshape(-1, copies.shape[2])
    return own, swap_cores(own)


def return_rows(own, other):
    swapped = swap_cores(other)
    both = low(own + swapped.astype(jnp.float32))
    blocks = both.reshape(NX, -1, both.shape[1])
    return lax.all_to_all(blocks, "x", split_axis=0, concat_axis=0, tiled=True)


def stacked(arrays, first, last):
    return jnp.concatenate([a[..., first:last].reshape(-1, last - first) for a in arrays], axis=0)


def ffn_kernel(spans, place, small, *rest):
    row_refs, arrays, (own_ref, other_ref) = rest[:spans], rest[spans:-2], rest[-2:]
    units = arrays[0].shape[-1] // 3
    core = place[2]
    if spans == 1:
        every = row_refs[0]
        sides = [core, 1 - core]
        rows = jnp.concatenate([every[2 * k + s] for s in sides for k in range(NX)], axis=0)
    else:
        rows = jnp.concatenate([r[...] for r in row_refs], axis=0)
    gate = dot(rows, stacked(arrays, 0, units)) * small[0:1, :]
    up = dot(rows, stacked(arrays, units, 2 * units)) * small[1:2, :]
    hidden = low(gate / (1.0 + jnp.exp(-gate)) * up)
    part = dot_t(hidden, stacked(arrays, 2 * units, 3 * units))
    half = own_ref.shape[0]
    own_ref[...] = part[:half]
    other_ref[...] = low(part[half:])


def feed_forward(place, small, row_arrays, arrays):
    wide = row_arrays[0].shape[-1]
    rows = NX * ROWS
    own_part, other_part = pl.pallas_call(
        lambda *refs: ffn_kernel(len(row_arrays), *refs),
        out_shape=(
            jax.ShapeDtypeStruct((rows, wide), jnp.float32),
            jax.ShapeDtypeStruct((rows, wide), jnp.bfloat16),
        ),
        in_specs=[SMEM, VMEM] + [VMEM] * len(row_arrays) + [VMEM] * len(arrays),
        out_specs=(VMEM, VMEM),
        compiler_params=pltpu.CompilerParams(vmem_limit_bytes=24 * 1024 * 1024),
        name="ffn",
    )(place, small, *row_arrays, *arrays)
    return return_rows(own_part, other_part)


def mix_kernel(place, rate, small, own_rows, other_rows, *rest):
    arrays, (own_ref, other_ref) = rest[:-2], rest[-2:]
    core = place[2]
    rows = jnp.concatenate([own_rows[...], other_rows[...]], axis=0)
    query = low(dot(rows, stacked(arrays, 0, DK)) * small[2:3, :DK])
    key_rows = low(dot(rows, stacked(arrays, DK, 2 * DK)) * small[3:4, :DK] / math.sqrt(DK))
    value = low(dot(rows, stacked(arrays, 2 * DK, 3 * DK)) * small[4:5, :DK])

    total = rows.shape[0]

    def position(axis):
        r = lax.broadcasted_iota(jnp.int32, (total, total), axis)
        half = r // (total // 2)
        side = jnp.where(half == 0, core, 1 - core)
        return (r % (total // 2)) // ROWS * (2 * ROWS) + side * ROWS + r % ROWS

    pi, pj = position(0), position(1)
    apart = jnp.abs(pi - pj).astype(jnp.float32)
    decay = jnp.where(pj // BLOCK <= pi // BLOCK, jnp.exp(-rate[0] * apart), 0.0)
    scores = low(dot_t(query, key_rows) * decay)
    retained = dot(scores, value)
    centred = retained - jnp.mean(retained, axis=-1, keepdims=True)
    scale = lax.rsqrt(jnp.mean(centred * centred, axis=-1, keepdims=True) + EPSILON)
    mixed = low(centred * scale * small[5:6, :DK])
    part = dot_t(mixed, stacked(arrays, 3 * DK, 4 * DK))
    half = own_ref.shape[0]
    own_ref[...] = part[:half]
    other_ref[...] = low(part[half:])


def mix(place, rate, small, own, other, arrays):
    rows, wide = own.shape
    own_part, other_part = pl.pallas_call(
        mix_kernel,
        out_shape=(
            jax.ShapeDtypeStruct((rows, wide), jnp.float32),
            jax.ShapeDtypeStruct((rows, wide), jnp.bfloat16),
        ),
        in_specs=[SMEM, SMEM] + [VMEM] * (3 + len(arrays)),
        out_specs=(VMEM, VMEM),
        compiler_params=pltpu.CompilerParams(vmem_limit_bytes=24 * 1024 * 1024),
        name="mix",
    )(place, rate, small, own, other, *arrays)
    return return_rows(own_part, other_part)


def on_device(
    tokens_in, norm_gains, gate_w, gate_scale, up_w, up_scale, down_w, down_scale,
    query_w, query_scale, key_w, key_scale, value_w, value_scale, out_w, out_scale,
    head_gain, decay_rate,
):
    def row(v):
        return v.reshape(1, -1)

    place = jnp.stack([lax.axis_index(a).astype(jnp.int32) for a in ("z", "y", "core")])
    ffn_mine, mix_mine, copies, small, stream, gains = pack(
        place, gate_w, up_w, down_w.T, row(down_scale), query_w, key_w, value_w, out_w.T,
        row(out_scale), tokens_in, norm_gains,
        [row(v) for v in (gate_scale, up_scale, query_scale, key_scale, value_scale, head_gain)],
    )
    ffn_arrays = gather_ffn(ffn_mine)
    every = lax.all_to_all(copies, ("x", "core"), split_axis=0, concat_axis=0, tiled=True)
    mix_arrays = gather_mix(mix_mine)

    arrived = feed_forward(place, small, [every], ffn_arrays)
    stream, copies = join(place, 0.5, 1, arrived, stream, gains, rows_as=FFN_TO_MIX)
    own, other = gather_rows(copies)
    arrived = mix(place, decay_rate, small, own, other, mix_arrays)
    stream, copies = join(place, 1.0, 2, arrived, stream, gains, arrived_as=MIX_TO_FFN)
    rows = gather_rows(copies)
    arrived = feed_forward(place, small, rows, ffn_arrays)
    return join(place, 0.5, None, arrived, stream, gains)[0]


def solution(mesh):
    devices = mesh.devices
    fine = Mesh(devices.reshape(2, NZ, NY, NX, 2), ("rep", "z", "y", "x", "core"))
    F, T = ("z", "y"), ("x", "core")
    rows = P(("rep", "z", "y", "x", "core"), None)
    wide, tall, cols, depth = P(F, T), P(T, F), P(T), P(F)
    placed = (
        rows, P(), wide, cols, wide, cols, tall, depth,
        wide, cols, wide, cols, wide, cols, tall, depth,
        P(), cols,
    )
    return jax.shard_map(on_device, mesh=fine, in_specs=placed, out_specs=rows, check_vma=False)
```

time: 228 us -> 225 us (0.987)
  waiting for transfers between devices: 30.9 us -> 47.1 us
  starting transfers between devices: 119 us -> 106 us
  Pallas kernels: 26.8 us -> 16.1 us
  local copies, waits for them, and re-layouts: 11.9 us -> 15.7 us
    ppermute x8 -> x6, waiting for transfers between devices: 3.85 us -> 18.9 us  [along_y(): return lax.ppermute(array, 'y', [(g, (g + step) % NY) for g in range(NY)])]
    pallas_call x3 -> x6, Pallas kernels: 24.5 us -> 14.4 us  [the longest x2 7.2 us: feed_forward(): pl.pallas_call(lambda *refs: ffn_kernel(len(row_arrays), *refs), out_shap...]
    all_to_all x1 -> x2, starting transfers between devices: 4.13 us -> 12.4 us  [the longest x1 8.36 us: on_device(): lax.all_to_all(copies, ('x', 'core'), split_axis=0, concat_axis=0, tiled=...]
    unnamed x28 -> x48, local copies, waits for them, and re-layouts: 6.53 us -> 14.3 us
    ppermute x6 -> x5, starting transfers between devices: 25.9 us -> 19.4 us  [swap_cores(): return lax.ppermute(array, 'core', [(0, 1), (1, 0)])]
    ppermute x8 -> x6, starting transfers between devices: 23.6 us -> 18.5 us  [along_y(): return lax.ppermute(array, 'y', [(g, (g + step) % NY) for g in range(NY)])]
    ppermute x14, starting transfers between devices: 52.5 us -> 47.5 us  [along_z(): lax.ppermute(array, ('rep', 'z'), [(g, (g + step) % (2 * NZ)) for g in ra...]
    slice x5 -> x0, local copies, waits for them, and re-layouts: 4.43 us -> none  [the longest x1 1.49 us: on_device(): own, other = gather_rows(norm_copies(stream, norm_gains[2]))]
  transfers between devices with their start and end apart: 32 -> 29, of which waited for: 12 -> 13; matrix products, arithmetic and copies ran while one was open for 3% -> 2% of each run, Pallas kernels for 4% -> 2%
where the time goes in v3:
time: 225 us; the launch traced here: 223 us
  starting transfers between devices  106 us (47%)
  waiting for transfers between devices  47.1 us (21%)
  blocking collectives  34.3 us (15%)
  Pallas kernels  16.1 us (7%)
  local copies, waits for them, and re-layouts  15.7 us (7%)
  other arithmetic  2.52 us (1%)
    ppermute x14, starting transfers between devices, along_z(): lax.ppermute(array, ('rep', 'z'), [(g, (g + step) % (2 * NZ)) for g in ra...  47.5 us
    all_to_all x2, blocking collectives, return_rows(): return lax.all_to_all(blocks, 'x', split_axis=0, concat_axis=0, tiled=True)  24.2 us
    ppermute x14, waiting for transfers between devices, along_z(): lax.ppermute(array, ('rep', 'z'), [(g, (g + step) % (2 * NZ)) for g in ra...  23.6 us
    ppermute x5, starting transfers between devices, swap_cores(): return lax.ppermute(array, 'core', [(0, 1), (1, 0)])  19.4 us
    ppermute x6, waiting for transfers between devices, along_y(): return lax.ppermute(array, 'y', [(g, (g + step) % NY) for g in range(NY)])  18.9 us
    ppermute x6, starting transfers between devices, along_y(): return lax.ppermute(array, 'y', [(g, (g + step) % NY) for g in range(NY)])  18.5 us
    unnamed x48, local copies, waits for them, and re-layouts  14.3 us
    all_to_all x1, blocking collectives, gather_rows(): own = lax.all_to_all(copies, 'x', split_axis=0, concat_axis=0, tiled=True)  10.2 us
  transfers between devices with their start and end apart: 29, of which 13 were waited for; matrix products, arithmetic and copies ran while one was open for 2% of the time, Pallas kernels for 2%

profile of v3, /device:TPU:1, one launch (start us, length us, event | category | flops | bytes accessed | tf_op | source)
XLA Modules:
  0.0 222.9 jit_solution(10477367965116366063)
XLA Ops:
  9.1 1.7 pack.1
  11.5 11.9 %collective-permute-start.1 = (bf16[64,1152]{1,0:T(8,128)(2,1)S(1)}, bf16[64,1152]{1,0:T(8,128)(2,1)}, u32[]{:S(2)}, u32[]{:S(2)}) collective-permute-start(bf16[64,1152]{1,0:T(8,128)(2,1)S(1)} %get-tuple-element.23), channel_id=1, source_target_pairs={{0,480},{32,0},{64,32},{96,64},{128,96},{160,128},{192,160},{224,1... | collective-permute-start | bytes 442376 | tf_op jit(solution)/shard_map/ppermute | solution.py:178
  23.5 1.9 collective-permute-start
  25.4 4.2 %all-to-all-start.3 = ((bf16[4,64,1024]{2,1,0:T(8,128)(2,1)}), bf16[4,64,1024]{2,1,0:T(8,128)(2,1)S(1)}, u32[]{:S(2)}, u32[]{:S(2)}) async-start(bf16[4,64,1024]{2,1,0:T(8,128)(2,1)} %get-tuple-element.29), calls=%async_computation.3 | async-start | bytes 1048576 | tf_op jit(solution)/shard_map/all_to_all | solution.py:205
  29.6 4.6 %collective-permute-start.3 = (bf16[64,1152]{1,0:T(8,128)(2,1)}, bf16[64,1152]{1,0:T(8,128)(2,1)S(1)}, u32[]{:S(2)}, u32[]{:S(2)}) collective-permute-start(bf16[64,1152]{1,0:T(8,128)(2,1)} %collective-permute-done.1), channel_id=1, source_target_pairs={{0,480},{32,0},{64,32},{96,64},{128,96},{160,128},{192,160},{224,1... | collective-permute-start | bytes 442376 | tf_op jit(solution)/shard_map/ppermute | solution.py:178
  34.2 1.9 collective-permute-start.2
  38.0 3.6 %collective-permute-done.2 = bf16[64,1152]{1,0:T(8,128)(2,1)} collective-permute-done((bf16[64,1152]{1,0:T(8,128)(2,1)}, bf16[64,1152]{1,0:T(8,128)(2,1)}, u32[]{:S(2)}, u32[]{:S(2)}) %collective-permute-start.2) | collective-permute-done | bytes 147488 | tf_op jit(solution)/shard_map/ppermute | solution.py:178
  42.6 3.4 %collective-permute-start.4 = (bf16[5,64,1152]{2,1,0:T(8,128)(2,1)S(1)}, bf16[5,64,1152]{2,1,0:T(8,128)(2,1)S(1)}, u32[]{:S(2)}, u32[]{:S(2)}) collective-permute-start(bf16[5,64,1152]{2,1,0:T(8,128)(2,1)S(1)} %bitcast_dynamic-update-slice_fusion.refs_3_.refs_4_), channel_id=1, source_target_pairs={{0,8},{8,16},{16,24},{24,0},{1,9},{9,17},{17,25},{25,1},{2,10},{10... | collective-permute-start | bytes 2211848 | tf_op jit(solution)/shard_map/ppermute | solution.py:182
  46.0 1.9 collective-permute-start.8
  47.9 4.3 %collective-permute-start.7 = (bf16[64,1152]{1,0:T(8,128)(2,1)}, bf16[64,1152]{1,0:T(8,128)(2,1)S(1)}, u32[]{:S(2)}, u32[]{:S(2)}) collective-permute-start(bf16[64,1152]{1,0:T(8,128)(2,1)} %collective-permute-done), channel_id=1, source_target_pairs={{0,64},{32,96},{64,128},{96,160},{128,192},{160,224},{192,256},{22... | collective-permute-start | bytes 442376 | tf_op jit(solution)/shard_map/ppermute | solution.py:178
  52.2 1.9 collective-permute-start.9
  54.9 8.4 %all-to-all-start = ((bf16[8,32,2048]{2,1,0:T(8,128)(2,1)}), bf16[8,32,2048]{2,1,0:T(8,128)(2,1)S(1)}, u32[]{:S(2)}, u32[]{:S(2)}) async-start(bf16[8,32,2048]{2,1,0:T(8,128)(2,1)} %copy-done), calls=%async_computation | async-start | bytes 2097152 | tf_op jit(solution)/shard_map/all_to_all | solution.py:334
  63.3 3.7 %collective-permute-done.9 = bf16[64,1152]{1,0:T(8,128)(2,1)S(1)} collective-permute-done((bf16[64,1152]{1,0:T(8,128)(2,1)}, bf16[64,1152]{1,0:T(8,128)(2,1)S(1)}, u32[]{:S(2)}, u32[]{:S(2)}) %collective-permute-start.9) | collective-permute-done | bytes 147488 | tf_op jit(solution)/shard_map/ppermute | solution.py:178
  67.0 3.1 %collective-permute-start.11 = (bf16[3,64,1152]{2,1,0:T(8,128)(2,1)S(1)}, bf16[3,64,1152]{2,1,0:T(8,128)(2,1)}, u32[]{:S(2)}, u32[]{:S(2)}) collective-permute-start(bf16[3,64,1152]{2,1,0:T(8,128)(2,1)S(1)} %pad_maximum_fusion.refs_7_.refs_8_), channel_id=1, source_target_pairs={{0,24},{8,0},{16,8},{24,16},{1,25},{9,1},{17,9},{25,17},{2,26},{10... | collective-permute-start | bytes 1327112 | tf_op jit(solution)/shard_map/ppermute | solution.py:182
  70.1 3.4 %collective-permute-start.5 = (bf16[5,64,1152]{2,1,0:T(8,128)(2,1)S(1)}, bf16[5,64,1152]{2,1,0:T(8,128)(2,1)}, u32[]{:S(2)}, u32[]{:S(2)}) collective-permute-start(bf16[5,64,1152]{2,1,0:T(8,128)(2,1)S(1)} %bitcast_dynamic-update-slice_fusion.refs_3_.refs_4_), channel_id=1, source_target_pairs={{0,24},{8,0},{16,8},{24,16},{1,25},{9,1},{17,9},{25,17},{2,26},{10... | collective-permute-start | bytes 2211848 | tf_op jit(solution)/shard_map/ppermute | solution.py:182
  73.5 1.9 collective-permute-start.6
  75.5 2.2 collective-permute-start.10
  79.0 4.6 %collective-permute-start.12 = (bf16[3,64,1152]{2,1,0:T(8,128)(2,1)}, bf16[3,64,1152]{2,1,0:T(8,128)(2,1)}, u32[]{:S(2)}, u32[]{:S(2)}) collective-permute-start(bf16[3,64,1152]{2,1,0:T(8,128)(2,1)} %collective-permute-done.11.refs_9_.refs_10_), channel_id=1, source_target_pairs={{0,24},{8,0},{16,8},{24,16},{1,25},{9,1},{17,9},{25,17},{2,26},{10... | collective-permute-start | bytes 1327112 | tf_op jit(solution)/shard_map/ppermute | solution.py:182
  84.9 1.9 collective-permute-start.15
  86.8 15.2 %collective-permute-done.10.refs_8_.refs_9_ = bf16[3,64,1152]{2,1,0:T(8,128)(2,1)} collective-permute-done((bf16[3,64,1152]{2,1,0:T(8,128)(2,1)S(1)}, bf16[3,64,1152]{2,1,0:T(8,128)(2,1)}, u32[]{:S(2)}, u32[]{:S(2)}) %collective-permute-start.10) | collective-permute-done | bytes 442400 | tf_op jit(solution)/shard_map/ppermute | solution.py:182
  102.0 2.3 %collective-permute-done.12.refs_10_.refs_11_ = bf16[3,64,1152]{2,1,0:T(8,128)(2,1)} collective-permute-done((bf16[3,64,1152]{2,1,0:T(8,128)(2,1)}, bf16[3,64,1152]{2,1,0:T(8,128)(2,1)}, u32[]{:S(2)}, u32[]{:S(2)}) %collective-permute-start.12) | collective-permute-done | bytes 442400 | tf_op jit(solution)/shard_map/ppermute | solution.py:182
  104.3 3.6 %ffn.2 = (f32[128,2048]{1,0:T(8,128)S(1)}, bf16[128,2048]{1,0:T(8,128)(2,1)S(1)}) custom-call(s32[3]{0:T(128)S(1)} %pad_add_fusion.place.refs_0_, f32[8,384]{1,0:T(8,128)S(1)} %get-tuple-element.21.refs_1_.small, bf16[8,32,2048]{2,1,0:T(8,128)(2,1)S(1)} %all-to-all-done.refs_2_, bf16[5,64,1152]{2,1,0:T(8,128)(2,1)S(1)} %bitcast_dynamic-update-slice_fusion.refs_3_.refs_4_, ...), custom_call_target="tpu_custom_call" | custom-call | tf_op jit(solution)/shard_map/ffn/pallas_call | solution.py:259
  107.9 4.5 %collective-permute-start.13 = (bf16[128,2048]{1,0:T(8,128)(2,1)S(1)}, bf16[128,2048]{1,0:T(8,128)(2,1)S(1)}, u32[]{:S(2)}, u32[]{:S(2)}) collective-permute-start(bf16[128,2048]{1,0:T(8,128)(2,1)S(1)} %get-tuple-element.25), channel_id=1, source_target_pairs={{0,1},{1,0},{2,3},{3,2},{4,5},{5,4},{6,7},{7,6},{8,9},{9,8},{10,11... | collective-permute-start | bytes 1572872 | tf_op jit(solution)/shard_map/ppermute | solution.py:217
  112.4 1.9 collective-permute-start.19
  114.3 3.4 %collective-permute-start.16 = (bf16[256,1024]{1,0:T(8,128)(2,1)}, bf16[256,1024]{1,0:T(8,128)(2,1)}, u32[]{:S(2)}, u32[]{:S(2)}) collective-permute-start(bf16[256,1024]{1,0:T(8,128)(2,1)} %collective-permute-done.15.rest_1_), channel_id=1, source_target_pairs={{0,32},{32,64},{64,96},{96,128},{128,160},{160,192},{192,224},{224... | collective-permute-start | bytes 1572872 | tf_op jit(solution)/shard_map/ppermute | solution.py:178
  118.6 4.0 %all-to-all-start.1 = ((bf16[4,32,2048]{2,1,0:T(8,128)(2,1)}), bf16[4,32,2048]{2,1,0:T(8,128)(2,1)S(1)}, u32[]{:S(2)}, u32[]{:S(2)}) async-start(bf16[4,32,2048]{2,1,0:T(8,128)(2,1)} %bitcast.45), calls=%async_computation.1 | async-start | bytes 1048576 | tf_op jit(solution)/shard_map/all_to_all | solution.py:230
  122.7 5.2 %collective-permute-done.19.rest_5_ = bf16[256,1024]{1,0:T(8,128)(2,1)S(1)} collective-permute-done((bf16[256,1024]{1,0:T(8,128)(2,1)S(1)}, bf16[256,1024]{1,0:T(8,128)(2,1)S(1)}, u32[]{:S(2)}, u32[]{:S(2)}) %collective-permute-start.19) | collective-permute-done | bytes 524320 | tf_op jit(solution)/shard_map/ppermute | solution.py:178
  127.9 3.3 %collective-permute-start.20 = (bf16[256,1024]{1,0:T(8,128)(2,1)S(1)}, bf16[256,1024]{1,0:T(8,128)(2,1)}, u32[]{:S(2)}, u32[]{:S(2)}) collective-permute-start(bf16[256,1024]{1,0:T(8,128)(2,1)S(1)} %collective-permute-done.19.rest_5_), channel_id=1, source_target_pairs={{0,480},{32,0},{64,32},{96,64},{128,96},{160,128},{192,160},{224,1... | collective-permute-start | bytes 1572872 | tf_op jit(solution)/shard_map/ppermute | solution.py:178
  131.2 1.9 collective-permute-start.17
  136.4 4.0 %all-to-all-start.2 = ((bf16[4,32,2048]{2,1,0:T(8,128)(2,1)}), bf16[4,32,2048]{2,1,0:T(8,128)(2,1)S(1)}, u32[]{:S(2)}, u32[]{:S(2)}) async-start(bf16[4,32,2048]{2,1,0:T(8,128)(2,1)} %copy-done.1), calls=%async_computation.2 | async-start | bytes 1048576 | tf_op jit(solution)/shard_map/all_to_all | solution.py:221
  140.4 2.1 collective-permute-done.20.rest_6_
  142.6 4.7 %collective-permute-start.21 = (bf16[256,1024]{1,0:T(8,128)(2,1)}, bf16[256,1024]{1,0:T(8,128)(2,1)}, u32[]{:S(2)}, u32[]{:S(2)}) collective-permute-start(bf16[256,1024]{1,0:T(8,128)(2,1)} %collective-permute-done.20.rest_6_), channel_id=1, source_target_pairs={{0,480},{32,0},{64,32},{96,64},{128,96},{160,128},{192,160},{224,1... | collective-permute-start | bytes 1572872 | tf_op jit(solution)/shard_map/ppermute | solution.py:178
  147.3 1.9 collective-permute-start.18
  149.2 3.6 %collective-permute-start.14 = (bf16[128,2048]{1,0:T(8,128)(2,1)S(1)}, bf16[128,2048]{1,0:T(8,128)(2,1)S(1)}, u32[]{:S(2)}, u32[]{:S(2)}) collective-permute-start(bf16[128,2048]{1,0:T(8,128)(2,1)S(1)} %bitcast.30), channel_id=1, source_target_pairs={{0,1},{1,0},{2,3},{3,2},{4,5},{5,4},{6,7},{7,6},{8,9},{9,8},{10,11... | collective-permute-start | bytes 1572872 | tf_op jit(solution)/shard_map/ppermute | solution.py:217
  153.5 3.9 %collective-permute-done.21.rest_7_ = bf16[256,1024]{1,0:T(8,128)(2,1)} collective-permute-done((bf16[256,1024]{1,0:T(8,128)(2,1)}, bf16[256,1024]{1,0:T(8,128)(2,1)}, u32[]{:S(2)}, u32[]{:S(2)}) %collective-permute-start.21) | collective-permute-done | bytes 524320 | tf_op jit(solution)/shard_map/ppermute | solution.py:178
  157.4 5.1 %collective-permute-done.18.rest_4_ = bf16[256,1024]{1,0:T(8,128)(2,1)} collective-permute-done((bf16[256,1024]{1,0:T(8,128)(2,1)}, bf16[256,1024]{1,0:T(8,128)(2,1)}, u32[]{:S(2)}, u32[]{:S(2)}) %collective-permute-start.18) | collective-permute-done | bytes 524320 | tf_op jit(solution)/shard_map/ppermute | solution.py:178
  162.5 4.1 %mix.1 = (f32[128,2048]{1,0:T(8,128)S(1)}, bf16[128,2048]{1,0:T(8,128)(2,1)S(1)}) custom-call(s32[3]{0:T(128)S(1)} %pad_add_fusion.place.refs_0_, f32[1]{0:T(128)S(6)} %copy.23.rate, f32[8,384]{1,0:T(8,128)S(1)} %get-tuple-element.21.refs_1_.small, bf16[128,2048]{1,0:T(8,128)(2,1)S(1)} %bitcast.31, bf16[128,2048]{1,0:T(8,128)(2,1)S(1)} %collective-permute-done.14.other_rows, ...), custom_call_target="tpu_custom_call" | custom-call | tf_op jit(solution)/shard_map/mix/pallas_call | solution.py:305
  166.5 4.5 %collective-permute-start.22 = (bf16[128,2048]{1,0:T(8,128)(2,1)S(1)}, bf16[128,2048]{1,0:T(8,128)(2,1)S(1)}, u32[]{:S(2)}, u32[]{:S(2)}) collective-permute-start(bf16[128,2048]{1,0:T(8,128)(2,1)S(1)} %get-tuple-element.31), channel_id=1, source_target_pairs={{0,1},{1,0},{2,3},{3,2},{4,5},{5,4},{6,7},{7,6},{8,9},{9,8},{10,11... | collective-permute-start | bytes 1572872 | tf_op jit(solution)/shard_map/ppermute | solution.py:217
  171.0 1.5 collective-permute-done.22
  172.7 12.6 %all_to_all.35.refs_1_ = bf16[4,32,2048]{2,1,0:T(8,128)(2,1)S(1)} all-to-all(bf16[4,32,2048]{2,1,0:T(8,128)(2,1)S(1)} %bitcast.46), channel_id=1, replica_groups=mesh['rep'=2,'z'=8,'y'=4,'x'=4,'core'=2] {'x'}, dimensions={0} | all-to-all | bytes 1048576 | tf_op jit(solution)/shard_map/all_to_all | solution.py:230
  186.0 10.2 %all_to_all.36 = bf16[4,32,2048]{2,1,0:T(8,128)(2,1)S(1)} all-to-all(bf16[4,32,2048]{2,1,0:T(8,128)(2,1)S(1)} %get-tuple-element.33), channel_id=1, replica_groups=mesh['rep'=2,'z'=8,'y'=4,'x'=4,'core'=2] {'x'}, dimensions={0} | all-to-all | bytes 1048576 | tf_op jit(solution)/shard_map/all_to_all | solution.py:221
  196.2 4.6 %collective-permute-start.23 = (bf16[128,2048]{1,0:T(8,128)(2,1)S(1)}, bf16[128,2048]{1,0:T(8,128)(2,1)S(1)}, u32[]{:S(2)}, u32[]{:S(2)}) collective-permute-start(bf16[128,2048]{1,0:T(8,128)(2,1)S(1)} %bitcast.35), channel_id=1, source_target_pairs={{0,1},{1,0},{2,3},{3,2},{4,5},{5,4},{6,7},{7,6},{8,9},{9,8},{10,11... | collective-permute-start | bytes 1572872 | tf_op jit(solution)/shard_map/ppermute | solution.py:217
  200.8 1.5 collective-permute-done.23.refs_3_
  202.3 3.6 %ffn.3 = (f32[128,2048]{1,0:T(8,128)S(1)}, bf16[128,2048]{1,0:T(8,128)(2,1)S(1)}) custom-call(s32[3]{0:T(128)S(1)} %pad_add_fusion.place.refs_0_, f32[8,384]{1,0:T(8,128)S(1)} %get-tuple-element.21.refs_1_.small, bf16[128,2048]{1,0:T(8,128)(2,1)S(1)} %bitcast.36, bf16[128,2048]{1,0:T(8,128)(2,1)S(1)} %collective-permute-done.23.refs_3_, ...), custom_call_target="tpu_custom_call" | custom-call | tf_op jit(solution)/shard_map/ffn/pallas_call | solution.py:259
  205.9 2.3 %collective-permute-start.24 = (bf16[128,2048]{1,0:T(8,128)(2,1)S(1)}, bf16[128,2048]{1,0:T(8,128)(2,1)S(1)}, u32[]{:S(2)}, u32[]{:S(2)}) collective-permute-start(bf16[128,2048]{1,0:T(8,128)(2,1)S(1)} %get-tuple-element.35), channel_id=1, source_target_pairs={{0,1},{1,0},{2,3},{3,2},{4,5},{5,4},{6,7},{7,6},{8,9},{9,8},{10,11... | collective-permute-start | bytes 1572872 | tf_op jit(solution)/shard_map/ppermute | solution.py:217
  208.2 1.5 collective-permute-done.24
  209.8 11.6 %all_to_all.37.refs_1_ = bf16[4,32,2048]{2,1,0:T(8,128)(2,1)S(1)} all-to-all(bf16[4,32,2048]{2,1,0:T(8,128)(2,1)S(1)} %bitcast.47), channel_id=1, replica_groups=mesh['rep'=2,'z'=8,'y'=4,'x'=4,'core'=2] {'x'}, dimensions={0} | all-to-all | bytes 1048576 | tf_op jit(solution)/shard_map/all_to_all | solution.py:230
  221.4 1.5 join.5
  (77 shorter events, 21.4 us)
Async XLA Ops:
  0.0 1.5 copy-start.14
  1.5 0.7 copy-start.16
  1.5 0.7 copy-start.17
  1.5 0.7 copy-start.15
  1.5 0.7 copy-start.19
  2.2 0.9 copy-start.4
  3.1 0.9 copy-start.7
  4.0 0.9 copy-start.8
  4.9 0.9 copy-start.9
  5.8 0.8 copy-start.10
  6.6 0.8 copy-start.11
  7.5 0.8 copy-start.12
  8.3 0.8 copy-start.13
  11.5 13.9 %copy-start = (bf16[8,32,2048]{2,1,0:T(8,128)(2,1)}, bf16[8,32,2048]{2,1,0:T(8,128)(2,1)S(1)}, u32[]{:S(2)}) copy-start(bf16[8,32,2048]{2,1,0:T(8,128)(2,1)S(1)} %get-tuple-element.22) | copy-start | bytes 3145732
  11.5 18.1 %collective-permute-start.1 = (bf16[64,1152]{1,0:T(8,128)(2,1)S(1)}, bf16[64,1152]{1,0:T(8,128)(2,1)}, u32[]{:S(2)}, u32[]{:S(2)}) collective-permute-start(bf16[64,1152]{1,0:T(8,128)(2,1)S(1)} %get-tuple-element.23), channel_id=1, source_target_pairs={{0,480},{32,0},{64,32},{96,64},{128,96},{160,128},{192,160},{224,1... | collective-permute-start | bytes 442376 | tf_op jit(solution)/shard_map/ppermute | solution.py:178
  23.5 10.7 %collective-permute-start = (bf16[64,1152]{1,0:T(8,128)(2,1)S(1)}, bf16[64,1152]{1,0:T(8,128)(2,1)}, u32[]{:S(2)}, u32[]{:S(2)}) collective-permute-start(bf16[64,1152]{1,0:T(8,128)(2,1)S(1)} %get-tuple-element.23), channel_id=1, source_target_pairs={{0,32},{32,64},{64,96},{96,128},{128,160},{160,192},{192,224},{224... | collective-permute-start | bytes 442376 | tf_op jit(solution)/shard_map/ppermute | solution.py:178
  25.4 28.7 %all-to-all-start.3 = ((bf16[4,64,1024]{2,1,0:T(8,128)(2,1)}), bf16[4,64,1024]{2,1,0:T(8,128)(2,1)S(1)}, u32[]{:S(2)}, u32[]{:S(2)}) async-start(bf16[4,64,1024]{2,1,0:T(8,128)(2,1)} %get-tuple-element.29), calls=%async_computation.3 | async-start | bytes 1048576 | tf_op jit(solution)/shard_map/all_to_all | solution.py:205
  29.6 12.9 %collective-permute-start.3 = (bf16[64,1152]{1,0:T(8,128)(2,1)}, bf16[64,1152]{1,0:T(8,128)(2,1)S(1)}, u32[]{:S(2)}, u32[]{:S(2)}) collective-permute-start(bf16[64,1152]{1,0:T(8,128)(2,1)} %collective-permute-done.1), channel_id=1, source_target_pairs={{0,480},{32,0},{64,32},{96,64},{128,96},{160,128},{192,160},{224,1... | collective-permute-start | bytes 442376 | tf_op jit(solution)/shard_map/ppermute | solution.py:178
  34.2 7.4 %collective-permute-start.2 = (bf16[64,1152]{1,0:T(8,128)(2,1)}, bf16[64,1152]{1,0:T(8,128)(2,1)}, u32[]{:S(2)}, u32[]{:S(2)}) collective-permute-start(bf16[64,1152]{1,0:T(8,128)(2,1)} %collective-permute-done), channel_id=1, source_target_pairs={{0,32},{32,64},{64,96},{96,128},{128,160},{160,192},{192,224},{224... | collective-permute-start | bytes 442376 | tf_op jit(solution)/shard_map/ppermute | solution.py:178
  42.6 30.9 %collective-permute-start.4 = (bf16[5,64,1152]{2,1,0:T(8,128)(2,1)S(1)}, bf16[5,64,1152]{2,1,0:T(8,128)(2,1)S(1)}, u32[]{:S(2)}, u32[]{:S(2)}) collective-permute-start(bf16[5,64,1152]{2,1,0:T(8,128)(2,1)S(1)} %bitcast_dynamic-update-slice_fusion.refs_3_.refs_4_), channel_id=1, source_target_pairs={{0,8},{8,16},{16,24},{24,0},{1,9},{9,17},{17,25},{25,1},{2,10},{10... | collective-permute-start | bytes 2211848 | tf_op jit(solution)/shard_map/ppermute | solution.py:182
  46.0 17.3 %collective-permute-start.8 = (bf16[64,1152]{1,0:T(8,128)(2,1)}, bf16[64,1152]{1,0:T(8,128)(2,1)S(1)}, u32[]{:S(2)}, u32[]{:S(2)}) collective-permute-start(bf16[64,1152]{1,0:T(8,128)(2,1)} %collective-permute-done.1), channel_id=1, source_target_pairs={{0,448},{32,480},{64,0},{96,32},{128,64},{160,96},{192,128},{224,1... | collective-permute-start | bytes 442376 | tf_op jit(solution)/shard_map/ppermute | solution.py:178
  47.9 15.4 %collective-permute-start.7 = (bf16[64,1152]{1,0:T(8,128)(2,1)}, bf16[64,1152]{1,0:T(8,128)(2,1)S(1)}, u32[]{:S(2)}, u32[]{:S(2)}) collective-permute-start(bf16[64,1152]{1,0:T(8,128)(2,1)} %collective-permute-done), channel_id=1, source_target_pairs={{0,64},{32,96},{64,128},{96,160},{128,192},{160,224},{192,256},{22... | collective-permute-start | bytes 442376 | tf_op jit(solution)/shard_map/ppermute | solution.py:178
  52.2 14.8 %collective-permute-start.9 = (bf16[64,1152]{1,0:T(8,128)(2,1)}, bf16[64,1152]{1,0:T(8,128)(2,1)S(1)}, u32[]{:S(2)}, u32[]{:S(2)}) collective-permute-start(bf16[64,1152]{1,0:T(8,128)(2,1)} %collective-permute-done.2), channel_id=1, source_target_pairs={{0,64},{32,96},{64,128},{96,160},{128,192},{160,224},{192,256},{22... | collective-permute-start | bytes 442376 | tf_op jit(solution)/shard_map/ppermute | solution.py:178
  54.1 0.8 copy-start.21
  54.9 47.1 %all-to-all-start = ((bf16[8,32,2048]{2,1,0:T(8,128)(2,1)}), bf16[8,32,2048]{2,1,0:T(8,128)(2,1)S(1)}, u32[]{:S(2)}, u32[]{:S(2)}) async-start(bf16[8,32,2048]{2,1,0:T(8,128)(2,1)} %copy-done), calls=%async_computation | async-start | bytes 2097152 | tf_op jit(solution)/shard_map/all_to_all | solution.py:334
  67.0 12.0 %collective-permute-start.11 = (bf16[3,64,1152]{2,1,0:T(8,128)(2,1)S(1)}, bf16[3,64,1152]{2,1,0:T(8,128)(2,1)}, u32[]{:S(2)}, u32[]{:S(2)}) collective-permute-start(bf16[3,64,1152]{2,1,0:T(8,128)(2,1)S(1)} %pad_maximum_fusion.refs_7_.refs_8_), channel_id=1, source_target_pairs={{0,24},{8,0},{16,8},{24,16},{1,25},{9,1},{17,9},{25,17},{2,26},{10... | collective-permute-start | bytes 1327112 | tf_op jit(solution)/shard_map/ppermute | solution.py:182
  70.1 31.9 %collective-permute-start.5 = (bf16[5,64,1152]{2,1,0:T(8,128)(2,1)S(1)}, bf16[5,64,1152]{2,1,0:T(8,128)(2,1)}, u32[]{:S(2)}, u32[]{:S(2)}) collective-permute-start(bf16[5,64,1152]{2,1,0:T(8,128)(2,1)S(1)} %bitcast_dynamic-update-slice_fusion.refs_3_.refs_4_), channel_id=1, source_target_pairs={{0,24},{8,0},{16,8},{24,16},{1,25},{9,1},{17,9},{25,17},{2,26},{10... | collective-permute-start | bytes 2211848 | tf_op jit(solution)/shard_map/ppermute | solution.py:182
  73.5 30.8 %collective-permute-start.6 = (bf16[5,64,1152]{2,1,0:T(8,128)(2,1)S(1)}, bf16[5,64,1152]{2,1,0:T(8,128)(2,1)}, u32[]{:S(2)}, u32[]{:S(2)}) collective-permute-start(bf16[5,64,1152]{2,1,0:T(8,128)(2,1)S(1)} %collective-permute-done.4.refs_4_.refs_5_), channel_id=1, source_target_pairs={{0,8},{8,16},{16,24},{24,0},{1,9},{9,17},{17,25},{25,1},{2,10},{10... | collective-permute-start | bytes 2211848 | tf_op jit(solution)/shard_map/ppermute | solution.py:182
  75.5 26.5 %collective-permute-start.10 = (bf16[3,64,1152]{2,1,0:T(8,128)(2,1)S(1)}, bf16[3,64,1152]{2,1,0:T(8,128)(2,1)}, u32[]{:S(2)}, u32[]{:S(2)}) collective-permute-start(bf16[3,64,1152]{2,1,0:T(8,128)(2,1)S(1)} %pad_maximum_fusion.refs_7_.refs_8_), channel_id=1, source_target_pairs={{0,8},{8,16},{16,24},{24,0},{1,9},{9,17},{17,25},{25,1},{2,10},{10... | collective-permute-start | bytes 1327112 | tf_op jit(solution)/shard_map/ppermute | solution.py:182
  79.0 25.3 %collective-permute-start.12 = (bf16[3,64,1152]{2,1,0:T(8,128)(2,1)}, bf16[3,64,1152]{2,1,0:T(8,128)(2,1)}, u32[]{:S(2)}, u32[]{:S(2)}) collective-permute-start(bf16[3,64,1152]{2,1,0:T(8,128)(2,1)} %collective-permute-done.11.refs_9_.refs_10_), channel_id=1, source_target_pairs={{0,24},{8,0},{16,8},{24,16},{1,25},{9,1},{17,9},{25,17},{2,26},{10... | collective-permute-start | bytes 1327112 | tf_op jit(solution)/shard_map/ppermute | solution.py:182
  84.9 29.5 %collective-permute-start.15 = (bf16[256,1024]{1,0:T(8,128)(2,1)S(1)}, bf16[256,1024]{1,0:T(8,128)(2,1)}, u32[]{:S(2)}, u32[]{:S(2)}) collective-permute-start(bf16[256,1024]{1,0:T(8,128)(2,1)S(1)} %bitcast.32), channel_id=1, source_target_pairs={{0,32},{32,64},{64,96},{96,128},{128,160},{160,192},{192,224},{224... | collective-permute-start | bytes 1572872 | tf_op jit(solution)/shard_map/ppermute | solution.py:178
  107.9 9.8 %collective-permute-start.13 = (bf16[128,2048]{1,0:T(8,128)(2,1)S(1)}, bf16[128,2048]{1,0:T(8,128)(2,1)S(1)}, u32[]{:S(2)}, u32[]{:S(2)}) collective-permute-start(bf16[128,2048]{1,0:T(8,128)(2,1)S(1)} %get-tuple-element.25), channel_id=1, source_target_pairs={{0,1},{1,0},{2,3},{3,2},{4,5},{5,4},{6,7},{7,6},{8,9},{9,8},{10,11... | collective-permute-start | bytes 1572872 | tf_op jit(solution)/shard_map/ppermute | solution.py:217
  112.4 15.5 %collective-permute-start.19 = (bf16[256,1024]{1,0:T(8,128)(2,1)S(1)}, bf16[256,1024]{1,0:T(8,128)(2,1)S(1)}, u32[]{:S(2)}, u32[]{:S(2)}) collective-permute-start(bf16[256,1024]{1,0:T(8,128)(2,1)S(1)} %bitcast.33), channel_id=1, source_target_pairs={{0,480},{32,0},{64,32},{96,64},{128,96},{160,128},{192,160},{224,1... | collective-permute-start | bytes 1572872 | tf_op jit(solution)/shard_map/ppermute | solution.py:178
  114.3 16.9 %collective-permute-start.16 = (bf16[256,1024]{1,0:T(8,128)(2,1)}, bf16[256,1024]{1,0:T(8,128)(2,1)}, u32[]{:S(2)}, u32[]{:S(2)}) collective-permute-start(bf16[256,1024]{1,0:T(8,128)(2,1)} %collective-permute-done.15.rest_1_), channel_id=1, source_target_pairs={{0,32},{32,64},{64,96},{96,128},{128,160},{160,192},{192,224},{224... | collective-permute-start | bytes 1572872 | tf_op jit(solution)/shard_map/ppermute | solution.py:178
  118.6 14.5 %all-to-all-start.1 = ((bf16[4,32,2048]{2,1,0:T(8,128)(2,1)}), bf16[4,32,2048]{2,1,0:T(8,128)(2,1)S(1)}, u32[]{:S(2)}, u32[]{:S(2)}) async-start(bf16[4,32,2048]{2,1,0:T(8,128)(2,1)} %bitcast.45), calls=%async_computation.1 | async-start | bytes 1048576 | tf_op jit(solution)/shard_map/all_to_all | solution.py:230
  127.9 14.7 %collective-permute-start.20 = (bf16[256,1024]{1,0:T(8,128)(2,1)S(1)}, bf16[256,1024]{1,0:T(8,128)(2,1)}, u32[]{:S(2)}, u32[]{:S(2)}) collective-permute-start(bf16[256,1024]{1,0:T(8,128)(2,1)S(1)} %collective-permute-done.19.rest_5_), channel_id=1, source_target_pairs={{0,480},{32,0},{64,32},{96,64},{128,96},{160,128},{192,160},{224,1... | collective-permute-start | bytes 1572872 | tf_op jit(solution)/shard_map/ppermute | solution.py:178
  131.2 16.0 %collective-permute-start.17 = (bf16[256,1024]{1,0:T(8,128)(2,1)}, bf16[256,1024]{1,0:T(8,128)(2,1)}, u32[]{:S(2)}, u32[]{:S(2)}) collective-permute-start(bf16[256,1024]{1,0:T(8,128)(2,1)} %collective-permute-done.16.rest_2_), channel_id=1, source_target_pairs={{0,32},{32,64},{64,96},{96,128},{128,160},{160,192},{192,224},{224... | collective-permute-start | bytes 1572872 | tf_op jit(solution)/shard_map/ppermute | solution.py:178
  133.2 0.9 copy-start.6
  134.9 0.8 copy-start.1
  135.7 0.7 copy-start.2
  136.4 12.8 %all-to-all-start.2 = ((bf16[4,32,2048]{2,1,0:T(8,128)(2,1)}), bf16[4,32,2048]{2,1,0:T(8,128)(2,1)S(1)}, u32[]{:S(2)}, u32[]{:S(2)}) async-start(bf16[4,32,2048]{2,1,0:T(8,128)(2,1)} %copy-done.1), calls=%async_computation.2 | async-start | bytes 1048576 | tf_op jit(solution)/shard_map/all_to_all | solution.py:221
  142.6 14.8 %collective-permute-start.21 = (bf16[256,1024]{1,0:T(8,128)(2,1)}, bf16[256,1024]{1,0:T(8,128)(2,1)}, u32[]{:S(2)}, u32[]{:S(2)}) collective-permute-start(bf16[256,1024]{1,0:T(8,128)(2,1)} %collective-permute-done.20.rest_6_), channel_id=1, source_target_pairs={{0,480},{32,0},{64,32},{96,64},{128,96},{160,128},{192,160},{224,1... | collective-permute-start | bytes 1572872 | tf_op jit(solution)/shard_map/ppermute | solution.py:178
  147.3 15.2 %collective-permute-start.18 = (bf16[256,1024]{1,0:T(8,128)(2,1)}, bf16[256,1024]{1,0:T(8,128)(2,1)}, u32[]{:S(2)}, u32[]{:S(2)}) collective-permute-start(bf16[256,1024]{1,0:T(8,128)(2,1)} %collective-permute-done.17.rest_3_), channel_id=1, source_target_pairs={{0,32},{32,64},{64,96},{96,128},{128,160},{160,192},{192,224},{224... | collective-permute-start | bytes 1572872 | tf_op jit(solution)/shard_map/ppermute | solution.py:178
  149.2 13.2 %collective-permute-start.14 = (bf16[128,2048]{1,0:T(8,128)(2,1)S(1)}, bf16[128,2048]{1,0:T(8,128)(2,1)S(1)}, u32[]{:S(2)}, u32[]{:S(2)}) collective-permute-start(bf16[128,2048]{1,0:T(8,128)(2,1)S(1)} %bitcast.30), channel_id=1, source_target_pairs={{0,1},{1,0},{2,3},{3,2},{4,5},{5,4},{6,7},{7,6},{8,9},{9,8},{10,11... | collective-permute-start | bytes 1572872 | tf_op jit(solution)/shard_map/ppermute | solution.py:217
  166.5 6.0 %collective-permute-start.22 = (bf16[128,2048]{1,0:T(8,128)(2,1)S(1)}, bf16[128,2048]{1,0:T(8,128)(2,1)S(1)}, u32[]{:S(2)}, u32[]{:S(2)}) collective-permute-start(bf16[128,2048]{1,0:T(8,128)(2,1)S(1)} %get-tuple-element.31), channel_id=1, source_target_pairs={{0,1},{1,0},{2,3},{3,2},{4,5},{5,4},{6,7},{7,6},{8,9},{9,8},{10,11... | collective-permute-start | bytes 1572872 | tf_op jit(solution)/shard_map/ppermute | solution.py:217
  172.6 12.6 %copy-start.3 = (f32[32,2048]{1,0:T(8,128)S(1)}, f32[32,2048]{1,0:T(8,128)}, u32[]{:S(2)}) copy-start(f32[32,2048]{1,0:T(8,128)} %copy-done.2) | copy-start | bytes 786436
  196.2 6.1 %collective-permute-start.23 = (bf16[128,2048]{1,0:T(8,128)(2,1)S(1)}, bf16[128,2048]{1,0:T(8,128)(2,1)S(1)}, u32[]{:S(2)}, u32[]{:S(2)}) collective-permute-start(bf16[128,2048]{1,0:T(8,128)(2,1)S(1)} %bitcast.35), channel_id=1, source_target_pairs={{0,1},{1,0},{2,3},{3,2},{4,5},{5,4},{6,7},{7,6},{8,9},{9,8},{10,11... | collective-permute-start | bytes 1572872 | tf_op jit(solution)/shard_map/ppermute | solution.py:217
  205.9 3.8 %collective-permute-start.24 = (bf16[128,2048]{1,0:T(8,128)(2,1)S(1)}, bf16[128,2048]{1,0:T(8,128)(2,1)S(1)}, u32[]{:S(2)}, u32[]{:S(2)}) collective-permute-start(bf16[128,2048]{1,0:T(8,128)(2,1)S(1)} %get-tuple-element.35), channel_id=1, source_target_pairs={{0,1},{1,0},{2,3},{3,2},{4,5},{5,4},{6,7},{7,6},{8,9},{9,8},{10,11... | collective-permute-start | bytes 1572872 | tf_op jit(solution)/shard_map/ppermute | solution.py:217
  (3 other events, 2.0 us)

commit v4 on v3

--- a/solution.py
+++ b/solution.py
@@ -64,6 +64,13 @@
         a, b = (value[:, i // 2 * 128 : i // 2 * 128 + 128] for i in (p, q))
         tiles.append(joined(((a, p % 2 == 1), (b, q % 2 == 0))))
     return jnp.concatenate(tiles, axis=1)
+
+
+def turned_in_place(value, y):
+    wide = 64 * NY
+    shift = lax.rem(wide - 64 * y, wide)
+    groups = [value[:, g : g + wide] for g in range(0, value.shape[1], wide)]
+    return jnp.concatenate([pltpu.roll(g, shift, 1) for g in groups], axis=1)
 
 
 def turned(ref, z, y):
@@ -113,7 +120,8 @@
     for k in range(rows_ref.shape[0]):
         rows_ref[k] = first
     for i, v in enumerate(small):
-        small_ref[i : i + 1, : v.shape[1]] = v[...]
+        for k in range(v.shape[0]):
+            small_ref[i : i + 1, k * 128 : k * 128 + 128] = v[k : k + 1, :]
 
 
 def pack(place, gate, up, down, ds, query, key, value, out, os, tokens, gains, small):
@@ -130,7 +138,6 @@
         ),
         in_specs=[SMEM] + [VMEM] * (11 + len(small)),
         out_specs=(VMEM,) * 6,
-        compiler_params=pltpu.CompilerParams(vmem_limit_bytes=12 * 1024 * 1024),
         name="pack",
     )(place, gate, up, down, ds, query, key, value, out, os, tokens, gains, *small)
 
@@ -140,7 +147,7 @@
     for k in range(1, NX):
         total = total + arrived[k].astype(jnp.float32)
     if arrived_as is not None:
-        total = shuffled(total, arrived_as)
+        total = shuffled(turned_in_place(total, place[1]), arrived_as)
     total = stream[...].astype(jnp.float32) + weight * total
     if which is None:
         z, y = place[0], place[1]
@@ -151,7 +158,7 @@
     rows = total * lax.rsqrt(jnp.mean(total * total, axis=-1, keepdims=True) + EPSILON)
     rows = rows * gains[which : which + 1, :]
     if rows_as is not None:
-        rows = shuffled(rows, rows_as)
+        rows = turned_in_place(shuffled(rows, rows_as), NY - place[1])
     rows = low(rows)
     for k in range(NX):
         last_ref[k] = rows
@@ -203,7 +210,6 @@
 
 def gather_mix(copies):
     mine = lax.all_to_all(copies, "y", split_axis=0, concat_axis=0, tiled=True)
-    mine = lax.dynamic_slice_in_dim(jnp.concatenate([mine, mine]), lax.axis_index("y"), NY)
     mine = mine.reshape(-1, copies.shape[2])
     up, down = [mine], [mine]
     for k in range(4):
@@ -328,7 +334,7 @@
     ffn_mine, mix_mine, copies, small, stream, gains = pack(
         place, gate_w, up_w, down_w.T, row(down_scale), query_w, key_w, value_w, out_w.T,
         row(out_scale), tokens_in, norm_gains,
-        [row(v) for v in (gate_scale, up_scale, query_scale, key_scale, value_scale, head_gain)],
+        [v.reshape(-1, 128) for v in (gate_scale, up_scale, query_scale, key_scale, value_scale, head_gain)],
     )
     ffn_arrays = gather_ffn(ffn_mine)
     every = lax.all_to_all(copies, ("x", "core"), split_axis=0, concat_axis=0, tiled=True)

time: 225 us -> 219 us (0.973)
  local copies, waits for them, and re-layouts: 15.7 us -> 7.71 us
    unnamed x48 -> x32, local copies, waits for them, and re-layouts: 14.3 us -> 7.69 us
where the time goes in v4:
time: 219 us; the launch traced here: 218 us
  starting transfers between devices  106 us (48%)
  waiting for transfers between devices  48 us (22%)
  blocking collectives  34.5 us (16%)
  Pallas kernels  17.2 us (8%)
  local copies, waits for them, and re-layouts  7.71 us (4%)
  other arithmetic  2.82 us (1%)
    ppermute x14, starting transfers between devices, along_z(): lax.ppermute(array, ('rep', 'z'), [(g, (g + step) % (2 * NZ)) for g in ra...  47.5 us
    all_to_all x2, blocking collectives, return_rows(): return lax.all_to_all(blocks, 'x', split_axis=0, concat_axis=0, tiled=True)  24.2 us
    ppermute x14, waiting for transfers between devices, along_z(): lax.ppermute(array, ('rep', 'z'), [(g, (g + step) % (2 * NZ)) for g in ra...  24.1 us
    ppermute x5, starting transfers between devices, swap_cores(): return lax.ppermute(array, 'core', [(0, 1), (1, 0)])  19.5 us
    ppermute x6, waiting for transfers between devices, along_y(): return lax.ppermute(array, 'y', [(g, (g + step) % NY) for g in range(NY)])  19.4 us
    ppermute x6, starting transfers between devices, along_y(): return lax.ppermute(array, 'y', [(g, (g + step) % NY) for g in range(NY)])  18.5 us
    all_to_all x1, blocking collectives, gather_rows(): own = lax.all_to_all(copies, 'x', split_axis=0, concat_axis=0, tiled=True)  10.3 us
    all_to_all x1, starting transfers between devices, on_device(): lax.all_to_all(copies, ('x', 'core'), split_axis=0, concat_axis=0, tiled=...  8.37 us
  transfers between devices with their start and end apart: 29, of which 13 were waited for; matrix products, arithmetic and copies ran while one was open for 2% of the time, Pallas kernels for 2%

profile of v4, /device:TPU:1, one launch (start us, length us, event | category | flops | bytes accessed | tf_op | source)
XLA Modules:
  0.0 217.7 jit_solution(4708490341043864434)
XLA Ops:
  0.6 2.9 %pack.1 = (bf16[64,1152]{1,0:T(8,128)(2,1)}, bf16[4,64,1024]{2,1,0:T(8,128)(2,1)}, bf16[8,32,2048]{2,1,0:T(8,128)(2,1)}, f32[8,384]{1,0:T(8,128)}, bf16[32,2048]{1,0:T(8,128)(2,1)}, /*index=5*/f32[3,2048]{1,0:T(4,128)}) custom-call(s32[3]{0:T(128)} %pad_add_fusion.place.refs_0_, f32[64,384]{1,0:T(8,128)} %gate.1, f32[64,384]{1,0:T(8,128)} %up.1, ...), custom_call_target="tpu_custom_call" | custom-call | tf_op jit(solution)/shard_map/pack/pallas_call | solution.py:129
  3.5 11.9 %collective-permute-start.1 = (bf16[64,1152]{1,0:T(8,128)(2,1)}, bf16[64,1152]{1,0:T(8,128)(2,1)}, u32[]{:S(2)}, u32[]{:S(2)}) collective-permute-start(bf16[64,1152]{1,0:T(8,128)(2,1)} %get-tuple-element.23), channel_id=1, source_target_pairs={{0,480},{32,0},{64,32},{96,64},{128,96},{160,128},{192,160},{224,1... | collective-permute-start | bytes 442376 | tf_op jit(solution)/shard_map/ppermute | solution.py:185
  15.4 1.9 collective-permute-start
  17.4 4.3 %all-to-all-start.3 = ((bf16[4,64,1024]{2,1,0:T(8,128)(2,1)}), bf16[4,64,1024]{2,1,0:T(8,128)(2,1)S(1)}, u32[]{:S(2)}, u32[]{:S(2)}) async-start(bf16[4,64,1024]{2,1,0:T(8,128)(2,1)} %get-tuple-element.29), calls=%async_computation.3 | async-start | bytes 1048576 | tf_op jit(solution)/shard_map/all_to_all | solution.py:212
  21.7 4.6 %collective-permute-start.3 = (bf16[64,1152]{1,0:T(8,128)(2,1)}, bf16[64,1152]{1,0:T(8,128)(2,1)S(1)}, u32[]{:S(2)}, u32[]{:S(2)}) collective-permute-start(bf16[64,1152]{1,0:T(8,128)(2,1)} %collective-permute-done.1), channel_id=1, source_target_pairs={{0,480},{32,0},{64,32},{96,64},{128,96},{160,128},{192,160},{224,1... | collective-permute-start | bytes 442376 | tf_op jit(solution)/shard_map/ppermute | solution.py:185
  26.3 1.9 collective-permute-start.2
  30.1 3.6 %collective-permute-done.2 = bf16[64,1152]{1,0:T(8,128)(2,1)} collective-permute-done((bf16[64,1152]{1,0:T(8,128)(2,1)}, bf16[64,1152]{1,0:T(8,128)(2,1)}, u32[]{:S(2)}, u32[]{:S(2)}) %collective-permute-start.2) | collective-permute-done | bytes 147488 | tf_op jit(solution)/shard_map/ppermute | solution.py:185
  34.7 3.4 %collective-permute-start.4 = (bf16[5,64,1152]{2,1,0:T(8,128)(2,1)S(1)}, bf16[5,64,1152]{2,1,0:T(8,128)(2,1)S(1)}, u32[]{:S(2)}, u32[]{:S(2)}) collective-permute-start(bf16[5,64,1152]{2,1,0:T(8,128)(2,1)S(1)} %bitcast_dynamic-update-slice_fusion.refs_3_.refs_4_), channel_id=1, source_target_pairs={{0,8},{8,16},{16,24},{24,0},{1,9},{9,17},{17,25},{25,1},{2,10},{10... | collective-permute-start | bytes 2211848 | tf_op jit(solution)/shard_map/ppermute | solution.py:189
  38.1 1.9 collective-permute-start.8
  40.0 4.3 %collective-permute-start.7 = (bf16[64,1152]{1,0:T(8,128)(2,1)}, bf16[64,1152]{1,0:T(8,128)(2,1)S(1)}, u32[]{:S(2)}, u32[]{:S(2)}) collective-permute-start(bf16[64,1152]{1,0:T(8,128)(2,1)} %collective-permute-done), channel_id=1, source_target_pairs={{0,64},{32,96},{64,128},{96,160},{128,192},{160,224},{192,256},{22... | collective-permute-start | bytes 442376 | tf_op jit(solution)/shard_map/ppermute | solution.py:185
  44.3 1.9 collective-permute-start.9
  46.2 8.4 %all-to-all-start = ((bf16[8,32,2048]{2,1,0:T(8,128)(2,1)}), bf16[8,32,2048]{2,1,0:T(8,128)(2,1)S(1)}, u32[]{:S(2)}, u32[]{:S(2)}) async-start(bf16[8,32,2048]{2,1,0:T(8,128)(2,1)} %get-tuple-element.22), calls=%async_computation | async-start | bytes 2097152 | tf_op jit(solution)/shard_map/all_to_all | solution.py:340
  54.6 4.4 %collective-permute-done.9 = bf16[64,1152]{1,0:T(8,128)(2,1)S(1)} collective-permute-done((bf16[64,1152]{1,0:T(8,128)(2,1)}, bf16[64,1152]{1,0:T(8,128)(2,1)S(1)}, u32[]{:S(2)}, u32[]{:S(2)}) %collective-permute-start.9) | collective-permute-done | bytes 147488 | tf_op jit(solution)/shard_map/ppermute | solution.py:185
  60.8 3.1 %collective-permute-start.11 = (bf16[3,64,1152]{2,1,0:T(8,128)(2,1)S(1)}, bf16[3,64,1152]{2,1,0:T(8,128)(2,1)}, u32[]{:S(2)}, u32[]{:S(2)}) collective-permute-start(bf16[3,64,1152]{2,1,0:T(8,128)(2,1)S(1)} %pad_maximum_fusion.refs_7_.refs_8_), channel_id=1, source_target_pairs={{0,24},{8,0},{16,8},{24,16},{1,25},{9,1},{17,9},{25,17},{2,26},{10... | collective-permute-start | bytes 1327112 | tf_op jit(solution)/shard_map/ppermute | solution.py:189
  63.9 3.4 %collective-permute-start.5 = (bf16[5,64,1152]{2,1,0:T(8,128)(2,1)S(1)}, bf16[5,64,1152]{2,1,0:T(8,128)(2,1)}, u32[]{:S(2)}, u32[]{:S(2)}) collective-permute-start(bf16[5,64,1152]{2,1,0:T(8,128)(2,1)S(1)} %bitcast_dynamic-update-slice_fusion.refs_3_.refs_4_), channel_id=1, source_target_pairs={{0,24},{8,0},{16,8},{24,16},{1,25},{9,1},{17,9},{25,17},{2,26},{10... | collective-permute-start | bytes 2211848 | tf_op jit(solution)/shard_map/ppermute | solution.py:189
  67.3 1.9 collective-permute-start.6
  69.3 2.2 collective-permute-start.10
  72.8 4.6 %collective-permute-start.12 = (bf16[3,64,1152]{2,1,0:T(8,128)(2,1)}, bf16[3,64,1152]{2,1,0:T(8,128)(2,1)}, u32[]{:S(2)}, u32[]{:S(2)}) collective-permute-start(bf16[3,64,1152]{2,1,0:T(8,128)(2,1)} %collective-permute-done.11.refs_9_.refs_10_), channel_id=1, source_target_pairs={{0,24},{8,0},{16,8},{24,16},{1,25},{9,1},{17,9},{25,17},{2,26},{10... | collective-permute-start | bytes 1327112 | tf_op jit(solution)/shard_map/ppermute | solution.py:189
  77.4 1.9 collective-permute-start.15
  79.3 16.4 %collective-permute-done.10.refs_8_.refs_9_ = bf16[3,64,1152]{2,1,0:T(8,128)(2,1)S(1)} collective-permute-done((bf16[3,64,1152]{2,1,0:T(8,128)(2,1)S(1)}, bf16[3,64,1152]{2,1,0:T(8,128)(2,1)S(1)}, u32[]{:S(2)}, u32[]{:S(2)}) %collective-permute-start.10) | collective-permute-done | bytes 442400 | tf_op jit(solution)/shard_map/ppermute | solution.py:189
  96.5 1.6 collective-permute-done.12.refs_10_.refs_11_
  99.2 3.5 %ffn.2 = (f32[128,2048]{1,0:T(8,128)S(1)}, bf16[128,2048]{1,0:T(8,128)(2,1)S(1)}) custom-call(s32[3]{0:T(128)S(1)} %copy-done.9, f32[8,384]{1,0:T(8,128)S(1)} %copy-done.8, bf16[8,32,2048]{2,1,0:T(8,128)(2,1)S(1)} %all-to-all-done.refs_2_, bf16[5,64,1152]{2,1,0:T(8,128)(2,1)S(1)} %bitcast_dynamic-update-slice_fusion.refs_3_.refs_4_, ...), custom_call_target="tpu_custom_call" | custom-call | tf_op jit(solution)/shard_map/ffn/pallas_call | solution.py:265
  102.6 4.5 %collective-permute-start.13 = (bf16[128,2048]{1,0:T(8,128)(2,1)S(1)}, bf16[128,2048]{1,0:T(8,128)(2,1)S(1)}, u32[]{:S(2)}, u32[]{:S(2)}) collective-permute-start(bf16[128,2048]{1,0:T(8,128)(2,1)S(1)} %get-tuple-element.25), channel_id=1, source_target_pairs={{0,1},{1,0},{2,3},{3,2},{4,5},{5,4},{6,7},{7,6},{8,9},{9,8},{10,11... | collective-permute-start | bytes 1572872 | tf_op jit(solution)/shard_map/ppermute | solution.py:223
  107.1 1.9 collective-permute-start.19
  109.0 3.4 %collective-permute-start.16 = (bf16[256,1024]{1,0:T(8,128)(2,1)}, bf16[256,1024]{1,0:T(8,128)(2,1)}, u32[]{:S(2)}, u32[]{:S(2)}) collective-permute-start(bf16[256,1024]{1,0:T(8,128)(2,1)} %collective-permute-done.15.rest_1_), channel_id=1, source_target_pairs={{0,32},{32,64},{64,96},{96,128},{128,160},{160,192},{192,224},{224... | collective-permute-start | bytes 1572872 | tf_op jit(solution)/shard_map/ppermute | solution.py:185
  113.3 4.1 %all-to-all-start.1 = ((bf16[4,32,2048]{2,1,0:T(8,128)(2,1)}), bf16[4,32,2048]{2,1,0:T(8,128)(2,1)S(1)}, u32[]{:S(2)}, u32[]{:S(2)}) async-start(bf16[4,32,2048]{2,1,0:T(8,128)(2,1)} %bitcast.39), calls=%async_computation.1 | async-start | bytes 1048576 | tf_op jit(solution)/shard_map/all_to_all | solution.py:236
  117.5 5.1 %collective-permute-done.19.rest_5_ = bf16[256,1024]{1,0:T(8,128)(2,1)S(1)} collective-permute-done((bf16[256,1024]{1,0:T(8,128)(2,1)S(1)}, bf16[256,1024]{1,0:T(8,128)(2,1)S(1)}, u32[]{:S(2)}, u32[]{:S(2)}) %collective-permute-start.19) | collective-permute-done | bytes 524320 | tf_op jit(solution)/shard_map/ppermute | solution.py:185
  122.6 3.3 %collective-permute-start.20 = (bf16[256,1024]{1,0:T(8,128)(2,1)S(1)}, bf16[256,1024]{1,0:T(8,128)(2,1)}, u32[]{:S(2)}, u32[]{:S(2)}) collective-permute-start(bf16[256,1024]{1,0:T(8,128)(2,1)S(1)} %collective-permute-done.19.rest_5_), channel_id=1, source_target_pairs={{0,480},{32,0},{64,32},{96,64},{128,96},{160,128},{192,160},{224,1... | collective-permute-start | bytes 1572872 | tf_op jit(solution)/shard_map/ppermute | solution.py:185
  125.9 1.9 collective-permute-start.17
  131.3 4.0 %all-to-all-start.2 = ((bf16[4,32,2048]{2,1,0:T(8,128)(2,1)}), bf16[4,32,2048]{2,1,0:T(8,128)(2,1)S(1)}, u32[]{:S(2)}, u32[]{:S(2)}) async-start(bf16[4,32,2048]{2,1,0:T(8,128)(2,1)} %copy-done.3), calls=%async_computation.2 | async-start | bytes 1048576 | tf_op jit(solution)/shard_map/all_to_all | solution.py:227
  135.3 2.0 collective-permute-done.20.rest_6_
  137.3 4.7 %collective-permute-start.21 = (bf16[256,1024]{1,0:T(8,128)(2,1)}, bf16[256,1024]{1,0:T(8,128)(2,1)}, u32[]{:S(2)}, u32[]{:S(2)}) collective-permute-start(bf16[256,1024]{1,0:T(8,128)(2,1)} %collective-permute-done.20.rest_6_), channel_id=1, source_target_pairs={{0,480},{32,0},{64,32},{96,64},{128,96},{160,128},{192,160},{224,1... | collective-permute-start | bytes 1572872 | tf_op jit(solution)/shard_map/ppermute | solution.py:185
  142.0 1.9 collective-permute-start.18
  143.9 3.7 %collective-permute-start.14 = (bf16[128,2048]{1,0:T(8,128)(2,1)S(1)}, bf16[128,2048]{1,0:T(8,128)(2,1)S(1)}, u32[]{:S(2)}, u32[]{:S(2)}) collective-permute-start(bf16[128,2048]{1,0:T(8,128)(2,1)S(1)} %bitcast.35), channel_id=1, source_target_pairs={{0,1},{1,0},{2,3},{3,2},{4,5},{5,4},{6,7},{7,6},{8,9},{9,8},{10,11... | collective-permute-start | bytes 1572872 | tf_op jit(solution)/shard_map/ppermute | solution.py:223
  148.3 3.8 %collective-permute-done.21.rest_7_ = bf16[256,1024]{1,0:T(8,128)(2,1)} collective-permute-done((bf16[256,1024]{1,0:T(8,128)(2,1)}, bf16[256,1024]{1,0:T(8,128)(2,1)}, u32[]{:S(2)}, u32[]{:S(2)}) %collective-permute-start.21) | collective-permute-done | bytes 524320 | tf_op jit(solution)/shard_map/ppermute | solution.py:185
  152.1 5.1 %collective-permute-done.18.rest_4_ = bf16[256,1024]{1,0:T(8,128)(2,1)} collective-permute-done((bf16[256,1024]{1,0:T(8,128)(2,1)}, bf16[256,1024]{1,0:T(8,128)(2,1)}, u32[]{:S(2)}, u32[]{:S(2)}) %collective-permute-start.18) | collective-permute-done | bytes 524320 | tf_op jit(solution)/shard_map/ppermute | solution.py:185
  157.1 4.1 %mix.1 = (f32[128,2048]{1,0:T(8,128)S(1)}, bf16[128,2048]{1,0:T(8,128)(2,1)S(1)}) custom-call(s32[3]{0:T(128)S(1)} %copy-done.9, f32[1]{0:T(128)S(6)} %copy.23.rate, f32[8,384]{1,0:T(8,128)S(1)} %copy-done.8, bf16[128,2048]{1,0:T(8,128)(2,1)S(1)} %bitcast.36, bf16[128,2048]{1,0:T(8,128)(2,1)S(1)} %collective-permute-done.14.other_rows, ...), custom_call_target="tpu_custom_call" | custom-call | tf_op jit(solution)/shard_map/mix/pallas_call | solution.py:311
  161.2 4.5 %collective-permute-start.22 = (bf16[128,2048]{1,0:T(8,128)(2,1)S(1)}, bf16[128,2048]{1,0:T(8,128)(2,1)S(1)}, u32[]{:S(2)}, u32[]{:S(2)}) collective-permute-start(bf16[128,2048]{1,0:T(8,128)(2,1)S(1)} %get-tuple-element.31), channel_id=1, source_target_pairs={{0,1},{1,0},{2,3},{3,2},{4,5},{5,4},{6,7},{7,6},{8,9},{9,8},{10,11... | collective-permute-start | bytes 1572872 | tf_op jit(solution)/shard_map/ppermute | solution.py:223
  165.7 1.5 collective-permute-done.22
  167.4 12.6 %all_to_all.35.refs_1_ = bf16[4,32,2048]{2,1,0:T(8,128)(2,1)S(1)} all-to-all(bf16[4,32,2048]{2,1,0:T(8,128)(2,1)S(1)} %bitcast.40), channel_id=1, replica_groups=mesh['rep'=2,'z'=8,'y'=4,'x'=4,'core'=2] {'x'}, dimensions={0} | all-to-all | bytes 1048576 | tf_op jit(solution)/shard_map/all_to_all | solution.py:236
  180.8 10.3 %all_to_all.36 = bf16[4,32,2048]{2,1,0:T(8,128)(2,1)S(1)} all-to-all(bf16[4,32,2048]{2,1,0:T(8,128)(2,1)S(1)} %get-tuple-element.33), channel_id=1, replica_groups=mesh['rep'=2,'z'=8,'y'=4,'x'=4,'core'=2] {'x'}, dimensions={0} | all-to-all | bytes 1048576 | tf_op jit(solution)/shard_map/all_to_all | solution.py:227
  191.1 4.6 %collective-permute-start.23 = (bf16[128,2048]{1,0:T(8,128)(2,1)S(1)}, bf16[128,2048]{1,0:T(8,128)(2,1)S(1)}, u32[]{:S(2)}, u32[]{:S(2)}) collective-permute-start(bf16[128,2048]{1,0:T(8,128)(2,1)S(1)} %bitcast.37), channel_id=1, source_target_pairs={{0,1},{1,0},{2,3},{3,2},{4,5},{5,4},{6,7},{7,6},{8,9},{9,8},{10,11... | collective-permute-start | bytes 1572872 | tf_op jit(solution)/shard_map/ppermute | solution.py:223
  195.7 1.5 collective-permute-done.23.refs_3_
  197.2 3.5 %ffn.3 = (f32[128,2048]{1,0:T(8,128)S(1)}, bf16[128,2048]{1,0:T(8,128)(2,1)S(1)}) custom-call(s32[3]{0:T(128)S(1)} %copy-done.9, f32[8,384]{1,0:T(8,128)S(1)} %copy-done.8, bf16[128,2048]{1,0:T(8,128)(2,1)S(1)} %bitcast.38, bf16[128,2048]{1,0:T(8,128)(2,1)S(1)} %collective-permute-done.23.refs_3_, ...), custom_call_target="tpu_custom_call" | custom-call | tf_op jit(solution)/shard_map/ffn/pallas_call | solution.py:265
  200.7 2.3 %collective-permute-start.24 = (bf16[128,2048]{1,0:T(8,128)(2,1)S(1)}, bf16[128,2048]{1,0:T(8,128)(2,1)S(1)}, u32[]{:S(2)}, u32[]{:S(2)}) collective-permute-start(bf16[128,2048]{1,0:T(8,128)(2,1)S(1)} %get-tuple-element.35), channel_id=1, source_target_pairs={{0,1},{1,0},{2,3},{3,2},{4,5},{5,4},{6,7},{7,6},{8,9},{9,8},{10,11... | collective-permute-start | bytes 1572872 | tf_op jit(solution)/shard_map/ppermute | solution.py:223
  203.0 1.5 collective-permute-done.24
  204.6 11.6 %all_to_all.37.refs_1_ = bf16[4,32,2048]{2,1,0:T(8,128)(2,1)S(1)} all-to-all(bf16[4,32,2048]{2,1,0:T(8,128)(2,1)S(1)} %bitcast.41), channel_id=1, replica_groups=mesh['rep'=2,'z'=8,'y'=4,'x'=4,'core'=2] {'x'}, dimensions={0} | all-to-all | bytes 1048576 | tf_op jit(solution)/shard_map/all_to_all | solution.py:236
  216.2 1.5 join.5
  (58 shorter events, 13.9 us)
Async XLA Ops:
  3.5 18.2 %collective-permute-start.1 = (bf16[64,1152]{1,0:T(8,128)(2,1)}, bf16[64,1152]{1,0:T(8,128)(2,1)}, u32[]{:S(2)}, u32[]{:S(2)}) collective-permute-start(bf16[64,1152]{1,0:T(8,128)(2,1)} %get-tuple-element.23), channel_id=1, source_target_pairs={{0,480},{32,0},{64,32},{96,64},{128,96},{160,128},{192,160},{224,1... | collective-permute-start | bytes 442376 | tf_op jit(solution)/shard_map/ppermute | solution.py:185
  15.4 10.9 %collective-permute-start = (bf16[64,1152]{1,0:T(8,128)(2,1)}, bf16[64,1152]{1,0:T(8,128)(2,1)}, u32[]{:S(2)}, u32[]{:S(2)}) collective-permute-start(bf16[64,1152]{1,0:T(8,128)(2,1)} %get-tuple-element.23), channel_id=1, source_target_pairs={{0,32},{32,64},{64,96},{96,128},{128,160},{160,192},{192,224},{224... | collective-permute-start | bytes 442376 | tf_op jit(solution)/shard_map/ppermute | solution.py:185
  17.4 4.3 %copy-start.13 = (bf16[64,1152]{1,0:T(8,128)(2,1)S(1)}, bf16[64,1152]{1,0:T(8,128)(2,1)}, u32[]{:S(2)}) copy-start(bf16[64,1152]{1,0:T(8,128)(2,1)} %get-tuple-element.23) | copy-start | bytes 442372
  17.4 28.8 %all-to-all-start.3 = ((bf16[4,64,1024]{2,1,0:T(8,128)(2,1)}), bf16[4,64,1024]{2,1,0:T(8,128)(2,1)S(1)}, u32[]{:S(2)}, u32[]{:S(2)}) async-start(bf16[4,64,1024]{2,1,0:T(8,128)(2,1)} %get-tuple-element.29), calls=%async_computation.3 | async-start | bytes 1048576 | tf_op jit(solution)/shard_map/all_to_all | solution.py:212
  21.7 12.9 %collective-permute-start.3 = (bf16[64,1152]{1,0:T(8,128)(2,1)}, bf16[64,1152]{1,0:T(8,128)(2,1)S(1)}, u32[]{:S(2)}, u32[]{:S(2)}) collective-permute-start(bf16[64,1152]{1,0:T(8,128)(2,1)} %collective-permute-done.1), channel_id=1, source_target_pairs={{0,480},{32,0},{64,32},{96,64},{128,96},{160,128},{192,160},{224,1... | collective-permute-start | bytes 442376 | tf_op jit(solution)/shard_map/ppermute | solution.py:185
  26.3 7.4 %collective-permute-start.2 = (bf16[64,1152]{1,0:T(8,128)(2,1)}, bf16[64,1152]{1,0:T(8,128)(2,1)}, u32[]{:S(2)}, u32[]{:S(2)}) collective-permute-start(bf16[64,1152]{1,0:T(8,128)(2,1)} %collective-permute-done), channel_id=1, source_target_pairs={{0,32},{32,64},{64,96},{96,128},{128,160},{160,192},{192,224},{224... | collective-permute-start | bytes 442376 | tf_op jit(solution)/shard_map/ppermute | solution.py:185
  34.7 32.6 %collective-permute-start.4 = (bf16[5,64,1152]{2,1,0:T(8,128)(2,1)S(1)}, bf16[5,64,1152]{2,1,0:T(8,128)(2,1)S(1)}, u32[]{:S(2)}, u32[]{:S(2)}) collective-permute-start(bf16[5,64,1152]{2,1,0:T(8,128)(2,1)S(1)} %bitcast_dynamic-update-slice_fusion.refs_3_.refs_4_), channel_id=1, source_target_pairs={{0,8},{8,16},{16,24},{24,0},{1,9},{9,17},{17,25},{25,1},{2,10},{10... | collective-permute-start | bytes 2211848 | tf_op jit(solution)/shard_map/ppermute | solution.py:189
  38.1 16.5 %collective-permute-start.8 = (bf16[64,1152]{1,0:T(8,128)(2,1)}, bf16[64,1152]{1,0:T(8,128)(2,1)S(1)}, u32[]{:S(2)}, u32[]{:S(2)}) collective-permute-start(bf16[64,1152]{1,0:T(8,128)(2,1)} %collective-permute-done.1), channel_id=1, source_target_pairs={{0,448},{32,480},{64,0},{96,32},{128,64},{160,96},{192,128},{224,1... | collective-permute-start | bytes 442376 | tf_op jit(solution)/shard_map/ppermute | solution.py:185
  40.0 14.6 %collective-permute-start.7 = (bf16[64,1152]{1,0:T(8,128)(2,1)}, bf16[64,1152]{1,0:T(8,128)(2,1)S(1)}, u32[]{:S(2)}, u32[]{:S(2)}) collective-permute-start(bf16[64,1152]{1,0:T(8,128)(2,1)} %collective-permute-done), channel_id=1, source_target_pairs={{0,64},{32,96},{64,128},{96,160},{128,192},{160,224},{192,256},{22... | collective-permute-start | bytes 442376 | tf_op jit(solution)/shard_map/ppermute | solution.py:185
  44.3 14.8 %collective-permute-start.9 = (bf16[64,1152]{1,0:T(8,128)(2,1)}, bf16[64,1152]{1,0:T(8,128)(2,1)S(1)}, u32[]{:S(2)}, u32[]{:S(2)}) collective-permute-start(bf16[64,1152]{1,0:T(8,128)(2,1)} %collective-permute-done.2), channel_id=1, source_target_pairs={{0,64},{32,96},{64,128},{96,160},{128,192},{160,224},{192,256},{22... | collective-permute-start | bytes 442376 | tf_op jit(solution)/shard_map/ppermute | solution.py:185
  46.2 50.3 %all-to-all-start = ((bf16[8,32,2048]{2,1,0:T(8,128)(2,1)}), bf16[8,32,2048]{2,1,0:T(8,128)(2,1)S(1)}, u32[]{:S(2)}, u32[]{:S(2)}) async-start(bf16[8,32,2048]{2,1,0:T(8,128)(2,1)} %get-tuple-element.22), calls=%async_computation | async-start | bytes 2097152 | tf_op jit(solution)/shard_map/all_to_all | solution.py:340
  54.6 4.4 %copy-start.10 = (bf16[64,1152]{1,0:T(8,128)(2,1)}, bf16[64,1152]{1,0:T(8,128)(2,1)S(1)}, u32[]{:S(2)}) copy-start(bf16[64,1152]{1,0:T(8,128)(2,1)S(1)} %collective-permute-done.8) | copy-start | bytes 442372
  54.6 4.4 %copy-start.11 = (bf16[64,1152]{1,0:T(8,128)(2,1)}, bf16[64,1152]{1,0:T(8,128)(2,1)S(1)}, u32[]{:S(2)}) copy-start(bf16[64,1152]{1,0:T(8,128)(2,1)S(1)} %collective-permute-done.7) | copy-start | bytes 442372
  59.0 0.6 copy-start.12
  59.7 38.4 %copy-start.8 = (f32[8,384]{1,0:T(8,128)S(1)}, f32[8,384]{1,0:T(8,128)}, u32[]{:S(2)}) copy-start(f32[8,384]{1,0:T(8,128)} %get-tuple-element.21.refs_1_.small) | copy-start | bytes 36868
  60.8 12.0 %collective-permute-start.11 = (bf16[3,64,1152]{2,1,0:T(8,128)(2,1)S(1)}, bf16[3,64,1152]{2,1,0:T(8,128)(2,1)}, u32[]{:S(2)}, u32[]{:S(2)}) collective-permute-start(bf16[3,64,1152]{2,1,0:T(8,128)(2,1)S(1)} %pad_maximum_fusion.refs_7_.refs_8_), channel_id=1, source_target_pairs={{0,24},{8,0},{16,8},{24,16},{1,25},{9,1},{17,9},{25,17},{2,26},{10... | collective-permute-start | bytes 1327112 | tf_op jit(solution)/shard_map/ppermute | solution.py:189
  63.9 32.6 %collective-permute-start.5 = (bf16[5,64,1152]{2,1,0:T(8,128)(2,1)S(1)}, bf16[5,64,1152]{2,1,0:T(8,128)(2,1)}, u32[]{:S(2)}, u32[]{:S(2)}) collective-permute-start(bf16[5,64,1152]{2,1,0:T(8,128)(2,1)S(1)} %bitcast_dynamic-update-slice_fusion.refs_3_.refs_4_), channel_id=1, source_target_pairs={{0,24},{8,0},{16,8},{24,16},{1,25},{9,1},{17,9},{25,17},{2,26},{10... | collective-permute-start | bytes 2211848 | tf_op jit(solution)/shard_map/ppermute | solution.py:189
  67.3 30.8 %collective-permute-start.6 = (bf16[5,64,1152]{2,1,0:T(8,128)(2,1)S(1)}, bf16[5,64,1152]{2,1,0:T(8,128)(2,1)}, u32[]{:S(2)}, u32[]{:S(2)}) collective-permute-start(bf16[5,64,1152]{2,1,0:T(8,128)(2,1)S(1)} %collective-permute-done.4.refs_4_.refs_5_), channel_id=1, source_target_pairs={{0,8},{8,16},{16,24},{24,0},{1,9},{9,17},{17,25},{25,1},{2,10},{10... | collective-permute-start | bytes 2211848 | tf_op jit(solution)/shard_map/ppermute | solution.py:189
  69.3 26.4 %collective-permute-start.10 = (bf16[3,64,1152]{2,1,0:T(8,128)(2,1)S(1)}, bf16[3,64,1152]{2,1,0:T(8,128)(2,1)S(1)}, u32[]{:S(2)}, u32[]{:S(2)}) collective-permute-start(bf16[3,64,1152]{2,1,0:T(8,128)(2,1)S(1)} %pad_maximum_fusion.refs_7_.refs_8_), channel_id=1, source_target_pairs={{0,8},{8,16},{16,24},{24,0},{1,9},{9,17},{17,25},{25,1},{2,10},{10... | collective-permute-start | bytes 1327112 | tf_op jit(solution)/shard_map/ppermute | solution.py:189
  72.8 25.3 %collective-permute-start.12 = (bf16[3,64,1152]{2,1,0:T(8,128)(2,1)}, bf16[3,64,1152]{2,1,0:T(8,128)(2,1)}, u32[]{:S(2)}, u32[]{:S(2)}) collective-permute-start(bf16[3,64,1152]{2,1,0:T(8,128)(2,1)} %collective-permute-done.11.refs_9_.refs_10_), channel_id=1, source_target_pairs={{0,24},{8,0},{16,8},{24,16},{1,25},{9,1},{17,9},{25,17},{2,26},{10... | collective-permute-start | bytes 1327112 | tf_op jit(solution)/shard_map/ppermute | solution.py:189
  77.4 20.7 %copy-start.9 = (s32[3]{0:T(128)S(1)}, s32[3]{0:T(128)}, u32[]{:S(2)}) copy-start(s32[3]{0:T(128)} %pad_add_fusion.place.refs_0_) | copy-start | bytes 40
  77.4 31.6 %collective-permute-start.15 = (bf16[256,1024]{1,0:T(8,128)(2,1)S(1)}, bf16[256,1024]{1,0:T(8,128)(2,1)}, u32[]{:S(2)}, u32[]{:S(2)}) collective-permute-start(bf16[256,1024]{1,0:T(8,128)(2,1)S(1)} %bitcast.32), channel_id=1, source_target_pairs={{0,32},{32,64},{64,96},{96,128},{128,160},{160,192},{192,224},{224... | collective-permute-start | bytes 1572872 | tf_op jit(solution)/shard_map/ppermute | solution.py:185
  95.7 0.8 copy-start
  98.1 1.0 copy-start.1
  102.6 9.8 %collective-permute-start.13 = (bf16[128,2048]{1,0:T(8,128)(2,1)S(1)}, bf16[128,2048]{1,0:T(8,128)(2,1)S(1)}, u32[]{:S(2)}, u32[]{:S(2)}) collective-permute-start(bf16[128,2048]{1,0:T(8,128)(2,1)S(1)} %get-tuple-element.25), channel_id=1, source_target_pairs={{0,1},{1,0},{2,3},{3,2},{4,5},{5,4},{6,7},{7,6},{8,9},{9,8},{10,11... | collective-permute-start | bytes 1572872 | tf_op jit(solution)/shard_map/ppermute | solution.py:223
  107.1 15.5 %collective-permute-start.19 = (bf16[256,1024]{1,0:T(8,128)(2,1)S(1)}, bf16[256,1024]{1,0:T(8,128)(2,1)S(1)}, u32[]{:S(2)}, u32[]{:S(2)}) collective-permute-start(bf16[256,1024]{1,0:T(8,128)(2,1)S(1)} %bitcast.33), channel_id=1, source_target_pairs={{0,480},{32,0},{64,32},{96,64},{128,96},{160,128},{192,160},{224,1... | collective-permute-start | bytes 1572872 | tf_op jit(solution)/shard_map/ppermute | solution.py:185
  109.0 16.9 %collective-permute-start.16 = (bf16[256,1024]{1,0:T(8,128)(2,1)}, bf16[256,1024]{1,0:T(8,128)(2,1)}, u32[]{:S(2)}, u32[]{:S(2)}) collective-permute-start(bf16[256,1024]{1,0:T(8,128)(2,1)} %collective-permute-done.15.rest_1_), channel_id=1, source_target_pairs={{0,32},{32,64},{64,96},{96,128},{128,160},{160,192},{192,224},{224... | collective-permute-start | bytes 1572872 | tf_op jit(solution)/shard_map/ppermute | solution.py:185
  113.3 14.5 %copy-start.4 = (f32[3,2048]{1,0:T(4,128)S(1)}, f32[3,2048]{1,0:T(4,128)}, u32[]{:S(2)}) copy-start(f32[3,2048]{1,0:T(4,128)} %get-tuple-element.27.refs_3_) | copy-start | bytes 73732
  113.3 14.5 %all-to-all-start.1 = ((bf16[4,32,2048]{2,1,0:T(8,128)(2,1)}), bf16[4,32,2048]{2,1,0:T(8,128)(2,1)S(1)}, u32[]{:S(2)}, u32[]{:S(2)}) async-start(bf16[4,32,2048]{2,1,0:T(8,128)(2,1)} %bitcast.39), calls=%async_computation.1 | async-start | bytes 1048576 | tf_op jit(solution)/shard_map/all_to_all | solution.py:236
  122.6 14.7 %collective-permute-start.20 = (bf16[256,1024]{1,0:T(8,128)(2,1)S(1)}, bf16[256,1024]{1,0:T(8,128)(2,1)}, u32[]{:S(2)}, u32[]{:S(2)}) collective-permute-start(bf16[256,1024]{1,0:T(8,128)(2,1)S(1)} %collective-permute-done.19.rest_5_), channel_id=1, source_target_pairs={{0,480},{32,0},{64,32},{96,64},{128,96},{160,128},{192,160},{224,1... | collective-permute-start | bytes 1572872 | tf_op jit(solution)/shard_map/ppermute | solution.py:185
  125.9 16.0 %collective-permute-start.17 = (bf16[256,1024]{1,0:T(8,128)(2,1)}, bf16[256,1024]{1,0:T(8,128)(2,1)}, u32[]{:S(2)}, u32[]{:S(2)}) collective-permute-start(bf16[256,1024]{1,0:T(8,128)(2,1)} %collective-permute-done.16.rest_2_), channel_id=1, source_target_pairs={{0,32},{32,64},{64,96},{96,128},{128,160},{160,192},{192,224},{224... | collective-permute-start | bytes 1572872 | tf_op jit(solution)/shard_map/ppermute | solution.py:185
  127.9 0.9 copy-start.7
  129.7 0.8 copy-start.3
  130.6 0.7 copy-start.5
  131.3 12.6 %all-to-all-start.2 = ((bf16[4,32,2048]{2,1,0:T(8,128)(2,1)}), bf16[4,32,2048]{2,1,0:T(8,128)(2,1)S(1)}, u32[]{:S(2)}, u32[]{:S(2)}) async-start(bf16[4,32,2048]{2,1,0:T(8,128)(2,1)} %copy-done.3), calls=%async_computation.2 | async-start | bytes 1048576 | tf_op jit(solution)/shard_map/all_to_all | solution.py:227
  137.3 14.8 %collective-permute-start.21 = (bf16[256,1024]{1,0:T(8,128)(2,1)}, bf16[256,1024]{1,0:T(8,128)(2,1)}, u32[]{:S(2)}, u32[]{:S(2)}) collective-permute-start(bf16[256,1024]{1,0:T(8,128)(2,1)} %collective-permute-done.20.rest_6_), channel_id=1, source_target_pairs={{0,480},{32,0},{64,32},{96,64},{128,96},{160,128},{192,160},{224,1... | collective-permute-start | bytes 1572872 | tf_op jit(solution)/shard_map/ppermute | solution.py:185
  142.0 15.2 %collective-permute-start.18 = (bf16[256,1024]{1,0:T(8,128)(2,1)}, bf16[256,1024]{1,0:T(8,128)(2,1)}, u32[]{:S(2)}, u32[]{:S(2)}) collective-permute-start(bf16[256,1024]{1,0:T(8,128)(2,1)} %collective-permute-done.17.rest_3_), channel_id=1, source_target_pairs={{0,32},{32,64},{64,96},{96,128},{128,160},{160,192},{192,224},{224... | collective-permute-start | bytes 1572872 | tf_op jit(solution)/shard_map/ppermute | solution.py:185
  143.9 13.2 %collective-permute-start.14 = (bf16[128,2048]{1,0:T(8,128)(2,1)S(1)}, bf16[128,2048]{1,0:T(8,128)(2,1)S(1)}, u32[]{:S(2)}, u32[]{:S(2)}) collective-permute-start(bf16[128,2048]{1,0:T(8,128)(2,1)S(1)} %bitcast.35), channel_id=1, source_target_pairs={{0,1},{1,0},{2,3},{3,2},{4,5},{5,4},{6,7},{7,6},{8,9},{9,8},{10,11... | collective-permute-start | bytes 1572872 | tf_op jit(solution)/shard_map/ppermute | solution.py:223
  161.2 6.0 %collective-permute-start.22 = (bf16[128,2048]{1,0:T(8,128)(2,1)S(1)}, bf16[128,2048]{1,0:T(8,128)(2,1)S(1)}, u32[]{:S(2)}, u32[]{:S(2)}) collective-permute-start(bf16[128,2048]{1,0:T(8,128)(2,1)S(1)} %get-tuple-element.31), channel_id=1, source_target_pairs={{0,1},{1,0},{2,3},{3,2},{4,5},{5,4},{6,7},{7,6},{8,9},{9,8},{10,11... | collective-permute-start | bytes 1572872 | tf_op jit(solution)/shard_map/ppermute | solution.py:223
  167.3 12.6 %copy-start.6 = (f32[32,2048]{1,0:T(8,128)S(1)}, f32[32,2048]{1,0:T(8,128)}, u32[]{:S(2)}) copy-start(f32[32,2048]{1,0:T(8,128)} %copy-done.5) | copy-start | bytes 786436
  180.8 16.4 %copy-start.2 = (bf16[3,64,1152]{2,1,0:T(8,128)(2,1)S(1)}, bf16[3,64,1152]{2,1,0:T(8,128)(2,1)}, u32[]{:S(2)}) copy-start(bf16[3,64,1152]{2,1,0:T(8,128)(2,1)} %copy-done) | copy-start | bytes 1327108
  191.1 6.1 %collective-permute-start.23 = (bf16[128,2048]{1,0:T(8,128)(2,1)S(1)}, bf16[128,2048]{1,0:T(8,128)(2,1)S(1)}, u32[]{:S(2)}, u32[]{:S(2)}) collective-permute-start(bf16[128,2048]{1,0:T(8,128)(2,1)S(1)} %bitcast.37), channel_id=1, source_target_pairs={{0,1},{1,0},{2,3},{3,2},{4,5},{5,4},{6,7},{7,6},{8,9},{9,8},{10,11... | collective-permute-start | bytes 1572872 | tf_op jit(solution)/shard_map/ppermute | solution.py:223
  200.7 3.8 %collective-permute-start.24 = (bf16[128,2048]{1,0:T(8,128)(2,1)S(1)}, bf16[128,2048]{1,0:T(8,128)(2,1)S(1)}, u32[]{:S(2)}, u32[]{:S(2)}) collective-permute-start(bf16[128,2048]{1,0:T(8,128)(2,1)S(1)} %get-tuple-element.35), channel_id=1, source_target_pairs={{0,1},{1,0},{2,3},{3,2},{4,5},{5,4},{6,7},{7,6},{8,9},{9,8},{10,11... | collective-permute-start | bytes 1572872 | tf_op jit(solution)/shard_map/ppermute | solution.py:223

commit v5 on v4

--- a/solution.py
+++ b/solution.py
@@ -14,8 +14,6 @@
 NZ, NY, NX = 8, 4, 4
 ROWS = 32
 VMEM = pl.BlockSpec(memory_space=pltpu.VMEM)
-SMEM = pl.BlockSpec(memory_space=pltpu.SMEM)
-ANY = pl.BlockSpec(memory_space=pl.ANY)
 
 
 def dot(a, b):
@@ -91,7 +89,7 @@
     return low(stream * scale * gain)
 
 
-def pack_kernel(place, gate, up, down, ds, query, key, value, out, os, tokens, gains, *rest):
+def pack_kernel(gate, up, down, ds, query, key, value, out, os, tokens, gains, *rest):
     small, (ffn_ref, mix_ref, rows_ref, small_ref, stream_ref, gains_ref) = rest[:-6], rest[-6:]
 
     def column(row):
@@ -111,7 +109,7 @@
     for k in range(NY):
         for i, w in enumerate(mix):
             mix_ref[k, :, i * DK : (i + 1) * DK] = w
-    z, y = place[0], place[1]
+    z, y = lax.axis_index("z"), lax.axis_index("y")
     stream = shuffled(turned(tokens, z, y), PLAIN_TO_FFN)
     ordered = shuffled(turned(gains, z, y), PLAIN_TO_FFN)
     stream_ref[...] = low(stream)
@@ -121,10 +119,11 @@
         rows_ref[k] = first
     for i, v in enumerate(small):
         for k in range(v.shape[0]):
-            small_ref[i : i + 1, k * 128 : k * 128 + 128] = v[k : k + 1, :]
-
-
-def pack(place, gate, up, down, ds, query, key, value, out, os, tokens, gains, small):
+            row = jnp.broadcast_to(v[k : k + 1, :], (1, 128))
+            small_ref[i : i + 1, k * 128 : k * 128 + 128] = row
+
+
+def pack(gate, up, down, ds, query, key, value, out, os, tokens, gains, small):
     rows, n = gate.shape
     return pl.pallas_call(
         pack_kernel,
@@ -136,21 +135,21 @@
             jax.ShapeDtypeStruct(tokens.shape, jnp.bfloat16),
             jax.ShapeDtypeStruct(gains.shape, jnp.float32),
         ),
-        in_specs=[SMEM] + [VMEM] * (11 + len(small)),
+        in_specs=[VMEM] * (11 + len(small)),
         out_specs=(VMEM,) * 6,
         name="pack",
-    )(place, gate, up, down, ds, query, key, value, out, os, tokens, gains, *small)
-
-
-def join_kernel(weight, which, arrived_as, rows_as, place, arrived, stream, gains, next_ref, last_ref):
+    )(gate, up, down, ds, query, key, value, out, os, tokens, gains, *small)
+
+
+def join_kernel(weight, which, arrived_as, rows_as, arrived, stream, gains, next_ref, last_ref):
     total = arrived[0].astype(jnp.float32)
     for k in range(1, NX):
         total = total + arrived[k].astype(jnp.float32)
     if arrived_as is not None:
-        total = shuffled(turned_in_place(total, place[1]), arrived_as)
+        total = shuffled(turned_in_place(total, lax.axis_index("y")), arrived_as)
     total = stream[...].astype(jnp.float32) + weight * total
     if which is None:
-        z, y = place[0], place[1]
+        z, y = lax.axis_index("z"), lax.axis_index("y")
         last_ref[...] = shuffled(total, FFN_TO_PLAIN)
         next_ref[...] = low(turned(last_ref, NZ - z, NY - y))
         return
@@ -158,13 +157,13 @@
     rows = total * lax.rsqrt(jnp.mean(total * total, axis=-1, keepdims=True) + EPSILON)
     rows = rows * gains[which : which + 1, :]
     if rows_as is not None:
-        rows = turned_in_place(shuffled(rows, rows_as), NY - place[1])
+        rows = turned_in_place(shuffled(rows, rows_as), NY - lax.axis_index("y"))
     rows = low(rows)
     for k in range(NX):
         last_ref[k] = rows
 
 
-def join(place, weight, which, arrived, stream, gains, arrived_as=None, rows_as=None):
+def join(weight, which, arrived, stream, gains, arrived_as=None, rows_as=None):
     shape = stream.shape
     last = which is None
     outs = [jax.ShapeDtypeStruct(shape, jnp.bfloat16 if last else jnp.float32)]
@@ -173,12 +172,12 @@
     return pl.pallas_call(
         lambda *refs: join_kernel(weight, which, arrived_as, rows_as, *refs),
         out_shape=outs,
-        in_specs=[SMEM] + [VMEM] * 3,
+        in_specs=[VMEM] * 3,
         out_specs=[VMEM] * len(outs),
         scratch_shapes=[pltpu.VMEM(shape, jnp.float32)] if last else [],
         compiler_params=pltpu.CompilerParams(vmem_limit_bytes=8 * 1024 * 1024),
         name="join",
-    )(place, arrived, stream, gains)
+    )(arrived, stream, gains)
 
 
 def along_z(array, step):
@@ -208,15 +207,35 @@
     return arrays
 
 
+def pick_kernel(first, second, out):
+    @pl.when(lax.axis_index("core") == 0)
+    def _():
+        out[...] = first[...]
+
+    @pl.when(lax.axis_index("core") != 0)
+    def _():
+        out[...] = second[...]
+
+
 def gather_mix(copies):
     mine = lax.all_to_all(copies, "y", split_axis=0, concat_axis=0, tiled=True)
     mine = mine.reshape(-1, copies.shape[2])
-    up, down = [mine], [mine]
-    for k in range(4):
-        up.append(along_z(up[-1], 1))
-        if k < 3:
-            down.append(along_z(down[-1], -1))
-    return up + down[1:]
+
+    u1, d1 = along_z(mine, 1), along_z(mine, -1)
+    u2, d2 = along_z(u1, 1), along_z(d1, -1)
+    d3, u3 = along_z(d1, -2), along_z(u2, 1)
+    last = pl.pallas_call(
+        pick_kernel,
+        out_shape=jax.ShapeDtypeStruct(mine.shape, mine.dtype),
+        in_specs=[VMEM, VMEM],
+        out_specs=VMEM,
+        compiler_params=pltpu.CompilerParams(vmem_limit_bytes=4 * 1024 * 1024),
+        name="pick",
+    )(u3, d3)
+    ring = 2 * NZ
+    pairs = [(2 * g + c, 2 * ((g + 1 - 2 * c) % ring) + c) for g in range(ring) for c in (0, 1)]
+    last = lax.ppermute(last, ("rep", "z", "core"), pairs)
+    return [mine, u1, u2, u3, last, d1, d2, d3]
 
 
 def swap_cores(array):
@@ -240,10 +259,10 @@
     return jnp.concatenate([a[..., first:last].reshape(-1, last - first) for a in arrays], axis=0)
 
 
-def ffn_kernel(spans, place, small, *rest):
+def ffn_kernel(spans, small, *rest):
     row_refs, arrays, (own_ref, other_ref) = rest[:spans], rest[spans:-2], rest[-2:]
     units = arrays[0].shape[-1] // 3
-    core = place[2]
+    core = lax.axis_index("core")
     if spans == 1:
         every = row_refs[0]
         sides = [core, 1 - core]
@@ -259,7 +278,7 @@
     other_ref[...] = low(part[half:])
 
 
-def feed_forward(place, small, row_arrays, arrays):
+def feed_forward(small, row_arrays, arrays):
     wide = row_arrays[0].shape[-1]
     rows = NX * ROWS
     own_part, other_part = pl.pallas_call(
@@ -268,17 +287,17 @@
             jax.ShapeDtypeStruct((rows, wide), jnp.float32),
             jax.ShapeDtypeStruct((rows, wide), jnp.bfloat16),
         ),
-        in_specs=[SMEM, VMEM] + [VMEM] * len(row_arrays) + [VMEM] * len(arrays),
+        in_specs=[VMEM] + [VMEM] * len(row_arrays) + [VMEM] * len(arrays),
         out_specs=(VMEM, VMEM),
         compiler_params=pltpu.CompilerParams(vmem_limit_bytes=24 * 1024 * 1024),
         name="ffn",
-    )(place, small, *row_arrays, *arrays)
+    )(small, *row_arrays, *arrays)
     return return_rows(own_part, other_part)
 
 
-def mix_kernel(place, rate, small, own_rows, other_rows, *rest):
+def mix_kernel(small, own_rows, other_rows, *rest):
     arrays, (own_ref, other_ref) = rest[:-2], rest[-2:]
-    core = place[2]
+    core = lax.axis_index("core")
     rows = jnp.concatenate([own_rows[...], other_rows[...]], axis=0)
     query = low(dot(rows, stacked(arrays, 0, DK)) * small[2:3, :DK])
     key_rows = low(dot(rows, stacked(arrays, DK, 2 * DK)) * small[3:4, :DK] / math.sqrt(DK))
@@ -294,7 +313,7 @@
 
     pi, pj = position(0), position(1)
     apart = jnp.abs(pi - pj).astype(jnp.float32)
-    decay = jnp.where(pj // BLOCK <= pi // BLOCK, jnp.exp(-rate[0] * apart), 0.0)
+    decay = jnp.where(pj // BLOCK <= pi // BLOCK, jnp.exp(-small[6:7, :1] * apart), 0.0)
     scores = low(dot_t(query, key_rows) * decay)
     retained = dot(scores, value)
     centred = retained - jnp.mean(retained, axis=-1, keepdims=True)
@@ -306,7 +325,7 @@
     other_ref[...] = low(part[half:])
 
 
-def mix(place, rate, small, own, other, arrays):
+def mix(small, own, other, arrays):
     rows, wide = own.shape
     own_part, other_part = pl.pallas_call(
         mix_kernel,
@@ -314,11 +333,11 @@
             jax.ShapeDtypeStruct((rows, wide), jnp.float32),
             jax.ShapeDtypeStruct((rows, wide), jnp.bfloat16),
         ),
-        in_specs=[SMEM, SMEM] + [VMEM] * (3 + len(arrays)),
+        in_specs=[VMEM] * (3 + len(arrays)),
         out_specs=(VMEM, VMEM),
         compiler_params=pltpu.CompilerParams(vmem_limit_bytes=24 * 1024 * 1024),
         name="mix",
-    )(place, rate, small, own, other, *arrays)
+    )(small, own, other, *arrays)
     return return_rows(own_part, other_part)
 
 
@@ -330,24 +349,24 @@
     def row(v):
         return v.reshape(1, -1)
 
-    place = jnp.stack([lax.axis_index(a).astype(jnp.int32) for a in ("z", "y", "core")])
     ffn_mine, mix_mine, copies, small, stream, gains = pack(
-        place, gate_w, up_w, down_w.T, row(down_scale), query_w, key_w, value_w, out_w.T,
+        gate_w, up_w, down_w.T, row(down_scale), query_w, key_w, value_w, out_w.T,
         row(out_scale), tokens_in, norm_gains,
-        [v.reshape(-1, 128) for v in (gate_scale, up_scale, query_scale, key_scale, value_scale, head_gain)],
+        [v.reshape(-1, 128) for v in (gate_scale, up_scale, query_scale, key_scale, value_scale, head_gain)]
+        + [row(decay_rate)],
     )
     ffn_arrays = gather_ffn(ffn_mine)
     every = lax.all_to_all(copies, ("x", "core"), split_axis=0, concat_axis=0, tiled=True)
     mix_arrays = gather_mix(mix_mine)
 
-    arrived = feed_forward(place, small, [every], ffn_arrays)
-    stream, copies = join(place, 0.5, 1, arrived, stream, gains, rows_as=FFN_TO_MIX)
+    arrived = feed_forward(small, [every], ffn_arrays)
+    stream, copies = join(0.5, 1, arrived, stream, gains, rows_as=FFN_TO_MIX)
     own, other = gather_rows(copies)
-    arrived = mix(place, decay_rate, small, own, other, mix_arrays)
-    stream, copies = join(place, 1.0, 2, arrived, stream, gains, arrived_as=MIX_TO_FFN)
+    arrived = mix(small, own, other, mix_arrays)
+    stream, copies = join(1.0, 2, arrived, stream, gains, arrived_as=MIX_TO_FFN)
     rows = gather_rows(copies)
-    arrived = feed_forward(place, small, rows, ffn_arrays)
-    return join(place, 0.5, None, arrived, stream, gains)[0]
+    arrived = feed_forward(small, rows, ffn_arrays)
+    return join(0.5, None, arrived, stream, gains)[0]
 
 
 def solution(mesh):

time: 219 us -> 227 us (1.037)
  starting transfers between devices: 106 us -> 111 us
  waiting for transfers between devices: 48 us -> 50.5 us
    ppermute x0 -> x1, starting transfers between devices: none -> 12.8 us  [gather_mix(): last = lax.ppermute(last, ('rep', 'z', 'core'), pairs)]
    ppermute x0 -> x1, waiting for transfers between devices: none -> 5.68 us  [gather_mix(): last = lax.ppermute(last, ('rep', 'z', 'core'), pairs)]
    ppermute x5, starting transfers between devices: 19.5 us -> 14.6 us  [swap_cores(): return lax.ppermute(array, 'core', [(0, 1), (1, 0)])]
    ppermute x14 -> x13, waiting for transfers between devices: 24.1 us -> 20.4 us  [along_z(): lax.ppermute(array, ('rep', 'z'), [(g, (g + step) % (2 * NZ)) for g in ra...]
    ppermute x14 -> x13, starting transfers between devices: 47.5 us -> 44.1 us  [along_z(): lax.ppermute(array, ('rep', 'z'), [(g, (g + step) % (2 * NZ)) for g in ra...]
    unnamed x32 -> x30, local copies, waits for them, and re-layouts: 7.69 us -> 7.69 us
  transfers between devices with their start and end apart: 29 -> 29, of which waited for: 13 -> 13; matrix products, arithmetic and copies ran while one was open for 2% -> 2% of each run, Pallas kernels for 2% -> 3%
where the time goes in v5:
time: 227 us; the launch traced here: 226 us
  starting transfers between devices  111 us (49%)
  waiting for transfers between devices  50.5 us (22%)
  blocking collectives  35.5 us (16%)
  Pallas kernels  17.4 us (8%)
  local copies, waits for them, and re-layouts  7.71 us (3%)
    ppermute x13, starting transfers between devices, along_z(): lax.ppermute(array, ('rep', 'z'), [(g, (g + step) % (2 * NZ)) for g in ra...  44.1 us
    all_to_all x2, blocking collectives, return_rows(): return lax.all_to_all(blocks, 'x', split_axis=0, concat_axis=0, tiled=True)  24.7 us
    ppermute x13, waiting for transfers between devices, along_z(): lax.ppermute(array, ('rep', 'z'), [(g, (g + step) % (2 * NZ)) for g in ra...  20.4 us
    ppermute x6, waiting for transfers between devices, along_y(): return lax.ppermute(array, 'y', [(g, (g + step) % NY) for g in range(NY)])  19.4 us
    ppermute x6, starting transfers between devices, along_y(): return lax.ppermute(array, 'y', [(g, (g + step) % NY) for g in range(NY)])  18.5 us
    ppermute x5, starting transfers between devices, swap_cores(): return lax.ppermute(array, 'core', [(0, 1), (1, 0)])  14.6 us
    ppermute x1, starting transfers between devices, gather_mix(): last = lax.ppermute(last, ('rep', 'z', 'core'), pairs)  12.8 us
    all_to_all x1, blocking collectives, gather_rows(): own = lax.all_to_all(copies, 'x', split_axis=0, concat_axis=0, tiled=True)  10.8 us
  transfers between devices with their start and end apart: 29, of which 13 were waited for; matrix products, arithmetic and copies ran while one was open for 2% of the time, Pallas kernels for 3%

profile of v5, /device:TPU:1, one launch (start us, length us, event | category | flops | bytes accessed | tf_op | source)
XLA Modules:
  0.0 225.6 jit_solution(4852008844884029383)
XLA Ops:
  0.7 2.9 %pack.1 = (bf16[64,1152]{1,0:T(8,128)(2,1)}, bf16[4,64,1024]{2,1,0:T(8,128)(2,1)}, bf16[8,32,2048]{2,1,0:T(8,128)(2,1)}, f32[8,384]{1,0:T(8,128)}, bf16[32,2048]{1,0:T(8,128)(2,1)}, /*index=5*/f32[3,2048]{1,0:T(4,128)}) custom-call(f32[64,384]{1,0:T(8,128)} %gate.1, f32[64,384]{1,0:T(8,128)} %up.1, f32[64,384]{1,0:T(8,128)} %bitcast.41, f32[1,64]{1,0:T(1,128)} %bitcast.49, ...), custom_call_target="tpu_custom_call" | custom-call | tf_op jit(solution)/shard_map/pack/pallas_call | solution.py:128
  3.5 11.9 %collective-permute-start.1 = (bf16[64,1152]{1,0:T(8,128)(2,1)}, bf16[64,1152]{1,0:T(8,128)(2,1)}, u32[]{:S(2)}, u32[]{:S(2)}) collective-permute-start(bf16[64,1152]{1,0:T(8,128)(2,1)} %get-tuple-element.23), channel_id=1, source_target_pairs={{0,480},{32,0},{64,32},{96,64},{128,96},{160,128},{192,160},{224,1... | collective-permute-start | bytes 442376 | tf_op jit(solution)/shard_map/ppermute | solution.py:184
  15.5 1.9 collective-permute-start
  17.4 4.3 %all-to-all-start.3 = ((bf16[4,64,1024]{2,1,0:T(8,128)(2,1)}), bf16[4,64,1024]{2,1,0:T(8,128)(2,1)S(1)}, u32[]{:S(2)}, u32[]{:S(2)}) async-start(bf16[4,64,1024]{2,1,0:T(8,128)(2,1)} %get-tuple-element.29), calls=%async_computation.3 | async-start | bytes 1048576 | tf_op jit(solution)/shard_map/all_to_all | solution.py:221
  21.8 4.6 %collective-permute-start.3 = (bf16[64,1152]{1,0:T(8,128)(2,1)}, bf16[64,1152]{1,0:T(8,128)(2,1)S(1)}, u32[]{:S(2)}, u32[]{:S(2)}) collective-permute-start(bf16[64,1152]{1,0:T(8,128)(2,1)} %collective-permute-done.1), channel_id=1, source_target_pairs={{0,480},{32,0},{64,32},{96,64},{128,96},{160,128},{192,160},{224,1... | collective-permute-start | bytes 442376 | tf_op jit(solution)/shard_map/ppermute | solution.py:184
  26.4 1.9 collective-permute-start.2
  30.2 3.6 %collective-permute-done.2 = bf16[64,1152]{1,0:T(8,128)(2,1)} collective-permute-done((bf16[64,1152]{1,0:T(8,128)(2,1)}, bf16[64,1152]{1,0:T(8,128)(2,1)}, u32[]{:S(2)}, u32[]{:S(2)}) %collective-permute-start.2) | collective-permute-done | bytes 147488 | tf_op jit(solution)/shard_map/ppermute | solution.py:184
  34.8 3.4 %collective-permute-start.4 = (bf16[5,64,1152]{2,1,0:T(8,128)(2,1)S(1)}, bf16[5,64,1152]{2,1,0:T(8,128)(2,1)S(1)}, u32[]{:S(2)}, u32[]{:S(2)}) collective-permute-start(bf16[5,64,1152]{2,1,0:T(8,128)(2,1)S(1)} %bitcast_dynamic-update-slice_fusion.refs_2_.refs_3_), channel_id=1, source_target_pairs={{0,8},{8,16},{16,24},{24,0},{1,9},{9,17},{17,25},{25,1},{2,10},{10... | collective-permute-start | bytes 2211848 | tf_op jit(solution)/shard_map/ppermute | solution.py:188
  38.1 1.9 collective-permute-start.8
  40.1 4.3 %collective-permute-start.7 = (bf16[64,1152]{1,0:T(8,128)(2,1)}, bf16[64,1152]{1,0:T(8,128)(2,1)S(1)}, u32[]{:S(2)}, u32[]{:S(2)}) collective-permute-start(bf16[64,1152]{1,0:T(8,128)(2,1)} %collective-permute-done), channel_id=1, source_target_pairs={{0,64},{32,96},{64,128},{96,160},{128,192},{160,224},{192,256},{22... | collective-permute-start | bytes 442376 | tf_op jit(solution)/shard_map/ppermute | solution.py:184
  44.3 1.9 collective-permute-start.9
  46.3 8.4 %all-to-all-start = ((bf16[8,32,2048]{2,1,0:T(8,128)(2,1)}), bf16[8,32,2048]{2,1,0:T(8,128)(2,1)S(1)}, u32[]{:S(2)}, u32[]{:S(2)}) async-start(bf16[8,32,2048]{2,1,0:T(8,128)(2,1)} %get-tuple-element.22), calls=%async_computation | async-start | bytes 2097152 | tf_op jit(solution)/shard_map/all_to_all | solution.py:359
  54.7 4.4 %collective-permute-done.9 = bf16[64,1152]{1,0:T(8,128)(2,1)S(1)} collective-permute-done((bf16[64,1152]{1,0:T(8,128)(2,1)}, bf16[64,1152]{1,0:T(8,128)(2,1)S(1)}, u32[]{:S(2)}, u32[]{:S(2)}) %collective-permute-start.9) | collective-permute-done | bytes 147488 | tf_op jit(solution)/shard_map/ppermute | solution.py:184
  60.9 3.1 %collective-permute-start.11 = (bf16[3,64,1152]{2,1,0:T(8,128)(2,1)S(1)}, bf16[3,64,1152]{2,1,0:T(8,128)(2,1)}, u32[]{:S(2)}, u32[]{:S(2)}) collective-permute-start(bf16[3,64,1152]{2,1,0:T(8,128)(2,1)S(1)} %pad_maximum_fusion.refs_6_.refs_7_), channel_id=1, source_target_pairs={{0,24},{8,0},{16,8},{24,16},{1,25},{9,1},{17,9},{25,17},{2,26},{10... | collective-permute-start | bytes 1327112 | tf_op jit(solution)/shard_map/ppermute | solution.py:188
  64.0 3.4 %collective-permute-start.5 = (bf16[5,64,1152]{2,1,0:T(8,128)(2,1)S(1)}, bf16[5,64,1152]{2,1,0:T(8,128)(2,1)}, u32[]{:S(2)}, u32[]{:S(2)}) collective-permute-start(bf16[5,64,1152]{2,1,0:T(8,128)(2,1)S(1)} %bitcast_dynamic-update-slice_fusion.refs_2_.refs_3_), channel_id=1, source_target_pairs={{0,24},{8,0},{16,8},{24,16},{1,25},{9,1},{17,9},{25,17},{2,26},{10... | collective-permute-start | bytes 2211848 | tf_op jit(solution)/shard_map/ppermute | solution.py:188
  67.4 1.9 collective-permute-start.6
  69.3 2.2 collective-permute-start.10
  72.9 4.6 %collective-permute-start.12 = (bf16[3,64,1152]{2,1,0:T(8,128)(2,1)}, bf16[3,64,1152]{2,1,0:T(8,128)(2,1)}, u32[]{:S(2)}, u32[]{:S(2)}) collective-permute-start(bf16[3,64,1152]{2,1,0:T(8,128)(2,1)} %collective-permute-done.11.refs_8_.refs_9_), channel_id=1, source_target_pairs={{0,24},{8,0},{16,8},{24,16},{1,25},{9,1},{17,9},{25,17},{2,26},{10... | collective-permute-start | bytes 1327112 | tf_op jit(solution)/shard_map/ppermute | solution.py:188
  77.5 1.9 collective-permute-start.15
  79.4 16.4 %collective-permute-done.10.refs_7_.refs_8_ = bf16[3,64,1152]{2,1,0:T(8,128)(2,1)S(1)} collective-permute-done((bf16[3,64,1152]{2,1,0:T(8,128)(2,1)S(1)}, bf16[3,64,1152]{2,1,0:T(8,128)(2,1)S(1)}, u32[]{:S(2)}, u32[]{:S(2)}) %collective-permute-start.10) | collective-permute-done | bytes 442400 | tf_op jit(solution)/shard_map/ppermute | solution.py:188
  96.5 1.6 collective-permute-done.12.refs_9_.refs_10_
  99.2 3.5 %ffn.2 = (f32[128,2048]{1,0:T(8,128)S(1)}, bf16[128,2048]{1,0:T(8,128)(2,1)S(1)}) custom-call(f32[8,384]{1,0:T(8,128)S(1)} %copy-done.8, bf16[8,32,2048]{2,1,0:T(8,128)(2,1)S(1)} %all-to-all-done.refs_1_, bf16[5,64,1152]{2,1,0:T(8,128)(2,1)S(1)} %bitcast_dynamic-update-slice_fusion.refs_2_.refs_3_, ...), custom_call_target="tpu_custom_call" | custom-call | tf_op jit(solution)/shard_map/ffn/pallas_call | solution.py:284
  102.7 4.5 %collective-permute-start.13 = (bf16[128,2048]{1,0:T(8,128)(2,1)S(1)}, bf16[128,2048]{1,0:T(8,128)(2,1)S(1)}, u32[]{:S(2)}, u32[]{:S(2)}) collective-permute-start(bf16[128,2048]{1,0:T(8,128)(2,1)S(1)} %get-tuple-element.25), channel_id=1, source_target_pairs={{0,1},{1,0},{2,3},{3,2},{4,5},{5,4},{6,7},{7,6},{8,9},{9,8},{10,11... | collective-permute-start | bytes 1572872 | tf_op jit(solution)/shard_map/ppermute | solution.py:242
  107.1 1.9 collective-permute-start.18
  109.1 3.4 %collective-permute-start.16 = (bf16[256,1024]{1,0:T(8,128)(2,1)}, bf16[256,1024]{1,0:T(8,128)(2,1)}, u32[]{:S(2)}, u32[]{:S(2)}) collective-permute-start(bf16[256,1024]{1,0:T(8,128)(2,1)} %collective-permute-done.15.rest_1_), channel_id=1, source_target_pairs={{0,32},{32,64},{64,96},{96,128},{128,160},{160,192},{192,224},{224... | collective-permute-start | bytes 1572872 | tf_op jit(solution)/shard_map/ppermute | solution.py:184
  113.4 4.3 %all-to-all-start.1 = ((bf16[4,32,2048]{2,1,0:T(8,128)(2,1)}), bf16[4,32,2048]{2,1,0:T(8,128)(2,1)}, u32[]{:S(2)}, u32[]{:S(2)}) async-start(bf16[4,32,2048]{2,1,0:T(8,128)(2,1)} %bitcast.19), calls=%async_computation.1 | async-start | bytes 1048576 | tf_op jit(solution)/shard_map/all_to_all | solution.py:255
  117.6 5.0 %collective-permute-done.18.rest_5_ = bf16[256,1024]{1,0:T(8,128)(2,1)} collective-permute-done((bf16[256,1024]{1,0:T(8,128)(2,1)S(1)}, bf16[256,1024]{1,0:T(8,128)(2,1)}, u32[]{:S(2)}, u32[]{:S(2)}) %collective-permute-start.18) | collective-permute-done | bytes 524320 | tf_op jit(solution)/shard_map/ppermute | solution.py:184
  122.6 1.9 collective-permute-start.19
  124.5 1.4 collective-permute-done.16.rest_2_
  126.0 3.1 %collective-permute-start.17 = (bf16[256,1024]{1,0:T(8,128)(2,1)}, bf16[256,1024]{1,0:T(8,128)(2,1)S(1)}, u32[]{:S(2)}, u32[]{:S(2)}) collective-permute-start(bf16[256,1024]{1,0:T(8,128)(2,1)} %collective-permute-done.16.rest_2_), channel_id=1, source_target_pairs={{0,32},{32,64},{64,96},{96,128},{128,160},{160,192},{192,224},{224... | collective-permute-start | bytes 1572872 | tf_op jit(solution)/shard_map/ppermute | solution.py:184
  133.0 4.1 %all-to-all-start.2 = ((bf16[4,32,2048]{2,1,0:T(8,128)(2,1)}), bf16[4,32,2048]{2,1,0:T(8,128)(2,1)}, u32[]{:S(2)}, u32[]{:S(2)}) async-start(bf16[4,32,2048]{2,1,0:T(8,128)(2,1)} %copy-done.3), calls=%async_computation.2 | async-start | bytes 1048576 | tf_op jit(solution)/shard_map/all_to_all | solution.py:246
  137.2 3.3 %collective-permute-start.21 = (bf16[256,1024]{1,0:T(8,128)(2,1)}, bf16[256,1024]{1,0:T(8,128)(2,1)}, u32[]{:S(2)}, u32[]{:S(2)}) collective-permute-start(bf16[256,1024]{1,0:T(8,128)(2,1)} %collective-permute-done.18.rest_5_), channel_id=1, source_target_pairs={{0,480},{32,0},{64,32},{96,64},{128,96},{160,128},{192,160},{224,1... | collective-permute-start | bytes 1572872 | tf_op jit(solution)/shard_map/ppermute | solution.py:184
  140.5 1.7 collective-permute-done.19.second.rest_7_
  143.1 12.8 %collective-permute-start.20 = (bf16[256,1024]{1,0:T(8,128)(2,1)}, bf16[256,1024]{1,0:T(8,128)(2,1)}, u32[]{:S(2)}, u32[]{:S(2)}) collective-permute-start(bf16[256,1024]{1,0:T(8,128)(2,1)} %pick.1), channel_id=1, source_target_pairs={{0,32},{1,481},{32,64},{33,1},{64,96},{65,33},{96,128},{97,65},{12... | collective-permute-start | bytes 1572872 | tf_op jit(solution)/shard_map/ppermute | solution.py:237
  155.9 1.9 collective-permute-start.14
  157.8 4.3 %collective-permute-done.21.rest_6_ = bf16[256,1024]{1,0:T(8,128)(2,1)} collective-permute-done((bf16[256,1024]{1,0:T(8,128)(2,1)}, bf16[256,1024]{1,0:T(8,128)(2,1)}, u32[]{:S(2)}, u32[]{:S(2)}) %collective-permute-start.21) | collective-permute-done | bytes 524320 | tf_op jit(solution)/shard_map/ppermute | solution.py:184
  162.1 5.7 %collective-permute-done.20.rest_4_ = bf16[256,1024]{1,0:T(8,128)(2,1)} collective-permute-done((bf16[256,1024]{1,0:T(8,128)(2,1)}, bf16[256,1024]{1,0:T(8,128)(2,1)}, u32[]{:S(2)}, u32[]{:S(2)}) %collective-permute-start.20) | collective-permute-done | bytes 524320 | tf_op jit(solution)/shard_map/ppermute | solution.py:237
  167.8 4.1 %mix.1 = (f32[128,2048]{1,0:T(8,128)S(1)}, bf16[128,2048]{1,0:T(8,128)(2,1)S(1)}) custom-call(f32[8,384]{1,0:T(8,128)S(1)} %copy-done.8, bf16[128,2048]{1,0:T(8,128)(2,1)} %bitcast.20.own_rows, bf16[128,2048]{1,0:T(8,128)(2,1)S(1)} %collective-permute-done.14.other_rows, bf16[256,1024]{1,0:T(8,128)(2,1)S(1)} %bitcast.33, ...), custom_call_target="tpu_custom_call" | custom-call | tf_op jit(solution)/shard_map/mix/pallas_call | solution.py:330
  171.9 1.9 collective-permute-start.22
  173.8 1.9 collective-permute-done.22
  175.8 13.1 %all_to_all.35.refs_0_ = bf16[4,32,2048]{2,1,0:T(8,128)(2,1)S(1)} all-to-all(bf16[4,32,2048]{2,1,0:T(8,128)(2,1)S(1)} %bitcast.36), channel_id=1, replica_groups=mesh['rep'=2,'z'=8,'y'=4,'x'=4,'core'=2] {'x'}, dimensions={0} | all-to-all | bytes 1048576 | tf_op jit(solution)/shard_map/all_to_all | solution.py:255
  189.2 10.8 %all_to_all.36 = bf16[4,32,2048]{2,1,0:T(8,128)(2,1)S(1)} all-to-all(bf16[4,32,2048]{2,1,0:T(8,128)(2,1)S(1)} %get-tuple-element.33), channel_id=1, replica_groups=mesh['rep'=2,'z'=8,'y'=4,'x'=4,'core'=2] {'x'}, dimensions={0} | all-to-all | bytes 1048576 | tf_op jit(solution)/shard_map/all_to_all | solution.py:246
  200.1 4.0 %collective-permute-start.23 = (bf16[128,2048]{1,0:T(8,128)(2,1)S(1)}, bf16[128,2048]{1,0:T(8,128)(2,1)S(1)}, u32[]{:S(2)}, u32[]{:S(2)}) collective-permute-start(bf16[128,2048]{1,0:T(8,128)(2,1)S(1)} %bitcast.34), channel_id=1, source_target_pairs={{0,1},{1,0},{2,3},{3,2},{4,5},{5,4},{6,7},{7,6},{8,9},{9,8},{10,11... | collective-permute-start | bytes 1572872 | tf_op jit(solution)/shard_map/ppermute | solution.py:242
  204.1 1.5 collective-permute-done.23.refs_2_
  205.6 3.5 %ffn.3 = (f32[128,2048]{1,0:T(8,128)S(1)}, bf16[128,2048]{1,0:T(8,128)(2,1)S(1)}) custom-call(f32[8,384]{1,0:T(8,128)S(1)} %copy-done.8, bf16[128,2048]{1,0:T(8,128)(2,1)S(1)} %bitcast.35, bf16[128,2048]{1,0:T(8,128)(2,1)S(1)} %collective-permute-done.23.refs_2_, bf16[5,64,1152]{2,1,0:T(8,128)(2,1)S(1)} %bitcast_dynamic-update-slice_fusion.refs_2_.refs_3_, ...), custom_call_target="tpu_custom_call" | custom-call | tf_op jit(solution)/shard_map/ffn/pallas_call | solution.py:284
  209.1 2.3 %collective-permute-start.24 = (bf16[128,2048]{1,0:T(8,128)(2,1)S(1)}, bf16[128,2048]{1,0:T(8,128)(2,1)S(1)}, u32[]{:S(2)}, u32[]{:S(2)}) collective-permute-start(bf16[128,2048]{1,0:T(8,128)(2,1)S(1)} %get-tuple-element.35), channel_id=1, source_target_pairs={{0,1},{1,0},{2,3},{3,2},{4,5},{5,4},{6,7},{7,6},{8,9},{9,8},{10,11... | collective-permute-start | bytes 1572872 | tf_op jit(solution)/shard_map/ppermute | solution.py:242
  211.4 1.5 collective-permute-done.24
  213.0 11.6 %all_to_all.37.refs_0_ = bf16[4,32,2048]{2,1,0:T(8,128)(2,1)S(1)} all-to-all(bf16[4,32,2048]{2,1,0:T(8,128)(2,1)S(1)} %bitcast.37), channel_id=1, replica_groups=mesh['rep'=2,'z'=8,'y'=4,'x'=4,'core'=2] {'x'}, dimensions={0} | all-to-all | bytes 1048576 | tf_op jit(solution)/shard_map/all_to_all | solution.py:255
  (56 shorter events, 14.9 us)
Async XLA Ops:
  3.5 18.2 %collective-permute-start.1 = (bf16[64,1152]{1,0:T(8,128)(2,1)}, bf16[64,1152]{1,0:T(8,128)(2,1)}, u32[]{:S(2)}, u32[]{:S(2)}) collective-permute-start(bf16[64,1152]{1,0:T(8,128)(2,1)} %get-tuple-element.23), channel_id=1, source_target_pairs={{0,480},{32,0},{64,32},{96,64},{128,96},{160,128},{192,160},{224,1... | collective-permute-start | bytes 442376 | tf_op jit(solution)/shard_map/ppermute | solution.py:184
  15.5 10.9 %collective-permute-start = (bf16[64,1152]{1,0:T(8,128)(2,1)}, bf16[64,1152]{1,0:T(8,128)(2,1)}, u32[]{:S(2)}, u32[]{:S(2)}) collective-permute-start(bf16[64,1152]{1,0:T(8,128)(2,1)} %get-tuple-element.23), channel_id=1, source_target_pairs={{0,32},{32,64},{64,96},{96,128},{128,160},{160,192},{192,224},{224... | collective-permute-start | bytes 442376 | tf_op jit(solution)/shard_map/ppermute | solution.py:184
  17.4 4.3 %copy-start.12 = (bf16[64,1152]{1,0:T(8,128)(2,1)S(1)}, bf16[64,1152]{1,0:T(8,128)(2,1)}, u32[]{:S(2)}) copy-start(bf16[64,1152]{1,0:T(8,128)(2,1)} %get-tuple-element.23) | copy-start | bytes 442372
  17.4 28.8 %all-to-all-start.3 = ((bf16[4,64,1024]{2,1,0:T(8,128)(2,1)}), bf16[4,64,1024]{2,1,0:T(8,128)(2,1)S(1)}, u32[]{:S(2)}, u32[]{:S(2)}) async-start(bf16[4,64,1024]{2,1,0:T(8,128)(2,1)} %get-tuple-element.29), calls=%async_computation.3 | async-start | bytes 1048576 | tf_op jit(solution)/shard_map/all_to_all | solution.py:221
  21.8 12.9 %collective-permute-start.3 = (bf16[64,1152]{1,0:T(8,128)(2,1)}, bf16[64,1152]{1,0:T(8,128)(2,1)S(1)}, u32[]{:S(2)}, u32[]{:S(2)}) collective-permute-start(bf16[64,1152]{1,0:T(8,128)(2,1)} %collective-permute-done.1), channel_id=1, source_target_pairs={{0,480},{32,0},{64,32},{96,64},{128,96},{160,128},{192,160},{224,1... | collective-permute-start | bytes 442376 | tf_op jit(solution)/shard_map/ppermute | solution.py:184
  26.4 7.4 %collective-permute-start.2 = (bf16[64,1152]{1,0:T(8,128)(2,1)}, bf16[64,1152]{1,0:T(8,128)(2,1)}, u32[]{:S(2)}, u32[]{:S(2)}) collective-permute-start(bf16[64,1152]{1,0:T(8,128)(2,1)} %collective-permute-done), channel_id=1, source_target_pairs={{0,32},{32,64},{64,96},{96,128},{128,160},{160,192},{192,224},{224... | collective-permute-start | bytes 442376 | tf_op jit(solution)/shard_map/ppermute | solution.py:184
  34.8 32.6 %collective-permute-start.4 = (bf16[5,64,1152]{2,1,0:T(8,128)(2,1)S(1)}, bf16[5,64,1152]{2,1,0:T(8,128)(2,1)S(1)}, u32[]{:S(2)}, u32[]{:S(2)}) collective-permute-start(bf16[5,64,1152]{2,1,0:T(8,128)(2,1)S(1)} %bitcast_dynamic-update-slice_fusion.refs_2_.refs_3_), channel_id=1, source_target_pairs={{0,8},{8,16},{16,24},{24,0},{1,9},{9,17},{17,25},{25,1},{2,10},{10... | collective-permute-start | bytes 2211848 | tf_op jit(solution)/shard_map/ppermute | solution.py:188
  38.1 16.5 %collective-permute-start.8 = (bf16[64,1152]{1,0:T(8,128)(2,1)}, bf16[64,1152]{1,0:T(8,128)(2,1)S(1)}, u32[]{:S(2)}, u32[]{:S(2)}) collective-permute-start(bf16[64,1152]{1,0:T(8,128)(2,1)} %collective-permute-done.1), channel_id=1, source_target_pairs={{0,448},{32,480},{64,0},{96,32},{128,64},{160,96},{192,128},{224,1... | collective-permute-start | bytes 442376 | tf_op jit(solution)/shard_map/ppermute | solution.py:184
  40.1 14.6 %collective-permute-start.7 = (bf16[64,1152]{1,0:T(8,128)(2,1)}, bf16[64,1152]{1,0:T(8,128)(2,1)S(1)}, u32[]{:S(2)}, u32[]{:S(2)}) collective-permute-start(bf16[64,1152]{1,0:T(8,128)(2,1)} %collective-permute-done), channel_id=1, source_target_pairs={{0,64},{32,96},{64,128},{96,160},{128,192},{160,224},{192,256},{22... | collective-permute-start | bytes 442376 | tf_op jit(solution)/shard_map/ppermute | solution.py:184
  44.3 14.8 %collective-permute-start.9 = (bf16[64,1152]{1,0:T(8,128)(2,1)}, bf16[64,1152]{1,0:T(8,128)(2,1)S(1)}, u32[]{:S(2)}, u32[]{:S(2)}) collective-permute-start(bf16[64,1152]{1,0:T(8,128)(2,1)} %collective-permute-done.2), channel_id=1, source_target_pairs={{0,64},{32,96},{64,128},{96,160},{128,192},{160,224},{192,256},{22... | collective-permute-start | bytes 442376 | tf_op jit(solution)/shard_map/ppermute | solution.py:184
  46.3 50.3 %all-to-all-start = ((bf16[8,32,2048]{2,1,0:T(8,128)(2,1)}), bf16[8,32,2048]{2,1,0:T(8,128)(2,1)S(1)}, u32[]{:S(2)}, u32[]{:S(2)}) async-start(bf16[8,32,2048]{2,1,0:T(8,128)(2,1)} %get-tuple-element.22), calls=%async_computation | async-start | bytes 2097152 | tf_op jit(solution)/shard_map/all_to_all | solution.py:359
  54.7 4.4 %copy-start.9 = (bf16[64,1152]{1,0:T(8,128)(2,1)}, bf16[64,1152]{1,0:T(8,128)(2,1)S(1)}, u32[]{:S(2)}) copy-start(bf16[64,1152]{1,0:T(8,128)(2,1)S(1)} %collective-permute-done.8) | copy-start | bytes 442372
  54.7 4.4 %copy-start.10 = (bf16[64,1152]{1,0:T(8,128)(2,1)}, bf16[64,1152]{1,0:T(8,128)(2,1)S(1)}, u32[]{:S(2)}) copy-start(bf16[64,1152]{1,0:T(8,128)(2,1)S(1)} %collective-permute-done.7) | copy-start | bytes 442372
  59.1 0.7 copy-start.11
  59.8 38.4 %copy-start.8 = (f32[8,384]{1,0:T(8,128)S(1)}, f32[8,384]{1,0:T(8,128)}, u32[]{:S(2)}) copy-start(f32[8,384]{1,0:T(8,128)} %get-tuple-element.21.refs_0_.small) | copy-start | bytes 36868
  60.9 12.0 %collective-permute-start.11 = (bf16[3,64,1152]{2,1,0:T(8,128)(2,1)S(1)}, bf16[3,64,1152]{2,1,0:T(8,128)(2,1)}, u32[]{:S(2)}, u32[]{:S(2)}) collective-permute-start(bf16[3,64,1152]{2,1,0:T(8,128)(2,1)S(1)} %pad_maximum_fusion.refs_6_.refs_7_), channel_id=1, source_target_pairs={{0,24},{8,0},{16,8},{24,16},{1,25},{9,1},{17,9},{25,17},{2,26},{10... | collective-permute-start | bytes 1327112 | tf_op jit(solution)/shard_map/ppermute | solution.py:188
  64.0 32.5 %collective-permute-start.5 = (bf16[5,64,1152]{2,1,0:T(8,128)(2,1)S(1)}, bf16[5,64,1152]{2,1,0:T(8,128)(2,1)}, u32[]{:S(2)}, u32[]{:S(2)}) collective-permute-start(bf16[5,64,1152]{2,1,0:T(8,128)(2,1)S(1)} %bitcast_dynamic-update-slice_fusion.refs_2_.refs_3_), channel_id=1, source_target_pairs={{0,24},{8,0},{16,8},{24,16},{1,25},{9,1},{17,9},{25,17},{2,26},{10... | collective-permute-start | bytes 2211848 | tf_op jit(solution)/shard_map/ppermute | solution.py:188
  67.4 30.8 %collective-permute-start.6 = (bf16[5,64,1152]{2,1,0:T(8,128)(2,1)S(1)}, bf16[5,64,1152]{2,1,0:T(8,128)(2,1)}, u32[]{:S(2)}, u32[]{:S(2)}) collective-permute-start(bf16[5,64,1152]{2,1,0:T(8,128)(2,1)S(1)} %collective-permute-done.4.refs_3_.refs_4_), channel_id=1, source_target_pairs={{0,8},{8,16},{16,24},{24,0},{1,9},{9,17},{17,25},{25,1},{2,10},{10... | collective-permute-start | bytes 2211848 | tf_op jit(solution)/shard_map/ppermute | solution.py:188
  69.3 26.4 %collective-permute-start.10 = (bf16[3,64,1152]{2,1,0:T(8,128)(2,1)S(1)}, bf16[3,64,1152]{2,1,0:T(8,128)(2,1)S(1)}, u32[]{:S(2)}, u32[]{:S(2)}) collective-permute-start(bf16[3,64,1152]{2,1,0:T(8,128)(2,1)S(1)} %pad_maximum_fusion.refs_6_.refs_7_), channel_id=1, source_target_pairs={{0,8},{8,16},{16,24},{24,0},{1,9},{9,17},{17,25},{25,1},{2,10},{10... | collective-permute-start | bytes 1327112 | tf_op jit(solution)/shard_map/ppermute | solution.py:188
  72.9 25.3 %collective-permute-start.12 = (bf16[3,64,1152]{2,1,0:T(8,128)(2,1)}, bf16[3,64,1152]{2,1,0:T(8,128)(2,1)}, u32[]{:S(2)}, u32[]{:S(2)}) collective-permute-start(bf16[3,64,1152]{2,1,0:T(8,128)(2,1)} %collective-permute-done.11.refs_8_.refs_9_), channel_id=1, source_target_pairs={{0,24},{8,0},{16,8},{24,16},{1,25},{9,1},{17,9},{25,17},{2,26},{10... | collective-permute-start | bytes 1327112 | tf_op jit(solution)/shard_map/ppermute | solution.py:188
  77.5 31.6 %collective-permute-start.15 = (bf16[256,1024]{1,0:T(8,128)(2,1)S(1)}, bf16[256,1024]{1,0:T(8,128)(2,1)}, u32[]{:S(2)}, u32[]{:S(2)}) collective-permute-start(bf16[256,1024]{1,0:T(8,128)(2,1)S(1)} %bitcast.31), channel_id=1, source_target_pairs={{0,32},{32,64},{64,96},{96,128},{128,160},{160,192},{192,224},{224... | collective-permute-start | bytes 1572872 | tf_op jit(solution)/shard_map/ppermute | solution.py:184
  95.8 0.8 copy-start
  98.2 1.0 copy-start.1
  102.7 9.8 %collective-permute-start.13 = (bf16[128,2048]{1,0:T(8,128)(2,1)S(1)}, bf16[128,2048]{1,0:T(8,128)(2,1)S(1)}, u32[]{:S(2)}, u32[]{:S(2)}) collective-permute-start(bf16[128,2048]{1,0:T(8,128)(2,1)S(1)} %get-tuple-element.25), channel_id=1, source_target_pairs={{0,1},{1,0},{2,3},{3,2},{4,5},{5,4},{6,7},{7,6},{8,9},{9,8},{10,11... | collective-permute-start | bytes 1572872 | tf_op jit(solution)/shard_map/ppermute | solution.py:242
  107.1 15.5 %collective-permute-start.18 = (bf16[256,1024]{1,0:T(8,128)(2,1)S(1)}, bf16[256,1024]{1,0:T(8,128)(2,1)}, u32[]{:S(2)}, u32[]{:S(2)}) collective-permute-start(bf16[256,1024]{1,0:T(8,128)(2,1)S(1)} %bitcast.32), channel_id=1, source_target_pairs={{0,480},{32,0},{64,32},{96,64},{128,96},{160,128},{192,160},{224,1... | collective-permute-start | bytes 1572872 | tf_op jit(solution)/shard_map/ppermute | solution.py:184
  109.1 16.9 %collective-permute-start.16 = (bf16[256,1024]{1,0:T(8,128)(2,1)}, bf16[256,1024]{1,0:T(8,128)(2,1)}, u32[]{:S(2)}, u32[]{:S(2)}) collective-permute-start(bf16[256,1024]{1,0:T(8,128)(2,1)} %collective-permute-done.15.rest_1_), channel_id=1, source_target_pairs={{0,32},{32,64},{64,96},{96,128},{128,160},{160,192},{192,224},{224... | collective-permute-start | bytes 1572872 | tf_op jit(solution)/shard_map/ppermute | solution.py:184
  113.4 15.8 %copy-start.4 = (f32[3,2048]{1,0:T(4,128)S(1)}, f32[3,2048]{1,0:T(4,128)}, u32[]{:S(2)}) copy-start(f32[3,2048]{1,0:T(4,128)} %get-tuple-element.27.refs_2_) | copy-start | bytes 73732
  113.4 15.8 %all-to-all-start.1 = ((bf16[4,32,2048]{2,1,0:T(8,128)(2,1)}), bf16[4,32,2048]{2,1,0:T(8,128)(2,1)}, u32[]{:S(2)}, u32[]{:S(2)}) async-start(bf16[4,32,2048]{2,1,0:T(8,128)(2,1)} %bitcast.19), calls=%async_computation.1 | async-start | bytes 1048576 | tf_op jit(solution)/shard_map/all_to_all | solution.py:255
  122.6 19.6 %collective-permute-start.19 = (bf16[256,1024]{1,0:T(8,128)(2,1)}, bf16[256,1024]{1,0:T(8,128)(2,1)S(1)}, u32[]{:S(2)}, u32[]{:S(2)}) collective-permute-start(bf16[256,1024]{1,0:T(8,128)(2,1)} %collective-permute-done.18.rest_5_), channel_id=1, source_target_pairs={{0,448},{32,480},{64,0},{96,32},{128,64},{160,96},{192,128},{224,1... | collective-permute-start | bytes 1572872 | tf_op jit(solution)/shard_map/ppermute | solution.py:184
  126.0 16.3 %collective-permute-start.17 = (bf16[256,1024]{1,0:T(8,128)(2,1)}, bf16[256,1024]{1,0:T(8,128)(2,1)S(1)}, u32[]{:S(2)}, u32[]{:S(2)}) collective-permute-start(bf16[256,1024]{1,0:T(8,128)(2,1)} %collective-permute-done.16.rest_2_), channel_id=1, source_target_pairs={{0,32},{32,64},{64,96},{96,128},{128,160},{160,192},{192,224},{224... | collective-permute-start | bytes 1572872 | tf_op jit(solution)/shard_map/ppermute | solution.py:184
  129.2 0.9 copy-start.7
  131.5 0.8 copy-start.3
  132.3 0.7 copy-start.5
  133.0 22.9 %all-to-all-start.2 = ((bf16[4,32,2048]{2,1,0:T(8,128)(2,1)}), bf16[4,32,2048]{2,1,0:T(8,128)(2,1)}, u32[]{:S(2)}, u32[]{:S(2)}) async-start(bf16[4,32,2048]{2,1,0:T(8,128)(2,1)} %copy-done.3), calls=%async_computation.2 | async-start | bytes 1048576 | tf_op jit(solution)/shard_map/all_to_all | solution.py:246
  137.2 24.9 %collective-permute-start.21 = (bf16[256,1024]{1,0:T(8,128)(2,1)}, bf16[256,1024]{1,0:T(8,128)(2,1)}, u32[]{:S(2)}, u32[]{:S(2)}) collective-permute-start(bf16[256,1024]{1,0:T(8,128)(2,1)} %collective-permute-done.18.rest_5_), channel_id=1, source_target_pairs={{0,480},{32,0},{64,32},{96,64},{128,96},{160,128},{192,160},{224,1... | collective-permute-start | bytes 1572872 | tf_op jit(solution)/shard_map/ppermute | solution.py:184
  143.1 24.7 %collective-permute-start.20 = (bf16[256,1024]{1,0:T(8,128)(2,1)}, bf16[256,1024]{1,0:T(8,128)(2,1)}, u32[]{:S(2)}, u32[]{:S(2)}) collective-permute-start(bf16[256,1024]{1,0:T(8,128)(2,1)} %pick.1), channel_id=1, source_target_pairs={{0,32},{1,481},{32,64},{33,1},{64,96},{65,33},{96,128},{97,65},{12... | collective-permute-start | bytes 1572872 | tf_op jit(solution)/shard_map/ppermute | solution.py:237
  155.9 11.9 %collective-permute-start.14 = (bf16[128,2048]{1,0:T(8,128)(2,1)}, bf16[128,2048]{1,0:T(8,128)(2,1)S(1)}, u32[]{:S(2)}, u32[]{:S(2)}) collective-permute-start(bf16[128,2048]{1,0:T(8,128)(2,1)} %bitcast.20.own_rows), channel_id=1, source_target_pairs={{0,1},{1,0},{2,3},{3,2},{4,5},{5,4},{6,7},{7,6},{8,9},{9,8},{10,11... | collective-permute-start | bytes 1572872 | tf_op jit(solution)/shard_map/ppermute | solution.py:242
  171.9 3.8 %collective-permute-start.22 = (bf16[128,2048]{1,0:T(8,128)(2,1)S(1)}, bf16[128,2048]{1,0:T(8,128)(2,1)S(1)}, u32[]{:S(2)}, u32[]{:S(2)}) collective-permute-start(bf16[128,2048]{1,0:T(8,128)(2,1)S(1)} %get-tuple-element.31), channel_id=1, source_target_pairs={{0,1},{1,0},{2,3},{3,2},{4,5},{5,4},{6,7},{7,6},{8,9},{9,8},{10,11... | collective-permute-start | bytes 1572872 | tf_op jit(solution)/shard_map/ppermute | solution.py:242
  175.8 13.1 %copy-start.6 = (f32[32,2048]{1,0:T(8,128)S(1)}, f32[32,2048]{1,0:T(8,128)}, u32[]{:S(2)}) copy-start(f32[32,2048]{1,0:T(8,128)} %copy-done.5) | copy-start | bytes 786436
  189.2 16.4 %copy-start.2 = (bf16[3,64,1152]{2,1,0:T(8,128)(2,1)S(1)}, bf16[3,64,1152]{2,1,0:T(8,128)(2,1)}, u32[]{:S(2)}) copy-start(bf16[3,64,1152]{2,1,0:T(8,128)(2,1)} %copy-done) | copy-start | bytes 1327108
  200.1 5.5 %collective-permute-start.23 = (bf16[128,2048]{1,0:T(8,128)(2,1)S(1)}, bf16[128,2048]{1,0:T(8,128)(2,1)S(1)}, u32[]{:S(2)}, u32[]{:S(2)}) collective-permute-start(bf16[128,2048]{1,0:T(8,128)(2,1)S(1)} %bitcast.34), channel_id=1, source_target_pairs={{0,1},{1,0},{2,3},{3,2},{4,5},{5,4},{6,7},{7,6},{8,9},{9,8},{10,11... | collective-permute-start | bytes 1572872 | tf_op jit(solution)/shard_map/ppermute | solution.py:242
  209.1 3.8 %collective-permute-start.24 = (bf16[128,2048]{1,0:T(8,128)(2,1)S(1)}, bf16[128,2048]{1,0:T(8,128)(2,1)S(1)}, u32[]{:S(2)}, u32[]{:S(2)}) collective-permute-start(bf16[128,2048]{1,0:T(8,128)(2,1)S(1)} %get-tuple-element.35), channel_id=1, source_target_pairs={{0,1},{1,0},{2,3},{3,2},{4,5},{5,4},{6,7},{7,6},{8,9},{9,8},{10,11... | collective-permute-start | bytes 1572872 | tf_op jit(solution)/shard_map/ppermute | solution.py:242

commit v6 on v5

--- a/solution.py
+++ b/solution.py
@@ -130,7 +130,7 @@
         out_shape=(
             jax.ShapeDtypeStruct((rows, 3 * n), jnp.bfloat16),
             jax.ShapeDtypeStruct((NY, rows, 4 * DK), jnp.bfloat16),
-            jax.ShapeDtypeStruct((2 * NX, *tokens.shape), jnp.bfloat16),
+            jax.ShapeDtypeStruct((NX, *tokens.shape), jnp.bfloat16),
             jax.ShapeDtypeStruct((8, n), jnp.float32),
             jax.ShapeDtypeStruct(tokens.shape, jnp.bfloat16),
             jax.ShapeDtypeStruct(gains.shape, jnp.float32),
@@ -262,13 +262,7 @@
 def ffn_kernel(spans, small, *rest):
     row_refs, arrays, (own_ref, other_ref) = rest[:spans], rest[spans:-2], rest[-2:]
     units = arrays[0].shape[-1] // 3
-    core = lax.axis_index("core")
-    if spans == 1:
-        every = row_refs[0]
-        sides = [core, 1 - core]
-        rows = jnp.concatenate([every[2 * k + s] for s in sides for k in range(NX)], axis=0)
-    else:
-        rows = jnp.concatenate([r[...] for r in row_refs], axis=0)
+    rows = jnp.concatenate([r[...] for r in row_refs], axis=0)
     gate = dot(rows, stacked(arrays, 0, units)) * small[0:1, :]
     up = dot(rows, stacked(arrays, units, 2 * units)) * small[1:2, :]
     hidden = low(gate / (1.0 + jnp.exp(-gate)) * up)
@@ -356,10 +350,10 @@
         + [row(decay_rate)],
     )
     ffn_arrays = gather_ffn(ffn_mine)
-    every = lax.all_to_all(copies, ("x", "core"), split_axis=0, concat_axis=0, tiled=True)
+    rows = gather_rows(copies)
     mix_arrays = gather_mix(mix_mine)
 
-    arrived = feed_forward(small, [every], ffn_arrays)
+    arrived = feed_forward(small, rows, ffn_arrays)
     stream, copies = join(0.5, 1, arrived, stream, gains, rows_as=FFN_TO_MIX)
     own, other = gather_rows(copies)
     arrived = mix(small, own, other, mix_arrays)

time: 227 us -> 229 us (level)
  blocking collectives: 35.5 us -> 58.6 us
  waiting for transfers between devices: 50.5 us -> 34.2 us
  local copies, waits for them, and re-layouts: 7.71 us -> 2.56 us
    all_to_all x0 -> x1, blocking collectives: none -> 23 us  [gather_mix(): mine = lax.all_to_all(copies, 'y', split_axis=0, concat_axis=0, tiled=True)]
    ppermute x6, waiting for transfers between devices: 19.4 us -> 0.02 us  [along_y(): return lax.ppermute(array, 'y', [(g, (g + step) % NY) for g in range(NY)])]
    all_to_all x2 -> x0, starting transfers between devices: 12.7 us -> none  [the longest x1 8.37 us: on_device(): lax.all_to_all(copies, ('x', 'core'), split_axis=0, concat_axis=0, tiled=...]
    unnamed x30 -> x26, local copies, waits for them, and re-layouts: 7.69 us -> 2.55 us
    ppermute x13, starting transfers between devices: 44.1 us -> 48.3 us  [along_z(): lax.ppermute(array, ('rep', 'z'), [(g, (g + step) % (2 * NZ)) for g in ra...]
    ppermute x5 -> x6, starting transfers between devices: 14.6 us -> 18.9 us  [swap_cores(): return lax.ppermute(array, 'core', [(0, 1), (1, 0)])]
    all_to_all x1 -> x2, starting transfers between devices: 4.13 us -> 8.28 us  [gather_rows(): own = lax.all_to_all(copies, 'x', split_axis=0, concat_axis=0, tiled=True)]
    ppermute x13, waiting for transfers between devices: 20.4 us -> 23.8 us  [along_z(): lax.ppermute(array, ('rep', 'z'), [(g, (g + step) % (2 * NZ)) for g in ra...]
  transfers between devices with their start and end apart: 29 -> 29, of which waited for: 13 -> 9; matrix products, arithmetic and copies ran while one was open for 2% -> 1% of each run, Pallas kernels for 3% -> 3%
where the time goes in v6:
time: 229 us; the launch traced here: 227 us
  starting transfers between devices  111 us (48%)
  blocking collectives  58.6 us (26%)
  waiting for transfers between devices  34.2 us (15%)
  Pallas kernels  18.1 us (8%)
  local copies, waits for them, and re-layouts  2.56 us (1%)
    ppermute x13, starting transfers between devices, along_z(): lax.ppermute(array, ('rep', 'z'), [(g, (g + step) % (2 * NZ)) for g in ra...  48.3 us
    all_to_all x2, blocking collectives, return_rows(): return lax.all_to_all(blocks, 'x', split_axis=0, concat_axis=0, tiled=True)  24.7 us
    ppermute x13, waiting for transfers between devices, along_z(): lax.ppermute(array, ('rep', 'z'), [(g, (g + step) % (2 * NZ)) for g in ra...  23.8 us
    all_to_all x1, blocking collectives, gather_mix(): mine = lax.all_to_all(copies, 'y', split_axis=0, concat_axis=0, tiled=True)  23 us
    ppermute x6, starting transfers between devices, swap_cores(): return lax.ppermute(array, 'core', [(0, 1), (1, 0)])  18.9 us
    ppermute x6, starting transfers between devices, along_y(): return lax.ppermute(array, 'y', [(g, (g + step) % NY) for g in range(NY)])  18.4 us
    ppermute x1, starting transfers between devices, gather_mix(): last = lax.ppermute(last, ('rep', 'z', 'core'), pairs)  13.1 us
    all_to_all x1, blocking collectives, gather_rows(): own = lax.all_to_all(copies, 'x', split_axis=0, concat_axis=0, tiled=True)  10.8 us
  transfers between devices with their start and end apart: 29, of which 9 were waited for; matrix products, arithmetic and copies ran while one was open for 1% of the time, Pallas kernels for 3%

profile of v6, /device:TPU:1, one launch (start us, length us, event | category | flops | bytes accessed | tf_op | source)
XLA Modules:
  0.0 227.1 jit_solution(9944689663602239069)
XLA Ops:
  0.7 2.7 %pack.1 = (bf16[64,1152]{1,0:T(8,128)(2,1)}, bf16[4,64,1024]{2,1,0:T(8,128)(2,1)}, bf16[4,32,2048]{2,1,0:T(8,128)(2,1)}, f32[8,384]{1,0:T(8,128)}, bf16[32,2048]{1,0:T(8,128)(2,1)}, /*index=5*/f32[3,2048]{1,0:T(4,128)}) custom-call(f32[64,384]{1,0:T(8,128)} %gate.1, f32[64,384]{1,0:T(8,128)} %up.1, f32[64,384]{1,0:T(8,128)} %bitcast.40, f32[1,64]{1,0:T(1,128)} %bitcast.48, ...), custom_call_target="tpu_custom_call" | custom-call | tf_op jit(solution)/shard_map/pack/pallas_call | solution.py:128
  3.4 11.9 %collective-permute-start.2 = (bf16[64,1152]{1,0:T(8,128)(2,1)}, bf16[64,1152]{1,0:T(8,128)(2,1)S(1)}, u32[]{:S(2)}, u32[]{:S(2)}) collective-permute-start(bf16[64,1152]{1,0:T(8,128)(2,1)} %get-tuple-element.23), channel_id=1, source_target_pairs={{0,480},{32,0},{64,32},{96,64},{128,96},{160,128},{192,160},{224,1... | collective-permute-start | bytes 442376 | tf_op jit(solution)/shard_map/ppermute | solution.py:184
  15.3 1.9 collective-permute-start.1
  18.2 5.2 %collective-permute-start.4 = (bf16[64,1152]{1,0:T(8,128)(2,1)S(1)}, bf16[64,1152]{1,0:T(8,128)(2,1)S(1)}, u32[]{:S(2)}, u32[]{:S(2)}) collective-permute-start(bf16[64,1152]{1,0:T(8,128)(2,1)S(1)} %collective-permute-done.2), channel_id=1, source_target_pairs={{0,480},{32,0},{64,32},{96,64},{128,96},{160,128},{192,160},{224,1... | collective-permute-start | bytes 442376 | tf_op jit(solution)/shard_map/ppermute | solution.py:184
  23.4 1.9 collective-permute-start.3
  25.3 5.1 %collective-permute-done.3 = bf16[64,1152]{1,0:T(8,128)(2,1)S(1)} collective-permute-done((bf16[64,1152]{1,0:T(8,128)(2,1)S(1)}, bf16[64,1152]{1,0:T(8,128)(2,1)S(1)}, u32[]{:S(2)}, u32[]{:S(2)}) %collective-permute-start.3) | collective-permute-done | bytes 147488 | tf_op jit(solution)/shard_map/ppermute | solution.py:184
  30.5 3.2 %collective-permute-start.5 = (bf16[5,64,1152]{2,1,0:T(8,128)(2,1)S(1)}, bf16[5,64,1152]{2,1,0:T(8,128)(2,1)S(1)}, u32[]{:S(2)}, u32[]{:S(2)}) collective-permute-start(bf16[5,64,1152]{2,1,0:T(8,128)(2,1)S(1)} %bitcast_dynamic-update-slice_fusion.refs_3_), channel_id=1, source_target_pairs={{0,8},{8,16},{16,24},{24,0},{1,9},{9,17},{17,25},{25,1},{2,10},{10... | collective-permute-start | bytes 2211848 | tf_op jit(solution)/shard_map/ppermute | solution.py:188
  33.7 1.9 collective-permute-start.9
  35.7 4.3 %collective-permute-start.8 = (bf16[64,1152]{1,0:T(8,128)(2,1)S(1)}, bf16[64,1152]{1,0:T(8,128)(2,1)S(1)}, u32[]{:S(2)}, u32[]{:S(2)}) collective-permute-start(bf16[64,1152]{1,0:T(8,128)(2,1)S(1)} %collective-permute-done.1), channel_id=1, source_target_pairs={{0,64},{32,96},{64,128},{96,160},{128,192},{160,224},{192,256},{22... | collective-permute-start | bytes 442376 | tf_op jit(solution)/shard_map/ppermute | solution.py:184
  39.9 1.9 collective-permute-start.10
  41.8 4.1 %all-to-all-start = ((bf16[4,32,2048]{2,1,0:T(8,128)(2,1)}), bf16[4,32,2048]{2,1,0:T(8,128)(2,1)}, u32[]{:S(2)}, u32[]{:S(2)}) async-start(bf16[4,32,2048]{2,1,0:T(8,128)(2,1)} %get-tuple-element.22), calls=%async_computation | async-start | bytes 1048576 | tf_op jit(solution)/shard_map/all_to_all | solution.py:246
  46.0 8.4 %collective-permute-done.10 = bf16[64,1152]{1,0:T(8,128)(2,1)S(1)} collective-permute-done((bf16[64,1152]{1,0:T(8,128)(2,1)S(1)}, bf16[64,1152]{1,0:T(8,128)(2,1)S(1)}, u32[]{:S(2)}, u32[]{:S(2)}) %collective-permute-start.10) | collective-permute-done | bytes 147488 | tf_op jit(solution)/shard_map/ppermute | solution.py:184
  54.5 3.4 %collective-permute-start.12 = (bf16[3,64,1152]{2,1,0:T(8,128)(2,1)S(1)}, bf16[3,64,1152]{2,1,0:T(8,128)(2,1)}, u32[]{:S(2)}, u32[]{:S(2)}) collective-permute-start(bf16[3,64,1152]{2,1,0:T(8,128)(2,1)S(1)} %pad_maximum_fusion.refs_7_), channel_id=1, source_target_pairs={{0,24},{8,0},{16,8},{24,16},{1,25},{9,1},{17,9},{25,17},{2,26},{10... | collective-permute-start | bytes 1327112 | tf_op jit(solution)/shard_map/ppermute | solution.py:188
  57.9 3.4 %collective-permute-start.6 = (bf16[5,64,1152]{2,1,0:T(8,128)(2,1)S(1)}, bf16[5,64,1152]{2,1,0:T(8,128)(2,1)S(1)}, u32[]{:S(2)}, u32[]{:S(2)}) collective-permute-start(bf16[5,64,1152]{2,1,0:T(8,128)(2,1)S(1)} %bitcast_dynamic-update-slice_fusion.refs_3_), channel_id=1, source_target_pairs={{0,24},{8,0},{16,8},{24,16},{1,25},{9,1},{17,9},{25,17},{2,26},{10... | collective-permute-start | bytes 2211848 | tf_op jit(solution)/shard_map/ppermute | solution.py:188
  61.3 1.9 collective-permute-start.7
  63.2 4.1 %collective-permute-start = (bf16[128,2048]{1,0:T(8,128)(2,1)}, bf16[128,2048]{1,0:T(8,128)(2,1)S(1)}, u32[]{:S(2)}, u32[]{:S(2)}) collective-permute-start(bf16[128,2048]{1,0:T(8,128)(2,1)} %bitcast.11.refs_1_), channel_id=1, source_target_pairs={{0,1},{1,0},{2,3},{3,2},{4,5},{5,4},{6,7},{7,6},{8,9},{9,8},{10,11... | collective-permute-start | bytes 1572872 | tf_op jit(solution)/shard_map/ppermute | solution.py:242
  67.3 2.0 collective-permute-start.11
  69.4 4.6 %collective-permute-start.13 = (bf16[3,64,1152]{2,1,0:T(8,128)(2,1)}, bf16[3,64,1152]{2,1,0:T(8,128)(2,1)S(1)}, u32[]{:S(2)}, u32[]{:S(2)}) collective-permute-start(bf16[3,64,1152]{2,1,0:T(8,128)(2,1)} %collective-permute-done.12.refs_9_), channel_id=1, source_target_pairs={{0,24},{8,0},{16,8},{24,16},{1,25},{9,1},{17,9},{25,17},{2,26},{10... | collective-permute-start | bytes 1327112 | tf_op jit(solution)/shard_map/ppermute | solution.py:188
  73.9 23.0 %all_to_all.35 = bf16[4,64,1024]{2,1,0:T(8,128)(2,1)} all-to-all(bf16[4,64,1024]{2,1,0:T(8,128)(2,1)} %get-tuple-element.29), channel_id=1, replica_groups=mesh['rep'=2,'z'=8,'y'=4,'x'=4,'core'=2] {'y'}, dimensions={0} | all-to-all | bytes 1048576 | tf_op jit(solution)/shard_map/all_to_all | solution.py:221
  97.0 1.9 collective-permute-start.16
  98.9 3.2 %ffn.2 = (f32[128,2048]{1,0:T(8,128)S(1)}, bf16[128,2048]{1,0:T(8,128)(2,1)S(1)}) custom-call(f32[8,384]{1,0:T(8,128)S(1)} %copy-done.9, bf16[128,2048]{1,0:T(8,128)(2,1)} %bitcast.11.refs_1_, bf16[128,2048]{1,0:T(8,128)(2,1)S(1)} %collective-permute-done.refs_2_, bf16[5,64,1152]{2,1,0:T(8,128)(2,1)S(1)} %bitcast_dynamic-update-slice_fusion.refs_3_, ...), custom_call_target="tpu_custom_call" | custom-call | tf_op jit(solution)/shard_map/ffn/pallas_call | solution.py:278
  102.2 4.6 %collective-permute-start.14 = (bf16[128,2048]{1,0:T(8,128)(2,1)S(1)}, bf16[128,2048]{1,0:T(8,128)(2,1)S(1)}, u32[]{:S(2)}, u32[]{:S(2)}) collective-permute-start(bf16[128,2048]{1,0:T(8,128)(2,1)S(1)} %get-tuple-element.25), channel_id=1, source_target_pairs={{0,1},{1,0},{2,3},{3,2},{4,5},{5,4},{6,7},{7,6},{8,9},{9,8},{10,11... | collective-permute-start | bytes 1572872 | tf_op jit(solution)/shard_map/ppermute | solution.py:242
  106.7 4.9 %collective-permute-start.19 = (bf16[256,1024]{1,0:T(8,128)(2,1)}, bf16[256,1024]{1,0:T(8,128)(2,1)}, u32[]{:S(2)}, u32[]{:S(2)}) collective-permute-start(bf16[256,1024]{1,0:T(8,128)(2,1)} %bitcast.22.rest_0_), channel_id=1, source_target_pairs={{0,480},{32,0},{64,32},{96,64},{128,96},{160,128},{192,160},{224,1... | collective-permute-start | bytes 1572872 | tf_op jit(solution)/shard_map/ppermute | solution.py:184
  111.6 1.9 collective-permute-start.17
  114.5 4.3 %all-to-all-start.1 = ((bf16[4,32,2048]{2,1,0:T(8,128)(2,1)}), bf16[4,32,2048]{2,1,0:T(8,128)(2,1)}, u32[]{:S(2)}, u32[]{:S(2)}) async-start(bf16[4,32,2048]{2,1,0:T(8,128)(2,1)} %bitcast.34), calls=%async_computation.1 | async-start | bytes 1048576 | tf_op jit(solution)/shard_map/all_to_all | solution.py:255
  118.8 4.4 %collective-permute-done.19.rest_5_ = bf16[256,1024]{1,0:T(8,128)(2,1)} collective-permute-done((bf16[256,1024]{1,0:T(8,128)(2,1)}, bf16[256,1024]{1,0:T(8,128)(2,1)}, u32[]{:S(2)}, u32[]{:S(2)}) %collective-permute-start.19) | collective-permute-done | bytes 524320 | tf_op jit(solution)/shard_map/ppermute | solution.py:184
  123.2 4.1 %collective-permute-start.20 = (bf16[256,1024]{1,0:T(8,128)(2,1)}, bf16[256,1024]{1,0:T(8,128)(2,1)}, u32[]{:S(2)}, u32[]{:S(2)}) collective-permute-start(bf16[256,1024]{1,0:T(8,128)(2,1)} %collective-permute-done.19.rest_5_), channel_id=1, source_target_pairs={{0,448},{32,480},{64,0},{96,32},{128,64},{160,96},{192,128},{224,1... | collective-permute-start | bytes 1572872 | tf_op jit(solution)/shard_map/ppermute | solution.py:184
  127.3 4.3 %collective-permute-start.18 = (bf16[256,1024]{1,0:T(8,128)(2,1)}, bf16[256,1024]{1,0:T(8,128)(2,1)}, u32[]{:S(2)}, u32[]{:S(2)}) collective-permute-start(bf16[256,1024]{1,0:T(8,128)(2,1)} %collective-permute-done.17.rest_2_), channel_id=1, source_target_pairs={{0,32},{32,64},{64,96},{96,128},{128,160},{160,192},{192,224},{224... | collective-permute-start | bytes 1572872 | tf_op jit(solution)/shard_map/ppermute | solution.py:184
  131.6 1.4 join.3
  134.6 4.1 %all-to-all-start.2 = ((bf16[4,32,2048]{2,1,0:T(8,128)(2,1)}), bf16[4,32,2048]{2,1,0:T(8,128)(2,1)}, u32[]{:S(2)}, u32[]{:S(2)}) async-start(bf16[4,32,2048]{2,1,0:T(8,128)(2,1)} %copy-done.4), calls=%async_computation.2 | async-start | bytes 1048576 | tf_op jit(solution)/shard_map/all_to_all | solution.py:246
  138.8 2.2 collective-permute-start.22
  141.0 2.9 %collective-permute-done.20.second.rest_7_ = bf16[256,1024]{1,0:T(8,128)(2,1)} collective-permute-done((bf16[256,1024]{1,0:T(8,128)(2,1)}, bf16[256,1024]{1,0:T(8,128)(2,1)}, u32[]{:S(2)}, u32[]{:S(2)}) %collective-permute-start.20) | collective-permute-done | bytes 524320 | tf_op jit(solution)/shard_map/ppermute | solution.py:184
  143.9 2.1 pick.1
  145.9 13.1 %collective-permute-start.21 = (bf16[256,1024]{1,0:T(8,128)(2,1)}, bf16[256,1024]{1,0:T(8,128)(2,1)}, u32[]{:S(2)}, u32[]{:S(2)}) collective-permute-start(bf16[256,1024]{1,0:T(8,128)(2,1)} %pick.1), channel_id=1, source_target_pairs={{0,32},{1,481},{32,64},{33,1},{64,96},{65,33},{96,128},{97,65},{12... | collective-permute-start | bytes 1572872 | tf_op jit(solution)/shard_map/ppermute | solution.py:237
  159.1 1.9 collective-permute-start.15
  161.0 2.9 %collective-permute-done.22.rest_6_ = bf16[256,1024]{1,0:T(8,128)(2,1)} collective-permute-done((bf16[256,1024]{1,0:T(8,128)(2,1)}, bf16[256,1024]{1,0:T(8,128)(2,1)}, u32[]{:S(2)}, u32[]{:S(2)}) %collective-permute-start.22) | collective-permute-done | bytes 524320 | tf_op jit(solution)/shard_map/ppermute | solution.py:184
  163.9 5.4 %collective-permute-done.21.rest_4_ = bf16[256,1024]{1,0:T(8,128)(2,1)} collective-permute-done((bf16[256,1024]{1,0:T(8,128)(2,1)}, bf16[256,1024]{1,0:T(8,128)(2,1)}, u32[]{:S(2)}, u32[]{:S(2)}) %collective-permute-start.21) | collective-permute-done | bytes 524320 | tf_op jit(solution)/shard_map/ppermute | solution.py:237
  169.4 4.5 %mix.1 = (f32[128,2048]{1,0:T(8,128)S(1)}, bf16[128,2048]{1,0:T(8,128)(2,1)S(1)}) custom-call(f32[8,384]{1,0:T(8,128)S(1)} %copy-done.10, bf16[128,2048]{1,0:T(8,128)(2,1)} %bitcast.21.own_rows, bf16[128,2048]{1,0:T(8,128)(2,1)S(1)} %collective-permute-done.15.other_rows, bf16[256,1024]{1,0:T(8,128)(2,1)} %bitcast.22.rest_0_, ...), custom_call_target="tpu_custom_call" | custom-call | tf_op jit(solution)/shard_map/mix/pallas_call | solution.py:324
  173.9 1.9 collective-permute-start.23
  175.8 1.9 collective-permute-done.23
  177.8 13.1 %all_to_all.36.refs_0_ = bf16[4,32,2048]{2,1,0:T(8,128)(2,1)S(1)} all-to-all(bf16[4,32,2048]{2,1,0:T(8,128)(2,1)S(1)} %bitcast.35), channel_id=1, replica_groups=mesh['rep'=2,'z'=8,'y'=4,'x'=4,'core'=2] {'x'}, dimensions={0} | all-to-all | bytes 1048576 | tf_op jit(solution)/shard_map/all_to_all | solution.py:255
  191.3 10.8 %all_to_all.37 = bf16[4,32,2048]{2,1,0:T(8,128)(2,1)S(1)} all-to-all(bf16[4,32,2048]{2,1,0:T(8,128)(2,1)S(1)} %get-tuple-element.33), channel_id=1, replica_groups=mesh['rep'=2,'z'=8,'y'=4,'x'=4,'core'=2] {'x'}, dimensions={0} | all-to-all | bytes 1048576 | tf_op jit(solution)/shard_map/all_to_all | solution.py:246
  202.2 4.0 %collective-permute-start.24 = (bf16[128,2048]{1,0:T(8,128)(2,1)S(1)}, bf16[128,2048]{1,0:T(8,128)(2,1)S(1)}, u32[]{:S(2)}, u32[]{:S(2)}) collective-permute-start(bf16[128,2048]{1,0:T(8,128)(2,1)S(1)} %bitcast.32), channel_id=1, source_target_pairs={{0,1},{1,0},{2,3},{3,2},{4,5},{5,4},{6,7},{7,6},{8,9},{9,8},{10,11... | collective-permute-start | bytes 1572872 | tf_op jit(solution)/shard_map/ppermute | solution.py:242
  206.2 1.5 collective-permute-done.24.refs_2_
  207.7 2.9 %ffn.3 = (f32[128,2048]{1,0:T(8,128)S(1)}, bf16[128,2048]{1,0:T(8,128)(2,1)S(1)}) custom-call(f32[8,384]{1,0:T(8,128)S(1)} %copy-done.10, bf16[128,2048]{1,0:T(8,128)(2,1)S(1)} %bitcast.33, bf16[128,2048]{1,0:T(8,128)(2,1)S(1)} %collective-permute-done.24.refs_2_, bf16[5,64,1152]{2,1,0:T(8,128)(2,1)S(1)} %bitcast_dynamic-update-slice_fusion.refs_3_, ...), custom_call_target="tpu_custom_call" | custom-call | tf_op jit(solution)/shard_map/ffn/pallas_call | solution.py:278
  210.6 2.3 %collective-permute-start.25 = (bf16[128,2048]{1,0:T(8,128)(2,1)S(1)}, bf16[128,2048]{1,0:T(8,128)(2,1)S(1)}, u32[]{:S(2)}, u32[]{:S(2)}) collective-permute-start(bf16[128,2048]{1,0:T(8,128)(2,1)S(1)} %get-tuple-element.35), channel_id=1, source_target_pairs={{0,1},{1,0},{2,3},{3,2},{4,5},{5,4},{6,7},{7,6},{8,9},{9,8},{10,11... | collective-permute-start | bytes 1572872 | tf_op jit(solution)/shard_map/ppermute | solution.py:242
  212.9 1.5 collective-permute-done.25
  214.5 11.6 %all_to_all.38.refs_0_ = bf16[4,32,2048]{2,1,0:T(8,128)(2,1)S(1)} all-to-all(bf16[4,32,2048]{2,1,0:T(8,128)(2,1)S(1)} %bitcast.36), channel_id=1, replica_groups=mesh['rep'=2,'z'=8,'y'=4,'x'=4,'core'=2] {'x'}, dimensions={0} | all-to-all | bytes 1048576 | tf_op jit(solution)/shard_map/all_to_all | solution.py:255
  (53 shorter events, 5.1 us)
Async XLA Ops:
  3.4 14.8 %collective-permute-start.2 = (bf16[64,1152]{1,0:T(8,128)(2,1)}, bf16[64,1152]{1,0:T(8,128)(2,1)S(1)}, u32[]{:S(2)}, u32[]{:S(2)}) collective-permute-start(bf16[64,1152]{1,0:T(8,128)(2,1)} %get-tuple-element.23), channel_id=1, source_target_pairs={{0,480},{32,0},{64,32},{96,64},{128,96},{160,128},{192,160},{224,1... | collective-permute-start | bytes 442376 | tf_op jit(solution)/shard_map/ppermute | solution.py:184
  15.3 8.0 %collective-permute-start.1 = (bf16[64,1152]{1,0:T(8,128)(2,1)}, bf16[64,1152]{1,0:T(8,128)(2,1)S(1)}, u32[]{:S(2)}, u32[]{:S(2)}) collective-permute-start(bf16[64,1152]{1,0:T(8,128)(2,1)} %get-tuple-element.23), channel_id=1, source_target_pairs={{0,32},{32,64},{64,96},{96,128},{128,160},{160,192},{192,224},{224... | collective-permute-start | bytes 442376 | tf_op jit(solution)/shard_map/ppermute | solution.py:184
  18.2 12.3 %collective-permute-start.4 = (bf16[64,1152]{1,0:T(8,128)(2,1)S(1)}, bf16[64,1152]{1,0:T(8,128)(2,1)S(1)}, u32[]{:S(2)}, u32[]{:S(2)}) collective-permute-start(bf16[64,1152]{1,0:T(8,128)(2,1)S(1)} %collective-permute-done.2), channel_id=1, source_target_pairs={{0,480},{32,0},{64,32},{96,64},{128,96},{160,128},{192,160},{224,1... | collective-permute-start | bytes 442376 | tf_op jit(solution)/shard_map/ppermute | solution.py:184
  23.4 7.1 %collective-permute-start.3 = (bf16[64,1152]{1,0:T(8,128)(2,1)S(1)}, bf16[64,1152]{1,0:T(8,128)(2,1)S(1)}, u32[]{:S(2)}, u32[]{:S(2)}) collective-permute-start(bf16[64,1152]{1,0:T(8,128)(2,1)S(1)} %collective-permute-done.1), channel_id=1, source_target_pairs={{0,32},{32,64},{64,96},{96,128},{128,160},{160,192},{192,224},{224... | collective-permute-start | bytes 442376 | tf_op jit(solution)/shard_map/ppermute | solution.py:184
  30.5 30.7 %collective-permute-start.5 = (bf16[5,64,1152]{2,1,0:T(8,128)(2,1)S(1)}, bf16[5,64,1152]{2,1,0:T(8,128)(2,1)S(1)}, u32[]{:S(2)}, u32[]{:S(2)}) collective-permute-start(bf16[5,64,1152]{2,1,0:T(8,128)(2,1)S(1)} %bitcast_dynamic-update-slice_fusion.refs_3_), channel_id=1, source_target_pairs={{0,8},{8,16},{16,24},{24,0},{1,9},{9,17},{17,25},{25,1},{2,10},{10... | collective-permute-start | bytes 2211848 | tf_op jit(solution)/shard_map/ppermute | solution.py:188
  33.7 12.3 %collective-permute-start.9 = (bf16[64,1152]{1,0:T(8,128)(2,1)S(1)}, bf16[64,1152]{1,0:T(8,128)(2,1)S(1)}, u32[]{:S(2)}, u32[]{:S(2)}) collective-permute-start(bf16[64,1152]{1,0:T(8,128)(2,1)S(1)} %collective-permute-done.2), channel_id=1, source_target_pairs={{0,448},{32,480},{64,0},{96,32},{128,64},{160,96},{192,128},{224,1... | collective-permute-start | bytes 442376 | tf_op jit(solution)/shard_map/ppermute | solution.py:184
  35.7 10.4 %collective-permute-start.8 = (bf16[64,1152]{1,0:T(8,128)(2,1)S(1)}, bf16[64,1152]{1,0:T(8,128)(2,1)S(1)}, u32[]{:S(2)}, u32[]{:S(2)}) collective-permute-start(bf16[64,1152]{1,0:T(8,128)(2,1)S(1)} %collective-permute-done.1), channel_id=1, source_target_pairs={{0,64},{32,96},{64,128},{96,160},{128,192},{160,224},{192,256},{22... | collective-permute-start | bytes 442376 | tf_op jit(solution)/shard_map/ppermute | solution.py:184
  39.9 14.5 %collective-permute-start.10 = (bf16[64,1152]{1,0:T(8,128)(2,1)S(1)}, bf16[64,1152]{1,0:T(8,128)(2,1)S(1)}, u32[]{:S(2)}, u32[]{:S(2)}) collective-permute-start(bf16[64,1152]{1,0:T(8,128)(2,1)S(1)} %collective-permute-done.3), channel_id=1, source_target_pairs={{0,64},{32,96},{64,128},{96,160},{128,192},{160,224},{192,256},{22... | collective-permute-start | bytes 442376 | tf_op jit(solution)/shard_map/ppermute | solution.py:184
  41.8 21.3 %all-to-all-start = ((bf16[4,32,2048]{2,1,0:T(8,128)(2,1)}), bf16[4,32,2048]{2,1,0:T(8,128)(2,1)}, u32[]{:S(2)}, u32[]{:S(2)}) async-start(bf16[4,32,2048]{2,1,0:T(8,128)(2,1)} %get-tuple-element.22), calls=%async_computation | async-start | bytes 1048576 | tf_op jit(solution)/shard_map/all_to_all | solution.py:246
  54.5 14.8 %collective-permute-start.12 = (bf16[3,64,1152]{2,1,0:T(8,128)(2,1)S(1)}, bf16[3,64,1152]{2,1,0:T(8,128)(2,1)}, u32[]{:S(2)}, u32[]{:S(2)}) collective-permute-start(bf16[3,64,1152]{2,1,0:T(8,128)(2,1)S(1)} %pad_maximum_fusion.refs_7_), channel_id=1, source_target_pairs={{0,24},{8,0},{16,8},{24,16},{1,25},{9,1},{17,9},{25,17},{2,26},{10... | collective-permute-start | bytes 1327112 | tf_op jit(solution)/shard_map/ppermute | solution.py:188
  57.9 41.0 %collective-permute-start.6 = (bf16[5,64,1152]{2,1,0:T(8,128)(2,1)S(1)}, bf16[5,64,1152]{2,1,0:T(8,128)(2,1)S(1)}, u32[]{:S(2)}, u32[]{:S(2)}) collective-permute-start(bf16[5,64,1152]{2,1,0:T(8,128)(2,1)S(1)} %bitcast_dynamic-update-slice_fusion.refs_3_), channel_id=1, source_target_pairs={{0,24},{8,0},{16,8},{24,16},{1,25},{9,1},{17,9},{25,17},{2,26},{10... | collective-permute-start | bytes 2211848 | tf_op jit(solution)/shard_map/ppermute | solution.py:188
  61.3 37.7 %collective-permute-start.7 = (bf16[5,64,1152]{2,1,0:T(8,128)(2,1)S(1)}, bf16[5,64,1152]{2,1,0:T(8,128)(2,1)S(1)}, u32[]{:S(2)}, u32[]{:S(2)}) collective-permute-start(bf16[5,64,1152]{2,1,0:T(8,128)(2,1)S(1)} %collective-permute-done.5.refs_4_), channel_id=1, source_target_pairs={{0,8},{8,16},{16,24},{24,0},{1,9},{9,17},{17,25},{25,1},{2,10},{10... | collective-permute-start | bytes 2211848 | tf_op jit(solution)/shard_map/ppermute | solution.py:188
  63.2 35.7 %collective-permute-start = (bf16[128,2048]{1,0:T(8,128)(2,1)}, bf16[128,2048]{1,0:T(8,128)(2,1)S(1)}, u32[]{:S(2)}, u32[]{:S(2)}) collective-permute-start(bf16[128,2048]{1,0:T(8,128)(2,1)} %bitcast.11.refs_1_), channel_id=1, source_target_pairs={{0,1},{1,0},{2,3},{3,2},{4,5},{5,4},{6,7},{7,6},{8,9},{9,8},{10,11... | collective-permute-start | bytes 1572872 | tf_op jit(solution)/shard_map/ppermute | solution.py:242
  67.3 29.6 %collective-permute-start.11 = (bf16[3,64,1152]{2,1,0:T(8,128)(2,1)S(1)}, bf16[3,64,1152]{2,1,0:T(8,128)(2,1)S(1)}, u32[]{:S(2)}, u32[]{:S(2)}) collective-permute-start(bf16[3,64,1152]{2,1,0:T(8,128)(2,1)S(1)} %pad_maximum_fusion.refs_7_), channel_id=1, source_target_pairs={{0,8},{8,16},{16,24},{24,0},{1,9},{9,17},{17,25},{25,1},{2,10},{10... | collective-permute-start | bytes 1327112 | tf_op jit(solution)/shard_map/ppermute | solution.py:188
  69.4 29.5 %collective-permute-start.13 = (bf16[3,64,1152]{2,1,0:T(8,128)(2,1)}, bf16[3,64,1152]{2,1,0:T(8,128)(2,1)S(1)}, u32[]{:S(2)}, u32[]{:S(2)}) collective-permute-start(bf16[3,64,1152]{2,1,0:T(8,128)(2,1)} %collective-permute-done.12.refs_9_), channel_id=1, source_target_pairs={{0,24},{8,0},{16,8},{24,16},{1,25},{9,1},{17,9},{25,17},{2,26},{10... | collective-permute-start | bytes 1327112 | tf_op jit(solution)/shard_map/ppermute | solution.py:188
  73.9 25.0 %copy-start.9 = (f32[8,384]{1,0:T(8,128)S(1)}, f32[8,384]{1,0:T(8,128)}, u32[]{:S(2)}) copy-start(f32[8,384]{1,0:T(8,128)} %get-tuple-element.21.refs_0_.small) | copy-start | bytes 36868
  97.0 5.2 %copy-start = (bf16[3,64,1152]{2,1,0:T(8,128)(2,1)}, bf16[3,64,1152]{2,1,0:T(8,128)(2,1)S(1)}, u32[]{:S(2)}) copy-start(bf16[3,64,1152]{2,1,0:T(8,128)(2,1)S(1)} %collective-permute-done.11.refs_8_) | copy-start | bytes 1327108
  97.0 14.7 %collective-permute-start.16 = (bf16[256,1024]{1,0:T(8,128)(2,1)}, bf16[256,1024]{1,0:T(8,128)(2,1)}, u32[]{:S(2)}, u32[]{:S(2)}) collective-permute-start(bf16[256,1024]{1,0:T(8,128)(2,1)} %bitcast.22.rest_0_), channel_id=1, source_target_pairs={{0,32},{32,64},{64,96},{96,128},{128,160},{160,192},{192,224},{224... | collective-permute-start | bytes 1572872 | tf_op jit(solution)/shard_map/ppermute | solution.py:184
  98.9 3.2 %copy-start.2 = (bf16[3,64,1152]{2,1,0:T(8,128)(2,1)}, bf16[3,64,1152]{2,1,0:T(8,128)(2,1)S(1)}, u32[]{:S(2)}) copy-start(bf16[3,64,1152]{2,1,0:T(8,128)(2,1)S(1)} %collective-permute-done.13.refs_10_) | copy-start | bytes 1327108
  102.2 11.4 %collective-permute-start.14 = (bf16[128,2048]{1,0:T(8,128)(2,1)S(1)}, bf16[128,2048]{1,0:T(8,128)(2,1)S(1)}, u32[]{:S(2)}, u32[]{:S(2)}) collective-permute-start(bf16[128,2048]{1,0:T(8,128)(2,1)S(1)} %get-tuple-element.25), channel_id=1, source_target_pairs={{0,1},{1,0},{2,3},{3,2},{4,5},{5,4},{6,7},{7,6},{8,9},{9,8},{10,11... | collective-permute-start | bytes 1572872 | tf_op jit(solution)/shard_map/ppermute | solution.py:242
  106.7 16.4 %collective-permute-start.19 = (bf16[256,1024]{1,0:T(8,128)(2,1)}, bf16[256,1024]{1,0:T(8,128)(2,1)}, u32[]{:S(2)}, u32[]{:S(2)}) collective-permute-start(bf16[256,1024]{1,0:T(8,128)(2,1)} %bitcast.22.rest_0_), channel_id=1, source_target_pairs={{0,480},{32,0},{64,32},{96,64},{128,96},{160,128},{192,160},{224,1... | collective-permute-start | bytes 1572872 | tf_op jit(solution)/shard_map/ppermute | solution.py:184
  111.6 15.7 %collective-permute-start.17 = (bf16[256,1024]{1,0:T(8,128)(2,1)}, bf16[256,1024]{1,0:T(8,128)(2,1)}, u32[]{:S(2)}, u32[]{:S(2)}) collective-permute-start(bf16[256,1024]{1,0:T(8,128)(2,1)} %collective-permute-done.16.rest_1_), channel_id=1, source_target_pairs={{0,32},{32,64},{64,96},{96,128},{128,160},{160,192},{192,224},{224... | collective-permute-start | bytes 1572872 | tf_op jit(solution)/shard_map/ppermute | solution.py:184
  114.5 17.1 %copy-start.5 = (f32[3,2048]{1,0:T(4,128)S(1)}, f32[3,2048]{1,0:T(4,128)}, u32[]{:S(2)}) copy-start(f32[3,2048]{1,0:T(4,128)} %get-tuple-element.27.refs_2_) | copy-start | bytes 73732
  114.5 17.1 %copy-start.8 = (bf16[32,2048]{1,0:T(8,128)(2,1)S(1)}, bf16[32,2048]{1,0:T(8,128)(2,1)}, u32[]{:S(2)}) copy-start(bf16[32,2048]{1,0:T(8,128)(2,1)} %get-tuple-element.26.refs_1_) | copy-start | bytes 393220
  114.5 17.1 %all-to-all-start.1 = ((bf16[4,32,2048]{2,1,0:T(8,128)(2,1)}), bf16[4,32,2048]{2,1,0:T(8,128)(2,1)}, u32[]{:S(2)}, u32[]{:S(2)}) async-start(bf16[4,32,2048]{2,1,0:T(8,128)(2,1)} %bitcast.34), calls=%async_computation.1 | async-start | bytes 1048576 | tf_op jit(solution)/shard_map/all_to_all | solution.py:255
  123.2 20.7 %collective-permute-start.20 = (bf16[256,1024]{1,0:T(8,128)(2,1)}, bf16[256,1024]{1,0:T(8,128)(2,1)}, u32[]{:S(2)}, u32[]{:S(2)}) collective-permute-start(bf16[256,1024]{1,0:T(8,128)(2,1)} %collective-permute-done.19.rest_5_), channel_id=1, source_target_pairs={{0,448},{32,480},{64,0},{96,32},{128,64},{160,96},{192,128},{224,1... | collective-permute-start | bytes 1572872 | tf_op jit(solution)/shard_map/ppermute | solution.py:184
  127.3 16.6 %collective-permute-start.18 = (bf16[256,1024]{1,0:T(8,128)(2,1)}, bf16[256,1024]{1,0:T(8,128)(2,1)}, u32[]{:S(2)}, u32[]{:S(2)}) collective-permute-start(bf16[256,1024]{1,0:T(8,128)(2,1)} %collective-permute-done.17.rest_2_), channel_id=1, source_target_pairs={{0,32},{32,64},{64,96},{96,128},{128,160},{160,192},{192,224},{224... | collective-permute-start | bytes 1572872 | tf_op jit(solution)/shard_map/ppermute | solution.py:184
  133.1 0.8 copy-start.4
  133.9 0.7 copy-start.6
  134.6 24.5 %all-to-all-start.2 = ((bf16[4,32,2048]{2,1,0:T(8,128)(2,1)}), bf16[4,32,2048]{2,1,0:T(8,128)(2,1)}, u32[]{:S(2)}, u32[]{:S(2)}) async-start(bf16[4,32,2048]{2,1,0:T(8,128)(2,1)} %copy-done.4), calls=%async_computation.2 | async-start | bytes 1048576 | tf_op jit(solution)/shard_map/all_to_all | solution.py:246
  138.7 30.6 %copy-start.10 = (f32[8,384]{1,0:T(8,128)S(1)}, f32[8,384]{1,0:T(8,128)}, u32[]{:S(2)}) copy-start(f32[8,384]{1,0:T(8,128)} %get-tuple-element.21.refs_0_.small) | copy-start | bytes 36868
  138.8 25.2 %collective-permute-start.22 = (bf16[256,1024]{1,0:T(8,128)(2,1)}, bf16[256,1024]{1,0:T(8,128)(2,1)}, u32[]{:S(2)}, u32[]{:S(2)}) collective-permute-start(bf16[256,1024]{1,0:T(8,128)(2,1)} %collective-permute-done.19.rest_5_), channel_id=1, source_target_pairs={{0,480},{32,0},{64,32},{96,64},{128,96},{160,128},{192,160},{224,1... | collective-permute-start | bytes 1572872 | tf_op jit(solution)/shard_map/ppermute | solution.py:184
  145.9 23.4 %collective-permute-start.21 = (bf16[256,1024]{1,0:T(8,128)(2,1)}, bf16[256,1024]{1,0:T(8,128)(2,1)}, u32[]{:S(2)}, u32[]{:S(2)}) collective-permute-start(bf16[256,1024]{1,0:T(8,128)(2,1)} %pick.1), channel_id=1, source_target_pairs={{0,32},{1,481},{32,64},{33,1},{64,96},{65,33},{96,128},{97,65},{12... | collective-permute-start | bytes 1572872 | tf_op jit(solution)/shard_map/ppermute | solution.py:237
  159.1 10.3 %collective-permute-start.15 = (bf16[128,2048]{1,0:T(8,128)(2,1)}, bf16[128,2048]{1,0:T(8,128)(2,1)S(1)}, u32[]{:S(2)}, u32[]{:S(2)}) collective-permute-start(bf16[128,2048]{1,0:T(8,128)(2,1)} %bitcast.21.own_rows), channel_id=1, source_target_pairs={{0,1},{1,0},{2,3},{3,2},{4,5},{5,4},{6,7},{7,6},{8,9},{9,8},{10,11... | collective-permute-start | bytes 1572872 | tf_op jit(solution)/shard_map/ppermute | solution.py:242
  173.9 3.8 %collective-permute-start.23 = (bf16[128,2048]{1,0:T(8,128)(2,1)S(1)}, bf16[128,2048]{1,0:T(8,128)(2,1)S(1)}, u32[]{:S(2)}, u32[]{:S(2)}) collective-permute-start(bf16[128,2048]{1,0:T(8,128)(2,1)S(1)} %get-tuple-element.31), channel_id=1, source_target_pairs={{0,1},{1,0},{2,3},{3,2},{4,5},{5,4},{6,7},{7,6},{8,9},{9,8},{10,11... | collective-permute-start | bytes 1572872 | tf_op jit(solution)/shard_map/ppermute | solution.py:242
  177.8 13.1 %copy-start.7 = (f32[32,2048]{1,0:T(8,128)S(1)}, f32[32,2048]{1,0:T(8,128)}, u32[]{:S(2)}) copy-start(f32[32,2048]{1,0:T(8,128)} %copy-done.6) | copy-start | bytes 786436
  191.3 16.4 %copy-start.1 = (bf16[3,64,1152]{2,1,0:T(8,128)(2,1)S(1)}, bf16[3,64,1152]{2,1,0:T(8,128)(2,1)}, u32[]{:S(2)}) copy-start(bf16[3,64,1152]{2,1,0:T(8,128)(2,1)} %copy-done) | copy-start | bytes 1327108
  191.3 16.4 %copy-start.3 = (bf16[3,64,1152]{2,1,0:T(8,128)(2,1)S(1)}, bf16[3,64,1152]{2,1,0:T(8,128)(2,1)}, u32[]{:S(2)}) copy-start(bf16[3,64,1152]{2,1,0:T(8,128)(2,1)} %copy-done.2) | copy-start | bytes 1327108
  202.2 5.5 %collective-permute-start.24 = (bf16[128,2048]{1,0:T(8,128)(2,1)S(1)}, bf16[128,2048]{1,0:T(8,128)(2,1)S(1)}, u32[]{:S(2)}, u32[]{:S(2)}) collective-permute-start(bf16[128,2048]{1,0:T(8,128)(2,1)S(1)} %bitcast.32), channel_id=1, source_target_pairs={{0,1},{1,0},{2,3},{3,2},{4,5},{5,4},{6,7},{7,6},{8,9},{9,8},{10,11... | collective-permute-start | bytes 1572872 | tf_op jit(solution)/shard_map/ppermute | solution.py:242
  210.6 3.8 %collective-permute-start.25 = (bf16[128,2048]{1,0:T(8,128)(2,1)S(1)}, bf16[128,2048]{1,0:T(8,128)(2,1)S(1)}, u32[]{:S(2)}, u32[]{:S(2)}) collective-permute-start(bf16[128,2048]{1,0:T(8,128)(2,1)S(1)} %get-tuple-element.35), channel_id=1, source_target_pairs={{0,1},{1,0},{2,3},{3,2},{4,5},{5,4},{6,7},{7,6},{8,9},{9,8},{10,11... | collective-permute-start | bytes 1572872 | tf_op jit(solution)/shard_map/ppermute | solution.py:242
